TPU v7x, 32 devices: a whole 2x2x4 slice. The times are simulated.
32 devices in a mesh: kv: 16 (over z, y, core), tp: 2 (over x).
Axes of the slice: x: 2, y: 2, z: 4, core: 2. Of those that a mesh axis runs over, the one named last changes fastest.
Arguments:
- queries: bfloat16 [4096, 4, 128], P('kv', 'tp'), may hold values from -6 to 6
- keys: bfloat16 [4096, 4, 128], P('kv', 'tp'), may hold values from -6 to 6
- values: bfloat16 [4096, 4, 128], P('kv', 'tp'), may hold values from -6 to 6
- attended: bfloat16 [4096, 4, 128], P('kv', 'tp'), may hold values from -6 to 6
- out_grad: bfloat16 [4096, 4, 128], P('kv', 'tp'), may hold values from -6 to 6
- log_sum: float32 [4096, 4], P('kv', 'tp'), may hold values from 2.5 to 4.5
- picked: int32 [32, 16], P('kv'), may hold values from -1 to 127, as said below
- layer_input: bfloat16 [4096, 4096], P('kv'), may hold values from -0.03125 to 0.03125
Outputs:
- query_grad: float32 [4096, 4, 128], P('kv', 'tp')
- key_grad: float32 [4096, 4, 128], P('kv', 'tp')
- value_grad: float32 [4096, 4, 128], P('kv', 'tp')
- weight_grad: float32 [4096, 512], P('kv', 'tp')
Inputs may be any that keep to these rules, and one draw needn't show every extreme that they name: Row r lists distinct key block numbers picked by query block r, followed by -1 to the end of the row; at least one entry is not -1, and at most 16 are. No picked block starts after the last position of its query block. With the span of a position being the position divided by 256 (rounded down), the span of every picked block is the query block's span or that span less 1, 2, 4, 8 and so on. The query blocks of one span pick at most 4 distinct blocks from any other single span.
All inputs are finite; a program needn't handle non-finite values.
Results may differ from a plain program's by a relative error of at most 0.004.
Values may be sent and summed in bfloat16 or wider, within the bound.
No kernel may reach another device: no remote copies, remote signals or barrier semaphores. Data moves between devices by JAX's collectives and lax.ppermute only.
A program may use at most 64 MiB of HBM per device.

v0:
```python
import functools

import jax
import jax.numpy as jnp
from jax import lax
from jax.experimental import pallas as pl
from jax.experimental.pallas import tpu as pltpu
from jax.sharding import PartitionSpec as P

QB = 128
KB = 32
F32 = jnp.float32
BF16 = jnp.bfloat16
VMEM = pl.BlockSpec(memory_space=pltpu.VMEM)
SMEM = pl.BlockSpec(memory_space=pltpu.SMEM)


def ring(value, by):
    count = lax.axis_size("kv")
    return lax.ppermute(value, "kv", [(i, (i + by) % count) for i in range(count)])


def swap(value, bit):
    count = lax.axis_size("kv")
    return lax.ppermute(value, "kv", [(i, i ^ bit) for i in range(count)])


def call(body, out_shape, specs, flops, nbytes):
    return pl.pallas_call(
        body,
        out_shape=out_shape,
        in_specs=specs,
        out_specs=jax.tree.map(lambda _: VMEM, out_shape),
        cost_estimate=pl.CostEstimate(flops=flops, bytes_accessed=nbytes, transcendentals=0),
    )


def nt(a, b):
    return lax.dot_general(a, b, (((1,), (1,)), ((), ())), preferred_element_type=F32)


def tn(a, b):
    return lax.dot_general(a, b, (((0,), (0,)), ((), ())), preferred_element_type=F32)


def nn(a, b):
    return lax.dot_general(a, b, (((1,), (0,)), ((), ())), preferred_element_type=F32)


def layout(tok, heads, sel):
    blocks = tok // QB
    codes = 2 * heads * tok
    stats = codes + blocks * sel
    per = -(-6 * heads // 16) * 16
    return blocks, codes, stats, per, stats + blocks * per


def thirds(row):
    high = row.astype(BF16).astype(F32)
    rest = row - high
    middle = rest.astype(BF16).astype(F32)
    return [high, middle, rest - middle]


def pack_body(levels, me_ref, picked_ref, q_ref, g_ref, a_ref, lse_ref, msg_ref):
    tok, heads, dim = q_ref.shape
    sel = picked_ref.shape[1]
    span_blocks = tok // KB
    blocks, codes, stats, per, _ = layout(tok, heads, sel)
    me = me_ref[0]
    rows = lax.broadcasted_iota(jnp.int32, (sel, QB), 0)
    for b in range(blocks):
        code = jnp.full((sel, QB), -1, jnp.int32)
        for p in range(sel):
            block = picked_ref[b, p]
            span = lax.div(jnp.maximum(block, 0), span_blocks)
            group = jnp.int32(0)
            for level in range(levels):
                group += ((me - span) >= (1 << level)).astype(jnp.int32)
            value = jnp.where(block < 0, -1, group * span_blocks + block - span * span_blocks)
            code = jnp.where(rows == p, value, code)
        msg_ref[codes + b * sel : codes + (b + 1) * sel, :] = code.astype(F32).astype(BF16)
    table = [[] for _ in range(blocks)]
    for h in range(heads):
        query = q_ref[:, h, :]
        grad = g_ref[:, h, :]
        msg_ref[h * tok : (h + 1) * tok, :] = query
        msg_ref[(heads + h) * tok : (heads + h + 1) * tok, :] = grad
        product = grad.astype(F32) * a_ref[:, h, :].astype(F32)
        for b in range(blocks):
            part = product[b * QB : (b + 1) * QB, :]
            dots = jnp.sum(part.T, axis=0, keepdims=True)
            table[b] += thirds(lse_ref[h : h + 1, b * QB : (b + 1) * QB]) + thirds(dots)
    for b in range(blocks):
        at = stats + b * per
        filled = table[b] + [jnp.zeros((per - 6 * heads, QB), F32)]
        msg_ref[at : at + per, :] = jnp.concatenate(filled, axis=0).astype(BF16)


def unsplit(rows):
    return (rows[0:1] + rows[1:2]) + rows[2:3]


def group_terms(msg_ref, key_of, value_of, group, tok, heads, dim, sel, causal, out):
    blocks, codes, stats, per, _ = layout(tok, heads, sel)
    span_blocks = tok // KB
    scale = dim ** (-0.5)
    lives, lse, dots = [], [[] for _ in range(heads)], [[] for _ in range(heads)]
    for b in range(blocks):
        code = msg_ref[codes + b * sel : codes + (b + 1) * sel, :].astype(F32)
        rows = []
        for k in range(span_blocks):
            hit = jnp.max(jnp.where(code == float(group * span_blocks + k), 1.0, 0.0), axis=0, keepdims=True)
            rows.append(jnp.broadcast_to(hit, (KB, QB)))
        lives.append(jnp.concatenate(rows, axis=0))
        stat = msg_ref[stats + b * per : stats + (b + 1) * per, :].astype(F32)
        for h in range(heads):
            lse[h].append(unsplit(stat[6 * h : 6 * h + 3]))
            dots[h].append(unsplit(stat[6 * h + 3 : 6 * h + 6]))
    live = jnp.concatenate(lives, axis=1) > 0.5
    if causal:
        key_pos = lax.broadcasted_iota(jnp.int32, (tok, tok), 0)
        query_pos = lax.broadcasted_iota(jnp.int32, (tok, tok), 1)
        live = live & (key_pos <= query_pos)
    for h in range(heads):
        query = msg_ref[h * tok : (h + 1) * tok, :]
        grad = msg_ref[(heads + h) * tok : (heads + h + 1) * tok, :]
        key, value = key_of(h), value_of(h)
        scores = nt(key, query) * scale
        weights = jnp.where(live, jnp.exp(scores - jnp.concatenate(lse[h], axis=1)), 0.0)
        slopes = nt(value, grad)
        score_grad = weights * (slopes - jnp.concatenate(dots[h], axis=1))
        weight_pairs = weights.astype(BF16)
        grad_pairs = score_grad.astype(BF16)
        out(h, nn(grad_pairs, query), nn(weight_pairs, grad), tn(grad_pairs, key))


def own_body(sel, msg_ref, k_ref, v_ref, kv_ref, dk_ref, dv_ref, dq_ref):
    tok, heads, dim = k_ref.shape
    for h in range(heads):
        kv_ref[h * tok : (h + 1) * tok, :] = k_ref[:, h, :]
        kv_ref[(heads + h) * tok : (heads + h + 1) * tok, :] = v_ref[:, h, :]

    def out(h, dk, dv, dq):
        at = slice(h * tok, (h + 1) * tok)
        dk_ref[at, :] = dk
        dv_ref[at, :] = dv
        dq_ref[at, :] = dq

    group_terms(
        msg_ref,
        lambda h: kv_ref[h * tok : (h + 1) * tok, :],
        lambda h: kv_ref[(heads + h) * tok : (heads + h + 1) * tok, :],
        0, tok, heads, dim, sel, True, out,
    )


def far_body(sel, tok, heads, groups, *refs):
    count = len(groups)
    msgs = refs[:count]
    kv_ref, dk_in, dv_in = refs[count : count + 3]
    dk_out, dv_out, round_ref = refs[count + 3 : count + 6]
    dqs = refs[count + 6 : count + 6 + count]
    dk_sum, dv_sum = refs[count + 6 + count :]
    dim = kv_ref.shape[1]
    scale = dim ** (-0.5)
    for index, group in enumerate(groups):

        def out(h, dk, dv, dq):
            at = slice(h * tok, (h + 1) * tok)
            dk_sum[at, :] = (dk_sum if index else dk_in)[at, :] + dk
            dv_sum[at, :] = (dv_sum if index else dv_in)[at, :] + dv
            dqs[index][at, :] = dq.astype(BF16)

        group_terms(
            msgs[index],
            lambda h: kv_ref[h * tok : (h + 1) * tok, :],
            lambda h: kv_ref[(heads + h) * tok : (heads + h + 1) * tok, :],
            group, tok, heads, dim, sel, False, out,
        )
    for h in range(heads):
        at = slice(h * tok, (h + 1) * tok)
        dk_out[:, h, :] = dk_sum[at, :] * scale
        dv = dv_sum[at, :]
        dv_out[:, h, :] = dv
        round_ref[:, h * dim : (h + 1) * dim] = dv.astype(BF16)


def query_body(dq_ref, *refs):
    out_ref = refs[-1]
    tok, heads, dim = out_ref.shape
    scale = dim ** (-0.5)
    for h in range(heads):
        at = slice(h * tok, (h + 1) * tok)
        total = dq_ref[at, :]
        for ref in refs[:-1]:
            total = total + ref[at, :].astype(F32)
        out_ref[:, h, :] = total * scale


def pieces_body(near, far, me_ref, x_ref, *out_refs):
    rank = lax.rem(me_ref[0], near)
    width = x_ref.shape[1] // (near * far)
    for index, ref in enumerate(out_refs):
        target = rank ^ (index + 1)
        for z in range(far):
            at = pl.multiple_of((z * near + target) * width, width)
            ref[:, z * width : (z + 1) * width] = x_ref[:, pl.ds(at, width)]


def weight_body(near, far, parity, out_type, me_ref, x_ref, *refs):
    pieces = refs[: near - 1]
    rounds_ref, out_ref = refs[near - 1 :]
    me = me_ref[0]
    rank, depth = lax.rem(me, near), lax.div(me, near)
    tok = x_ref.shape[0]
    width = x_ref.shape[1] // (near * far)
    step = 2 if parity is not None else 1
    for index, rel in enumerate(range(parity or 0, far, step)):
        z = depth ^ rel
        at = pl.multiple_of((z * near + rank) * width, width)
        total = tn(x_ref[:, pl.ds(at, width)], rounds_ref[pl.ds(pl.multiple_of(rank * tok, tok), tok), :])
        for m in range(1, near):
            left = pieces[m - 1][:, pl.ds(pl.multiple_of(z * width, width), width)]
            right = rounds_ref[pl.ds(pl.multiple_of((rank ^ m) * tok, tok), tok), :]
            total += tn(left, right)
        out_ref[index * width : (index + 1) * width, :] = total.astype(out_type)


def per_device(queries, keys, values, attended, out_grad, log_sum, picked, layer_input):
    tok, heads, dim = queries.shape
    sel = picked.shape[1]
    count = lax.axis_size("kv")
    levels = count.bit_length() - 1
    near = 1 << (levels // 2)
    far = count // near
    me = lax.axis_index("kv").astype(jnp.int32).reshape(1)
    rows = heads * tok
    msg_rows = layout(tok, heads, sel)[-1]

    def shape(dims, kind):
        return jax.ShapeDtypeStruct(dims, kind)

    pairs = tok * tok * dim * heads * 10
    msg = call(
        functools.partial(pack_body, levels),
        shape((msg_rows, dim), BF16),
        [SMEM, SMEM, VMEM, VMEM, VMEM, VMEM],
        1 << 20, 4 * rows * dim * 2,
    )(me, picked, queries, out_grad, attended, log_sum.T)
    got = [ring(msg, -(1 << level)) for level in range(levels)]
    width = layer_input.shape[1] // count
    blocked = width % 128 == 0 and far > 1
    if blocked:
        sent = call(
            functools.partial(pieces_body, near, far),
            [shape((tok, far * width), BF16)] * (near - 1),
            [SMEM, VMEM],
            1 << 20, 2 * layer_input.size * 2,
        )(me, layer_input)
        pieces = [swap(piece, m + 1) for m, piece in enumerate(sent)]
    kv, dk_own, dv_own, dq_own = call(
        functools.partial(own_body, sel),
        [shape((2 * rows, dim), BF16)] + [shape((rows, dim), F32)] * 3,
        [VMEM] * 3,
        pairs, 8 * rows * dim * 4,
    )(msg, keys, values)
    groups = tuple(range(1, levels + 1))
    outs = pl.pallas_call(
        functools.partial(far_body, sel, tok, heads, groups),
        out_shape=[shape((tok, heads, dim), F32)] * 2
        + [shape((tok, heads * dim), BF16)]
        + [shape((rows, dim), BF16)] * levels,
        in_specs=[VMEM] * (levels + 3),
        out_specs=[VMEM] * (levels + 3),
        scratch_shapes=[pltpu.VMEM((rows, dim), F32)] * 2,
        cost_estimate=pl.CostEstimate(
            flops=pairs * levels, bytes_accessed=levels * 8 * rows * dim, transcendentals=0
        ),
    )(*got, kv, dk_own, dv_own)
    key_grad, value_grad, rounded = outs[:3]
    sides = outs[3:]
    if blocked:
        bunches = [[g * near + r for r in range(near)] for g in range(far)]
        rounds = lax.all_gather(rounded, "kv", axis_index_groups=bunches, tiled=True)

        def weight(parity, kind):
            blocks = far // 2 if parity is not None else far
            return call(
                functools.partial(weight_body, near, far, parity, kind),
                shape((blocks * width, heads * dim), kind),
                [SMEM] + [VMEM] * (near + 1),
                2 * near * tok * blocks * width * heads * dim, layer_input.size * 2,
            )(me, layer_input, *pieces, rounds)

        send = weight(1, BF16)
        keep = weight(0, F32)
        bit = near
        total = keep + swap(send, bit).astype(F32)
        left = far // 2
        while left > 1:
            bit *= 2
            stacked = total.reshape(left // 2, 2, width, heads * dim)
            send = stacked[:, 1].reshape(-1, heads * dim).astype(BF16)
            total = stacked[:, 0].reshape(-1, heads * dim) + swap(send, bit).astype(F32)
            left //= 2
    else:
        terms = lax.dot_general(
            layer_input, rounded, (((0,), (0,)), ((), ())), preferred_element_type=F32
        )
        total = lax.psum_scatter(terms, "kv", scatter_dimension=0, tiled=True)
    back = [ring(side, 1 << level) for level, side in enumerate(sides)]
    query_grad = call(
        query_body, shape((tok, heads, dim), F32), [VMEM] * (levels + 1), 1 << 20, rows * dim * 16
    )(dq_own, *back)
    return query_grad, key_grad, value_grad, total


def solution(mesh):
    placed = (
        P("kv", "tp", None),
        P("kv", "tp", None),
        P("kv", "tp", None),
        P("kv", "tp", None),
        P("kv", "tp", None),
        P("kv", "tp"),
        P("kv", None),
        P("kv", None),
    )
    return jax.shard_map(
        per_device,
        mesh=mesh,
        in_specs=placed,
        out_specs=(P("kv", "tp", None), P("kv", "tp", None), P("kv", "tp", None), P("kv", "tp")),
        check_vma=False,
    )
```

profile of v0, /device:TPU:4, one launch (start us, length us, event | category | flops | bytes accessed | tf_op | source)
XLA Modules:
  0.0 97.1 jit_solution(3643336735699504198)
XLA Ops:
  0.6 3.6 %shard_map.111.msg_ref = bf16[1088,128]{1,0:T(8,128)(2,1)} custom-call(s32[1]{0:T(128)} %bitcast.me_ref, s32[2,16]{1,0:T(2,128)} %picked_ref.1, bf16[256,2,128]{2,1,0:T(2,128)(2,1)} %q_ref.1, bf16[256,2,128]{2,1,0:T(2,128)(2,1)} %g_ref.1, bf16[256,2,128]{2,1,0:T(2,128)(2,1)} %a_ref.1, f32[2,256]{1,0:T(2,128)} %bitcast.11), custom_call_target="tpu_custom_call" | custom-call | flops 1048576 | bytes 524288 | tf_op jit(solution)/shard_map/pallas_call | solution.py:245
  4.2 2.6 %collective-permute-start.3 = (bf16[1088,128]{1,0:T(8,128)(2,1)}, bf16[1088,128]{1,0:T(8,128)(2,1)S(1)}, u32[]{:S(2)}, u32[]{:S(2)}) collective-permute-start(bf16[1088,128]{1,0:T(8,128)(2,1)} %shard_map.111.msg_ref), channel_id=1, source_target_pairs={{0,16},{2,18},{4,20},{6,22},{8,24},{10,26},{12,28},{14,30},{16,0},... | collective-permute-start | bytes 835592 | tf_op jit(solution)/shard_map/ppermute | solution.py:20
  6.8 1.3 %collective-permute-start.2 = (bf16[1088,128]{1,0:T(8,128)(2,1)}, bf16[1088,128]{1,0:T(8,128)(2,1)S(1)}, u32[]{:S(2)}, u32[]{:S(2)}) collective-permute-start(bf16[1088,128]{1,0:T(8,128)(2,1)} %shard_map.111.msg_ref), channel_id=1, source_target_pairs={{0,24},{2,26},{4,28},{6,30},{8,0},{10,2},{12,4},{14,6},{16,8},{18,... | collective-permute-start | bytes 835592 | tf_op jit(solution)/shard_map/ppermute | solution.py:20
  8.1 0.5 collective-permute-start.1
  8.6 0.0 collective-permute-start
  8.7 3.0 %shard_map.115 = (bf16[256,1024]{1,0:T(8,128)(2,1)}, bf16[256,1024]{1,0:T(8,128)(2,1)}, bf16[256,1024]{1,0:T(8,128)(2,1)}) custom-call(s32[1]{0:T(128)} %bitcast.me_ref, bf16[256,4096]{1,0:T(8,128)(2,1)} %x_ref.5), custom_call_target="tpu_custom_call" | custom-call | flops 1048576 | bytes 4194304 | tf_op jit(solution)/shard_map/pallas_call | solution.py:255
  11.7 0.5 collective-permute-start.8
  12.2 8.7 %collective-permute-done.3.refs_3_ = bf16[1088,128]{1,0:T(8,128)(2,1)S(1)} collective-permute-done((bf16[1088,128]{1,0:T(8,128)(2,1)}, bf16[1088,128]{1,0:T(8,128)(2,1)S(1)}, u32[]{:S(2)}, u32[]{:S(2)}) %collective-permute-start.3) | collective-permute-done | bytes 278560 | tf_op jit(solution)/shard_map/ppermute | solution.py:20
  20.8 0.2 collective-permute-start.9
  21.0 3.3 %shard_map.112 = (bf16[1024,128]{1,0:T(8,128)(2,1)}, f32[512,128]{1,0:T(8,128)}, f32[512,128]{1,0:T(8,128)}, f32[512,128]{1,0:T(8,128)}) custom-call(bf16[1088,128]{1,0:T(8,128)(2,1)} %shard_map.111.msg_ref, bf16[256,2,128]{2,1,0:T(2,128)(2,1)} %k_ref.1, bf16[256,2,128]{2,1,0:T(2,128)(2,1)} %v_ref.1), custom_call_target="tpu_custom_call" | custom-call | flops 167772160 | bytes 2097152 | tf_op jit(solution)/shard_map/pallas_call | solution.py:262
  24.4 1.6 %collective-permute-done.1.refs_1_ = bf16[1088,128]{1,0:T(8,128)(2,1)S(1)} collective-permute-done((bf16[1088,128]{1,0:T(8,128)(2,1)}, bf16[1088,128]{1,0:T(8,128)(2,1)S(1)}, u32[]{:S(2)}, u32[]{:S(2)}) %collective-permute-start.1) | collective-permute-done | bytes 278560 | tf_op jit(solution)/shard_map/ppermute | solution.py:20
  26.0 0.7 copy-done.9
  26.6 0.1 copy-done.10
  26.7 4.8 %shard_map.113 = (f32[256,2,128]{2,1,0:T(2,128)}, f32[256,2,128]{2,1,0:T(2,128)}, bf16[256,256]{1,0:T(8,128)(2,1)}, bf16[512,128]{1,0:T(8,128)(2,1)}, bf16[512,1...) custom-call(bf16[1088,128]{1,0:T(8,128)(2,1)} %copy-done.10, bf16[1088,128]{1,0:T(8,128)(2,1)} %copy-done.9, ...), custom_call_target="tpu_custom_call" | custom-call | flops 671088640 | bytes 2097152 | tf_op jit(solution)/shard_map/pallas_call | solution.py:269
  31.5 23.9 %all_gather.3.refs_3_ = bf16[1024,256]{1,0:T(8,128)(2,1)} all-gather(bf16[256,256]{1,0:T(8,128)(2,1)} %get-tuple-element.31), channel_id=1, replica_groups={{0,2,4,6},{8,10,12,14},{16,18,20,22},{24,26,28,30},{1,3,5,7},{9,11,13,1..., dimensions={0}, use_global_device_ids=true | all-gather | bytes 655360 | tf_op jit(solution)/shard_map/all_gather | solution.py:285
  55.5 0.8 copy-done
  56.2 0.2 copy-done.1
  56.4 0.8 copy-done.2
  57.2 3.4 %shard_map.117 = bf16[512,256]{1,0:T(8,128)(2,1)} custom-call(s32[1]{0:T(128)} %bitcast.me_ref, bf16[256,4096]{1,0:T(8,128)(2,1)} %x_ref.5, bf16[256,1024]{1,0:T(8,128)(2,1)} %copy-done, bf16[256,1024]{1,0:T(8,128)(2,1)} %copy-done.1, bf16[256,1024]{1,0:T(8,128)(2,1)} %copy-done.2, bf16[1024,256]{1,0:T(8,128)(2,1)} %all_gather.3.refs_3_), custom_call_target="tpu_custom_call" | custom-call | flops 268435456 | bytes 2097152 | tf_op jit(solution)/shard_map/pallas_call | solution.py:289
  60.6 8.1 %collective-permute-start.11 = (bf16[512,256]{1,0:T(8,128)(2,1)}, bf16[512,256]{1,0:T(8,128)(2,1)S(1)}, u32[]{:S(2)}, u32[]{:S(2)}) collective-permute-start(bf16[512,256]{1,0:T(8,128)(2,1)} %shard_map.117), channel_id=1, source_target_pairs={{0,8},{2,10},{4,12},{6,14},{8,0},{10,2},{12,4},{14,6},{16,24},{18,... | collective-permute-start | bytes 786440 | tf_op jit(solution)/shard_map/ppermute | solution.py:25
  68.8 0.1 collective-permute-start.4
  68.8 1.5 %collective-permute-start.5 = (bf16[512,128]{1,0:T(8,128)(2,1)S(1)}, bf16[512,128]{1,0:T(8,128)(2,1)S(1)}, u32[]{:S(2)}, u32[]{:S(2)}) collective-permute-start(bf16[512,128]{1,0:T(8,128)(2,1)S(1)} %copy-done.13), channel_id=1, source_target_pairs={{0,4},{2,6},{4,8},{6,10},{8,12},{10,14},{12,16},{14,18},{16,20},{1... | collective-permute-start | bytes 393224 | tf_op jit(solution)/shard_map/ppermute | solution.py:20
  70.3 3.6 %collective-permute-start.6 = (bf16[512,128]{1,0:T(8,128)(2,1)S(1)}, bf16[512,128]{1,0:T(8,128)(2,1)S(1)}, u32[]{:S(2)}, u32[]{:S(2)}) collective-permute-start(bf16[512,128]{1,0:T(8,128)(2,1)S(1)} %copy-done.12), channel_id=1, source_target_pairs={{0,8},{2,10},{4,12},{6,14},{8,16},{10,18},{12,20},{14,22},{16,24},... | collective-permute-start | bytes 393224 | tf_op jit(solution)/shard_map/ppermute | solution.py:20
  73.9 0.5 collective-permute-start.7
  74.4 3.5 %shard_map.116 = f32[512,256]{1,0:T(8,128)} custom-call(s32[1]{0:T(128)} %bitcast.me_ref, bf16[256,4096]{1,0:T(8,128)(2,1)} %x_ref.5, bf16[256,1024]{1,0:T(8,128)(2,1)} %copy-done, bf16[256,1024]{1,0:T(8,128)(2,1)} %copy-done.1, bf16[256,1024]{1,0:T(8,128)(2,1)} %copy-done.2, bf16[1024,256]{1,0:T(8,128)(2,1)} %all_gather.3.refs_3_), custom_call_target="tpu_custom_call" | custom-call | flops 268435456 | bytes 2097152 | tf_op jit(solution)/shard_map/pallas_call | solution.py:289
  77.9 1.1 %convert_add_fusion = f32[512,256]{1,0:T(8,128)S(1)} fusion(f32[512,256]{1,0:T(8,128)} %shard_map.116, bf16[512,256]{1,0:T(8,128)(2,1)S(1)} %collective-permute-done.11), kind=kLoop, calls=%fused_computation | loop fusion | flops 262144 | bytes 1310720 | tf_op jit(solution)/shard_map/add | solution.py:299
  79.0 2.4 %collective-permute-start.12 = (bf16[256,256]{1,0:T(8,128)(2,1)S(1)}, bf16[256,256]{1,0:T(8,128)(2,1)S(1)}, u32[]{:S(2)}, u32[]{:S(2)}) collective-permute-start(bf16[256,256]{1,0:T(8,128)(2,1)S(1)} %fusion.1), channel_id=1, source_target_pairs={{0,16},{2,18},{4,20},{6,22},{8,24},{10,26},{12,28},{14,30},{16,0},... | collective-permute-start | bytes 393224 | tf_op jit(solution)/shard_map/ppermute | solution.py:25
  81.5 3.1 %collective-permute-done.6.refs_2_ = bf16[512,128]{1,0:T(8,128)(2,1)S(1)} collective-permute-done((bf16[512,128]{1,0:T(8,128)(2,1)S(1)}, bf16[512,128]{1,0:T(8,128)(2,1)S(1)}, u32[]{:S(2)}, u32[]{:S(2)}) %collective-permute-start.6) | collective-permute-done | bytes 131104 | tf_op jit(solution)/shard_map/ppermute | solution.py:20
  84.6 9.1 %collective-permute-done.7.refs_3_ = bf16[512,128]{1,0:T(8,128)(2,1)S(1)} collective-permute-done((bf16[512,128]{1,0:T(8,128)(2,1)S(1)}, bf16[512,128]{1,0:T(8,128)(2,1)S(1)}, u32[]{:S(2)}, u32[]{:S(2)}) %collective-permute-start.7) | collective-permute-done | bytes 131104 | tf_op jit(solution)/shard_map/ppermute | solution.py:20
  93.7 0.6 copy-done.6
  94.4 2.1 %shard_map.114 = f32[256,2,128]{2,1,0:T(2,128)} custom-call(f32[512,128]{1,0:T(8,128)} %get-tuple-element.18.dq_ref, bf16[512,128]{1,0:T(8,128)(2,1)} %copy-done.3, bf16[512,128]{1,0:T(8,128)(2,1)} %copy-done.4, bf16[512,128]{1,0:T(8,128)(2,1)} %copy-done.5, bf16[512,128]{1,0:T(8,128)(2,1)} %copy-done.6), custom_call_target="tpu_custom_call" | custom-call | flops 1048576 | bytes 1048576 | tf_op jit(solution)/shard_map/pallas_call | solution.py:313
  96.4 0.7 fusion
  (35 shorter events, 0.1 us)
Async XLA Ops:
  4.2 16.6 %collective-permute-start.3 = (bf16[1088,128]{1,0:T(8,128)(2,1)}, bf16[1088,128]{1,0:T(8,128)(2,1)S(1)}, u32[]{:S(2)}, u32[]{:S(2)}) collective-permute-start(bf16[1088,128]{1,0:T(8,128)(2,1)} %shard_map.111.msg_ref), channel_id=1, source_target_pairs={{0,16},{2,18},{4,20},{6,22},{8,24},{10,26},{12,28},{14,30},{16,0},... | collective-permute-start | bytes 835592 | tf_op jit(solution)/shard_map/ppermute | solution.py:20
  6.8 14.2 %collective-permute-start.2 = (bf16[1088,128]{1,0:T(8,128)(2,1)}, bf16[1088,128]{1,0:T(8,128)(2,1)S(1)}, u32[]{:S(2)}, u32[]{:S(2)}) collective-permute-start(bf16[1088,128]{1,0:T(8,128)(2,1)} %shard_map.111.msg_ref), channel_id=1, source_target_pairs={{0,24},{2,26},{4,28},{6,30},{8,0},{10,2},{12,4},{14,6},{16,8},{18,... | collective-permute-start | bytes 835592 | tf_op jit(solution)/shard_map/ppermute | solution.py:20
  8.1 17.8 %collective-permute-start.1 = (bf16[1088,128]{1,0:T(8,128)(2,1)}, bf16[1088,128]{1,0:T(8,128)(2,1)S(1)}, u32[]{:S(2)}, u32[]{:S(2)}) collective-permute-start(bf16[1088,128]{1,0:T(8,128)(2,1)} %shard_map.111.msg_ref), channel_id=1, source_target_pairs={{0,28},{2,30},{4,0},{6,2},{8,4},{10,6},{12,8},{14,10},{16,12},{18,... | collective-permute-start | bytes 835592 | tf_op jit(solution)/shard_map/ppermute | solution.py:20
  8.6 17.3 %collective-permute-start = (bf16[1088,128]{1,0:T(8,128)(2,1)}, bf16[1088,128]{1,0:T(8,128)(2,1)S(1)}, u32[]{:S(2)}, u32[]{:S(2)}) collective-permute-start(bf16[1088,128]{1,0:T(8,128)(2,1)} %shard_map.111.msg_ref), channel_id=1, source_target_pairs={{0,30},{2,0},{4,2},{6,4},{8,6},{10,8},{12,10},{14,12},{16,14},{18,... | collective-permute-start | bytes 835592 | tf_op jit(solution)/shard_map/ppermute | solution.py:20
  11.7 43.8 %collective-permute-start.8 = (bf16[256,1024]{1,0:T(8,128)(2,1)}, bf16[256,1024]{1,0:T(8,128)(2,1)S(1)}, u32[]{:S(2)}, u32[]{:S(2)}) collective-permute-start(bf16[256,1024]{1,0:T(8,128)(2,1)} %get-tuple-element.28), channel_id=1, source_target_pairs={{0,2},{2,0},{4,6},{6,4},{8,10},{10,8},{12,14},{14,12},{16,18},{18,... | collective-permute-start | bytes 1572872 | tf_op jit(solution)/shard_map/ppermute | solution.py:25
  20.8 5.1 %copy-start.7 = (bf16[1088,128]{1,0:T(8,128)(2,1)}, bf16[1088,128]{1,0:T(8,128)(2,1)S(1)}, u32[]{:S(2)}) copy-start(bf16[1088,128]{1,0:T(8,128)(2,1)S(1)} %collective-permute-done.3.refs_3_) | copy-start | bytes 835588
  20.8 34.6 %collective-permute-start.9 = (bf16[256,1024]{1,0:T(8,128)(2,1)}, bf16[256,1024]{1,0:T(8,128)(2,1)S(1)}, u32[]{:S(2)}, u32[]{:S(2)}) collective-permute-start(bf16[256,1024]{1,0:T(8,128)(2,1)} %get-tuple-element.29), channel_id=1, source_target_pairs={{0,4},{2,6},{4,0},{6,2},{8,12},{10,14},{12,8},{14,10},{16,20},{18,... | collective-permute-start | bytes 1572872 | tf_op jit(solution)/shard_map/ppermute | solution.py:25
  21.0 4.9 %copy-start.8 = (bf16[1088,128]{1,0:T(8,128)(2,1)}, bf16[1088,128]{1,0:T(8,128)(2,1)S(1)}, u32[]{:S(2)}) copy-start(bf16[1088,128]{1,0:T(8,128)(2,1)S(1)} %collective-permute-done.2.refs_2_) | copy-start | bytes 835588
  21.0 34.4 %collective-permute-start.10 = (bf16[256,1024]{1,0:T(8,128)(2,1)}, bf16[256,1024]{1,0:T(8,128)(2,1)S(1)}, u32[]{:S(2)}, u32[]{:S(2)}) collective-permute-start(bf16[256,1024]{1,0:T(8,128)(2,1)} %get-tuple-element.30), channel_id=1, source_target_pairs={{0,6},{2,4},{4,2},{6,0},{8,14},{10,12},{12,10},{14,8},{16,22},{18,... | collective-permute-start | bytes 1572872 | tf_op jit(solution)/shard_map/ppermute | solution.py:25
  25.9 0.7 copy-start.9
  25.9 0.8 copy-start.10
  55.4 13.4 %copy-start.14 = (bf16[512,128]{1,0:T(8,128)(2,1)S(1)}, bf16[512,128]{1,0:T(8,128)(2,1)}, u32[]{:S(2)}) copy-start(bf16[512,128]{1,0:T(8,128)(2,1)} %get-tuple-element.22) | copy-start | bytes 393220
  55.4 13.4 %copy-start.13 = (bf16[512,128]{1,0:T(8,128)(2,1)S(1)}, bf16[512,128]{1,0:T(8,128)(2,1)}, u32[]{:S(2)}) copy-start(bf16[512,128]{1,0:T(8,128)(2,1)} %get-tuple-element.23) | copy-start | bytes 393220
  55.4 14.9 %copy-start.12 = (bf16[512,128]{1,0:T(8,128)(2,1)S(1)}, bf16[512,128]{1,0:T(8,128)(2,1)}, u32[]{:S(2)}) copy-start(bf16[512,128]{1,0:T(8,128)(2,1)} %get-tuple-element.24) | copy-start | bytes 393220
  55.4 18.5 %copy-start.11 = (bf16[512,128]{1,0:T(8,128)(2,1)S(1)}, bf16[512,128]{1,0:T(8,128)(2,1)}, u32[]{:S(2)}) copy-start(bf16[512,128]{1,0:T(8,128)(2,1)} %get-tuple-element.25) | copy-start | bytes 393220
  55.4 0.8 copy-start
  55.4 1.0 %copy-start.1 = (bf16[256,1024]{1,0:T(8,128)(2,1)}, bf16[256,1024]{1,0:T(8,128)(2,1)S(1)}, u32[]{:S(2)}) copy-start(bf16[256,1024]{1,0:T(8,128)(2,1)S(1)} %collective-permute-done.9.refs_1_) | copy-start | bytes 1572868
  56.4 0.8 copy-start.2
  60.6 17.3 %collective-permute-start.11 = (bf16[512,256]{1,0:T(8,128)(2,1)}, bf16[512,256]{1,0:T(8,128)(2,1)S(1)}, u32[]{:S(2)}, u32[]{:S(2)}) collective-permute-start(bf16[512,256]{1,0:T(8,128)(2,1)} %shard_map.117), channel_id=1, source_target_pairs={{0,8},{2,10},{4,12},{6,14},{8,0},{10,2},{12,4},{14,6},{16,24},{18,... | collective-permute-start | bytes 786440 | tf_op jit(solution)/shard_map/ppermute | solution.py:25
  68.8 12.7 %collective-permute-start.4 = (bf16[512,128]{1,0:T(8,128)(2,1)S(1)}, bf16[512,128]{1,0:T(8,128)(2,1)S(1)}, u32[]{:S(2)}, u32[]{:S(2)}) collective-permute-start(bf16[512,128]{1,0:T(8,128)(2,1)S(1)} %copy-done.14), channel_id=1, source_target_pairs={{0,2},{2,4},{4,6},{6,8},{8,10},{10,12},{12,14},{14,16},{16,18},{18... | collective-permute-start | bytes 393224 | tf_op jit(solution)/shard_map/ppermute | solution.py:20
  68.8 12.6 %collective-permute-start.5 = (bf16[512,128]{1,0:T(8,128)(2,1)S(1)}, bf16[512,128]{1,0:T(8,128)(2,1)S(1)}, u32[]{:S(2)}, u32[]{:S(2)}) collective-permute-start(bf16[512,128]{1,0:T(8,128)(2,1)S(1)} %copy-done.13), channel_id=1, source_target_pairs={{0,4},{2,6},{4,8},{6,10},{8,12},{10,14},{12,16},{14,18},{16,20},{1... | collective-permute-start | bytes 393224 | tf_op jit(solution)/shard_map/ppermute | solution.py:20
  70.3 14.2 %collective-permute-start.6 = (bf16[512,128]{1,0:T(8,128)(2,1)S(1)}, bf16[512,128]{1,0:T(8,128)(2,1)S(1)}, u32[]{:S(2)}, u32[]{:S(2)}) collective-permute-start(bf16[512,128]{1,0:T(8,128)(2,1)S(1)} %copy-done.12), channel_id=1, source_target_pairs={{0,8},{2,10},{4,12},{6,14},{8,16},{10,18},{12,20},{14,22},{16,24},... | collective-permute-start | bytes 393224 | tf_op jit(solution)/shard_map/ppermute | solution.py:20
  73.9 19.8 %collective-permute-start.7 = (bf16[512,128]{1,0:T(8,128)(2,1)S(1)}, bf16[512,128]{1,0:T(8,128)(2,1)S(1)}, u32[]{:S(2)}, u32[]{:S(2)}) collective-permute-start(bf16[512,128]{1,0:T(8,128)(2,1)S(1)} %copy-done.11), channel_id=1, source_target_pairs={{0,16},{2,18},{4,20},{6,22},{8,24},{10,26},{12,28},{14,30},{16,0},... | collective-permute-start | bytes 393224 | tf_op jit(solution)/shard_map/ppermute | solution.py:20
  79.0 17.4 %collective-permute-start.12 = (bf16[256,256]{1,0:T(8,128)(2,1)S(1)}, bf16[256,256]{1,0:T(8,128)(2,1)S(1)}, u32[]{:S(2)}, u32[]{:S(2)}) collective-permute-start(bf16[256,256]{1,0:T(8,128)(2,1)S(1)} %fusion.1), channel_id=1, source_target_pairs={{0,16},{2,18},{4,20},{6,22},{8,24},{10,26},{12,28},{14,30},{16,0},... | collective-permute-start | bytes 393224 | tf_op jit(solution)/shard_map/ppermute | solution.py:25
  81.5 12.2 %copy-start.3 = (bf16[512,128]{1,0:T(8,128)(2,1)}, bf16[512,128]{1,0:T(8,128)(2,1)S(1)}, u32[]{:S(2)}) copy-start(bf16[512,128]{1,0:T(8,128)(2,1)S(1)} %collective-permute-done.4.refs_0_) | copy-start | bytes 393220
  81.5 12.2 %copy-start.4 = (bf16[512,128]{1,0:T(8,128)(2,1)}, bf16[512,128]{1,0:T(8,128)(2,1)S(1)}, u32[]{:S(2)}) copy-start(bf16[512,128]{1,0:T(8,128)(2,1)S(1)} %collective-permute-done.5.refs_1_) | copy-start | bytes 393220
  84.6 9.2 %copy-start.5 = (bf16[512,128]{1,0:T(8,128)(2,1)}, bf16[512,128]{1,0:T(8,128)(2,1)S(1)}, u32[]{:S(2)}) copy-start(bf16[512,128]{1,0:T(8,128)(2,1)S(1)} %collective-permute-done.6.refs_2_) | copy-start | bytes 393220
  93.7 0.6 copy-start.6
where the time goes:
time: 97.5 us; the launch traced here: 97.1 us
  blocking collectives  23.9 us (25%)
  Pallas kernels  23.6 us (24%)
  waiting for transfers between devices  22.5 us (23%)
  starting transfers between devices  21.4 us (22%)
  local copies, waits for them, and re-layouts  3.27 us (3%)
  other arithmetic  1.82 us (2%)
    all_gather x1, blocking collectives, per_device(): lax.all_gather(rounded, 'kv', axis_index_groups=bunches, tiled=True)  23.9 us
    ppermute x8, waiting for transfers between devices, ring(): lax.ppermute(value, 'kv', [(i, (i + by) % count) for i in range(count)])  22.5 us
    ppermute x5, starting transfers between devices, swap(): return lax.ppermute(value, 'kv', [(i, i ^ bit) for i in range(count)])  11.3 us
    ppermute x8, starting transfers between devices, ring(): lax.ppermute(value, 'kv', [(i, (i + by) % count) for i in range(count)])  10.1 us
    pallas_call x2, Pallas kernels, weight(): call(functools.partial(weight_body, near, far, parity, kind), shape((bloc...  6.86 us
    pallas_call x1, Pallas kernels, per_device(): pl.pallas_call(functools.partial(far_body, sel, tok, heads, groups), out_...  4.81 us
    pallas_call x1, Pallas kernels, per_device(): call(functools.partial(pack_body, levels), shape((msg_rows, dim), BF16),...  3.56 us
    pallas_call x1, Pallas kernels, per_device(): call(functools.partial(own_body, sel), [shape((2 * rows, dim), BF16)] + [...  3.31 us
  transfers between devices with their start and end apart: 13, of which 4 were waited for; matrix products, arithmetic and copies ran while one was open for 1% of the time, Pallas kernels for 17%

commit v1 on v0

v1 whole, which is shorter than its diff:
```python
import functools

import jax
import jax.numpy as jnp
from jax import lax
from jax.experimental import pallas as pl
from jax.experimental.pallas import tpu as pltpu
from jax.sharding import PartitionSpec as P


QB = 128
KB = 32
LIMIT = 12 << 20
F32 = jnp.float32
BF16 = jnp.bfloat16
VMEM = pl.BlockSpec(memory_space=pltpu.VMEM)
HBM = pl.BlockSpec(memory_space=pltpu.HBM)


def ring(value, by):
    count = lax.axis_size("kv")
    return lax.ppermute(value, "kv", [(i, (i + by) % count) for i in range(count)])


def swap(value, bit):
    count = lax.axis_size("kv")
    return lax.ppermute(value, "kv", [(i, i ^ bit) for i in range(count)])


def forward(msg, levels, mix):
    if levels < 4:
        return [ring(msg, -(1 << level)) for level in range(levels)]
    four = ring(msg, -4)
    eight = ring(four, -4)
    payload = mix(2, msg, four)
    two = swap(payload, 2)
    payload = mix(1, msg, two)
    one = swap(payload, 1)
    return [one, two, four, eight] + [ring(msg, -(1 << level)) for level in range(4, levels)]


def call(body, out_shape, specs, flops, nbytes, local=True):
    kept = jax.tree.map(lambda x: pltpu.VMEM(x.shape, x.dtype) if local else x, out_shape)
    return pl.pallas_call(
        body,
        out_shape=kept,
        in_specs=specs,
        out_specs=jax.tree.map(lambda _: VMEM, out_shape),
        cost_estimate=pl.CostEstimate(flops=flops, bytes_accessed=nbytes, transcendentals=0),
        compiler_params=pltpu.CompilerParams(vmem_limit_bytes=LIMIT),
    )


def nt(a, b):
    return lax.dot_general(a, b, (((1,), (1,)), ((), ())), preferred_element_type=F32)


def tn(a, b):
    return lax.dot_general(a, b, (((0,), (0,)), ((), ())), preferred_element_type=F32)


def nn(a, b):
    return lax.dot_general(a, b, (((1,), (0,)), ((), ())), preferred_element_type=F32)


PER = 8
BIG = 16384.0
LOG2E = 1.4426950408889634


def layout(tok, heads, sel):
    rows = heads * tok
    codes = 2 * rows
    stats = codes + tok // QB * sel
    return rows, codes, stats, stats + rows // 128 * PER


def thirds(row):
    high = row.astype(BF16)
    rest = row - high.astype(F32)
    middle = rest.astype(BF16)
    return high, middle, (rest - middle.astype(F32)).astype(BF16)


def pack_body(levels, heads, picked_hbm, q_hbm, g_hbm, a_hbm, lse_hbm, msg_ref, picked_ref, a_ref, lse_ref, sem):
    rows = q_hbm.shape[0]
    tok = rows // heads
    sel = picked_ref.shape[1]
    span_blocks = tok // KB
    blocks = tok // QB
    _, codes, stats, _ = layout(tok, heads, sel)
    copies = [
        pltpu.make_async_copy(picked_hbm, picked_ref, sem.at[0]),
        pltpu.make_async_copy(lse_hbm, lse_ref, sem.at[1]),
        pltpu.make_async_copy(g_hbm, msg_ref.at[rows : 2 * rows, :], sem.at[2]),
        pltpu.make_async_copy(a_hbm, a_ref, sem.at[3]),
        pltpu.make_async_copy(q_hbm, msg_ref.at[0:rows, :], sem.at[4]),
    ]
    for copy in copies:
        copy.start()
    me = lax.axis_index("kv")
    copies[0].wait()
    order = lax.broadcasted_iota(jnp.int32, (sel, QB), 0)
    for b in range(blocks):
        code = jnp.full((sel, QB), -1, jnp.int32)
        for p in range(sel):
            block = picked_ref[b, p]
            span = lax.div(jnp.maximum(block, 0), span_blocks)
            group = jnp.int32(0)
            for level in range(levels):
                group += ((me - span) >= (1 << level)).astype(jnp.int32)
            value = jnp.where(block < 0, -1, group * span_blocks + block - span * span_blocks)
            code = jnp.where(order == p, value, code)
        msg_ref[codes + b * sel : codes + (b + 1) * sel, :] = code.astype(F32).astype(BF16)
    copies[1].wait()
    source = lax.broadcasted_iota(jnp.int32, (tok, rows), 0)
    target = lax.broadcasted_iota(jnp.int32, (tok, rows), 1)
    logs = jnp.zeros((PER, rows), F32)
    empty = jnp.zeros((PER - 3, tok), BF16)
    for h in range(heads):
        spread = jnp.where(target == source * heads + h, 1.0, 0.0).astype(BF16)
        parts = jnp.concatenate(list(thirds(lse_ref[h : h + 1, :])) + [empty], axis=0)
        logs += nn(parts, spread)
    copies[2].wait()
    copies[3].wait()
    product = msg_ref[rows : 2 * rows, :].astype(F32) * a_ref[...].astype(F32)
    ones = jnp.ones((PER, product.shape[1]), BF16)
    dots = sum(nt(ones, part) for part in thirds(product))
    split = [part.astype(F32) for part in thirds(dots)]
    row = lax.broadcasted_iota(jnp.int32, (PER, rows), 0)
    table = jnp.where(row < 3, logs, jnp.where(row == 3, split[0], jnp.where(row == 4, split[1], split[2])))
    table = jnp.where(row < 6, table, 0.0).astype(BF16)
    for c in range(rows // 128):
        msg_ref[stats + c * PER : stats + (c + 1) * PER, :] = table[:, c * 128 : (c + 1) * 128]
    copies[4].wait()


def unsplit(rows):
    return (rows[0:1] + rows[1:2]) + rows[2:3]


def group_terms(msg_ref, key, value, group, heads, sel, causal):
    rows, dim = key.shape
    tok = rows // heads
    _, codes, stats, _ = layout(tok, heads, sel)
    span_blocks = tok // KB
    chunks = QB * heads // 128
    dead = [[] for _ in range(span_blocks)]
    lse, dots = [], []
    for b in range(tok // QB):
        code = msg_ref[codes + b * sel : codes + (b + 1) * sel, :].astype(F32)
        for k in range(span_blocks):
            hit = jnp.where(code == float(group * span_blocks + k), 0.0, BIG)
            dead[k] += [jnp.min(hit, axis=0, keepdims=True)] * chunks
    for c in range(rows // 128):
        stat = msg_ref[stats + c * PER : stats + (c + 1) * PER, :].astype(F32)
        lse.append(unsplit(stat[0:3]))
        dots.append(unsplit(stat[3:6]))
    lse = jnp.concatenate(lse, axis=1) * LOG2E
    dots = jnp.concatenate(dots, axis=1)
    down = lax.broadcasted_iota(jnp.int32, (8, rows), 0)
    along = lax.broadcasted_iota(jnp.int32, (8, rows), 1)
    base = jnp.where(lax.rem(down, heads) == lax.rem(along, heads), 0.0, BIG) + lse
    shift = jnp.stack([base + jnp.concatenate(dead[k], axis=1) for k in range(span_blocks)])
    query = msg_ref[0:rows, :]
    grad = msg_ref[rows : 2 * rows, :]
    scores = nt(key, query) * (dim ** (-0.5) * LOG2E)
    scores = scores.reshape(span_blocks, KB * heads // 8, 8, rows) - shift[:, None]
    scores = scores.reshape(rows, rows)
    if causal:
        key_pos = lax.broadcasted_iota(jnp.int32, (rows, rows), 0)
        query_pos = lax.broadcasted_iota(jnp.int32, (rows, rows), 1)
        scores = jnp.where(lax.div(key_pos, heads) <= lax.div(query_pos, heads), scores, -BIG)
    weights = jnp.exp2(scores)
    score_grad = weights * (nt(value, grad) - dots)
    weight_pairs = weights.astype(BF16)
    grad_pairs = score_grad.astype(BF16)
    return nn(grad_pairs, query), nn(weight_pairs, grad), tn(grad_pairs, key)


def own_body(sel, heads, msg_ref, k_ref, v_ref, dk_ref, dv_ref, dq_ref):
    dk_ref[...], dv_ref[...], dq_ref[...] = group_terms(msg_ref, k_ref[...], v_ref[...], 0, heads, sel, True)


def far_body(sel, heads, groups, last, *refs):
    count = len(groups)
    msgs = refs[:count]
    k_ref, v_ref, dk_in, dv_in = refs[count : count + 4]
    dqs = refs[count + 4 : 2 * count + 4]
    dk_out, dv_out = refs[2 * count + 4 : 2 * count + 6]
    rows, dim = k_ref.shape
    scale = dim ** (-0.5)
    dk, dv = dk_in[...], dv_in[...]
    for index, group in enumerate(groups):
        dk_term, dv_term, dq = group_terms(msgs[index], k_ref[...], v_ref[...], group, heads, sel, False)
        dk, dv = dk + dk_term, dv + dv_term
        dqs[index][...] = dq.astype(BF16)
    dv_out[...] = dv
    if not last:
        dk_out[...] = dk
        return
    round_ref = refs[-1]
    for h in range(heads):
        at = pl.ds(h, rows // heads, stride=heads) if heads > 1 else slice(None)
        round_ref[:, h * dim : (h + 1) * dim] = dv_out[at, :].astype(BF16)
    dk_out[...] = dk * scale


def query_body(dq_ref, *refs):
    out_ref = refs[-1]
    total = dq_ref[...]
    for ref in refs[:-1]:
        total = total + ref[...].astype(F32)
    out_ref[...] = total * (out_ref.shape[1] ** (-0.5))


def mix_body(bit, yes_ref, no_ref, out_ref):
    picked = (lax.axis_index("kv") & bit) != 0

    @pl.when(picked)
    def _():
        out_ref[...] = yes_ref[...]

    @pl.when(jnp.logical_not(picked))
    def _():
        out_ref[...] = no_ref[...]


def share_of(tok, m, tp):
    return tok // tp if m > 1 and tok % (16 * tp) == 0 else tok


def cut_body(near, far, x_hbm, *refs):
    out_refs, sem = refs[:-1], refs[-1]
    rank = lax.rem(lax.axis_index("kv"), near)
    width = x_hbm.shape[1] // (near * far)
    copies = []
    for m in [*range(1, near), 0]:
        share = out_refs[m].shape[0]
        rows = slice(None)
        if share < x_hbm.shape[0]:
            rows = pl.ds(pl.multiple_of(lax.axis_index("tp") * share, share), share)
        for z in range(far):
            at = pl.multiple_of((z * near + (rank ^ m)) * width, width)
            copies.append(
                pltpu.make_async_copy(
                    x_hbm.at[rows, pl.ds(at, width)],
                    out_refs[m].at[:, z * width : (z + 1) * width],
                    sem.at[m * far + z],
                )
            )
    for copy in copies:
        copy.start()
    for copy in copies:
        copy.wait()


def weight_body(near, far, parity, counts, *refs):
    pieces = refs[: sum(counts)]
    rounds_ref, out_ref = refs[sum(counts) :]
    me = lax.axis_index("kv")
    rank, depth = lax.rem(me, near), lax.div(me, near)
    tok = rounds_ref.shape[0] // near
    width = pieces[0].shape[1] // far
    step = 2 if parity is not None else 1
    rights = []
    for m in range(near):
        for s in range(counts[m]):
            share = tok // counts[m]
            at = (rank ^ m) * tok + lax.rem(lax.axis_index("tp") + s, counts[m]) * share
            rights.append(rounds_ref[pl.ds(pl.multiple_of(at, share), share), :])
    right = jnp.concatenate(rights, axis=0)
    for index, rel in enumerate(range(parity or 0, far, step)):
        at = pl.multiple_of((depth ^ rel) * width, width)
        left = jnp.concatenate([piece[:, pl.ds(at, width)] for piece in pieces], axis=0)
        out_ref[index * width : (index + 1) * width, :] = tn(left, right).astype(out_ref.dtype)


def halve_body(blocks, keep_ref, came_ref, rest_ref, send_ref):
    width = keep_ref.shape[0] // blocks
    for block in range(blocks):
        at = slice(block * width, (block + 1) * width)
        to = slice(block // 2 * width, (block // 2 + 1) * width)
        total = keep_ref[at, :] + came_ref[at, :].astype(F32)
        if block % 2:
            send_ref[to, :] = total.astype(BF16)
        else:
            rest_ref[to, :] = total


def add_body(keep_ref, came_ref, out_ref):
    out_ref[...] = keep_ref[...] + came_ref[...].astype(F32)


def per_device(queries, keys, values, attended, out_grad, log_sum, picked, layer_input):
    tok, heads, dim = queries.shape
    sel = picked.shape[1]
    count = lax.axis_size("kv")
    levels = count.bit_length() - 1
    near = 1 << (levels // 2)
    far = count // near
    tp = lax.axis_size("tp")
    rows, _, _, msg_rows = layout(tok, heads, sel)
    flat = lambda x: x.reshape(rows, dim)
    key, value = flat(keys), flat(values)

    def shape(dims, kind):
        return jax.ShapeDtypeStruct(dims, kind)

    pairs = rows * rows * dim * 10
    msg = pl.pallas_call(
        functools.partial(pack_body, levels, heads),
        out_shape=pltpu.VMEM((msg_rows, dim), BF16),
        in_specs=[HBM] * 5,
        out_specs=VMEM,
        scratch_shapes=[
            pltpu.SMEM(picked.shape, jnp.int32),
            pltpu.VMEM((rows, dim), BF16),
            pltpu.VMEM((heads, tok), F32),
            pltpu.SemaphoreType.DMA((5,)),
        ],
        compiler_params=pltpu.CompilerParams(vmem_limit_bytes=62000000),
    )(picked, flat(queries), flat(out_grad), flat(attended), log_sum.T)

    def mix(bit, yes, no):
        return call(
            functools.partial(mix_body, bit), shape(yes.shape, BF16), [VMEM, VMEM], 1 << 18, yes.size * 6
        )(yes, no)

    got = forward(msg, levels, mix)
    width = layer_input.shape[1] // count
    blocked = width % 128 == 0 and far > 1
    if blocked:
        shares = [share_of(tok, m, tp) for m in range(near)]
        cuts = pl.pallas_call(
            functools.partial(cut_body, near, far),
            out_shape=[pltpu.VMEM((share, far * width), BF16) for share in shares],
            in_specs=[HBM],
            out_specs=[VMEM] * near,
            scratch_shapes=[pltpu.SemaphoreType.DMA((near * far,))],
            cost_estimate=pl.CostEstimate(flops=1 << 20, bytes_accessed=layer_input.size, transcendentals=0),
            compiler_params=pltpu.CompilerParams(vmem_limit_bytes=56 << 20),
        )(layer_input)
        pieces, counts = [cuts[0]], [1]
        for m in range(1, near):
            pieces.append(swap(cuts[m], m))
            counts.append(tok // shares[m])
            first = pieces[-1]
            for s in range(1, counts[m]):
                pieces.append(lax.ppermute(first, "tp", [((i + s) % tp, i) for i in range(tp)]))
    dk_own, dv_own, dq_own = call(
        functools.partial(own_body, sel, heads),
        [shape((rows, dim), F32)] * 3,
        [VMEM] * 3,
        pairs, 8 * rows * dim * 4,
    )(msg, key, value)

    def far_call(groups, dk, dv, last):
        kinds = [shape((rows, dim), BF16)] * len(groups) + [shape((rows, dim), F32)] * 2
        if last:
            kinds.append(shape((tok, heads * dim), BF16))
        return call(
            functools.partial(far_body, sel, heads, groups, last),
            kinds,
            [VMEM] * (len(groups) + 4),
            pairs * len(groups), 8 * rows * dim, not last,
        )(*[got[group - 1] for group in groups], key, value, dk, dv)

    back, dk, dv = {}, dk_own, dv_own
    stages = [(3,), (2,), (4,), (1,)] + [(level,) for level in range(5, levels + 1)]
    if levels < 4:
        stages = [tuple(range(1, levels + 1))]
    elif levels > 4:
        stages = [(level,) for level in range(1, levels + 1)]
    for stage in stages:
        outs = far_call(stage, dk, dv, stage == stages[-1])
        for group, side in zip(stage, outs):
            back[group] = ring(side, 1 << (group - 1))
        outs = outs[len(stage) :]
        dk, dv = outs[:2]
    key_grad, value_grad, rounded = outs
    if blocked:
        bunches = [[g * near + r for r in range(near)] for g in range(far)]
        rounds = lax.all_gather(rounded, "kv", axis_index_groups=bunches, tiled=True)

        columns = heads * dim

        def weight(parity, kind):
            blocks = far // 2
            return call(
                functools.partial(weight_body, near, far, parity, counts),
                shape((blocks * width, columns), kind),
                [VMEM] * (len(pieces) + 1),
                2 * near * tok * blocks * width * columns, near * tok * far * width * 2,
            )(*pieces, rounds)

        send = weight(1, BF16)
        total = weight(0, F32)
        bit, left = near, far // 2
        came = swap(send, bit)
        while left > 1:
            bit *= 2
            total, send = call(
                functools.partial(halve_body, left),
                [shape((left // 2 * width, columns), F32), shape((left // 2 * width, columns), BF16)],
                [VMEM] * 2, 1 << 18, left * width * columns * 8,
            )(total, came)
            left //= 2
            came = swap(send, bit)
        total = call(add_body, shape(total.shape, F32), [VMEM] * 2, 1 << 18, total.size * 10, False)(total, came)
    else:
        terms = lax.dot_general(
            layer_input, rounded, (((0,), (0,)), ((), ())), preferred_element_type=F32
        )
        total = lax.psum_scatter(terms, "kv", scatter_dimension=0, tiled=True)
    query_grad = call(
        query_body, shape((rows, dim), F32), [VMEM] * (levels + 1), 1 << 20, rows * dim * 16, False
    )(dq_own, *[back[group] for group in range(1, levels + 1)])
    grads = [x.reshape(tok, heads, dim) for x in (query_grad, key_grad, value_grad)]
    return (*grads, total)


def solution(mesh):
    placed = (
        P("kv", "tp", None),
        P("kv", "tp", None),
        P("kv", "tp", None),
        P("kv", "tp", None),
        P("kv", "tp", None),
        P("kv", "tp"),
        P("kv", None),
        P("kv", None),
    )
    return jax.shard_map(
        per_device,
        mesh=mesh,
        in_specs=placed,
        out_specs=(P("kv", "tp", None), P("kv", "tp", None), P("kv", "tp", None), P("kv", "tp")),
        check_vma=False,
    )
```

time: 97.5 us -> 70.4 us (0.72)
  blocking collectives: 23.9 us -> 7.82 us
  Pallas kernels: 23.6 us -> 11 us
  waiting for transfers between devices: 22.5 us -> 30.5 us
  local copies, waits for them, and re-layouts: 3.27 us -> 0.01 us
  other arithmetic: 1.82 us -> 0 us
  starting transfers between devices: 21.4 us -> 19.9 us
    ppermute x5 -> x7, waiting for transfers between devices: 0.01 us -> 22.8 us  [swap(): return lax.ppermute(value, 'kv', [(i, i ^ bit) for i in range(count)])]
    all_gather x1, blocking collectives: 23.9 us -> 7.82 us  [per_device(): lax.all_gather(rounded, 'kv', axis_index_groups=bunches, tiled=True)]
    ppermute x8 -> x6, waiting for transfers between devices: 22.5 us -> 7.72 us  [ring(): lax.ppermute(value, 'kv', [(i, (i + by) % count) for i in range(count)])]
    pallas_call x7 -> x14, Pallas kernels: 23.6 us -> 11 us  [the longest x4 4.22 us: far_call(): call(functools.partial(far_body, sel, heads, groups, last), kinds, [VMEM]...]
    ppermute x5 -> x7, starting transfers between devices: 11.3 us -> 3.15 us  [swap(): return lax.ppermute(value, 'kv', [(i, i ^ bit) for i in range(count)])]
    ppermute x8 -> x6, starting transfers between devices: 10.1 us -> 13.7 us  [ring(): lax.ppermute(value, 'kv', [(i, (i + by) % count) for i in range(count)])]
    unnamed x30 -> x4, local copies, waits for them, and re-layouts: 3.25 us -> 0.01 us
    ppermute x0 -> x2, starting transfers between devices: none -> 2.98 us  [per_device(): lax.ppermute(first, 'tp', [((i + s) % tp, i) for i in range(tp)])]
  transfers between devices with their start and end apart: 13 -> 15, of which waited for: 4 -> 8; matrix products, arithmetic and copies ran while one was open for 1% -> 0% of each run, Pallas kernels for 17% -> 12%
where the time goes in v1:
time: 70.4 us; the launch traced here: 70 us
  waiting for transfers between devices  30.5 us (43%)
  starting transfers between devices  19.9 us (28%)
  Pallas kernels  11 us (16%)
  blocking collectives  7.82 us (11%)
  between operations  0.78 us (1%)
    ppermute x7, waiting for transfers between devices, swap(): return lax.ppermute(value, 'kv', [(i, i ^ bit) for i in range(count)])  22.8 us
    ppermute x6, starting transfers between devices, ring(): lax.ppermute(value, 'kv', [(i, (i + by) % count) for i in range(count)])  13.7 us
    all_gather x1, blocking collectives, per_device(): lax.all_gather(rounded, 'kv', axis_index_groups=bunches, tiled=True)  7.82 us
    ppermute x6, waiting for transfers between devices, ring(): lax.ppermute(value, 'kv', [(i, (i + by) % count) for i in range(count)])  7.72 us
    pallas_call x4, Pallas kernels, far_call(): call(functools.partial(far_body, sel, heads, groups, last), kinds, [VMEM]...  4.22 us
    ppermute x7, starting transfers between devices, swap(): return lax.ppermute(value, 'kv', [(i, i ^ bit) for i in range(count)])  3.15 us
    ppermute x2, starting transfers between devices, per_device(): lax.ppermute(first, 'tp', [((i + s) % tp, i) for i in range(tp)])  2.98 us
    pallas_call x1, Pallas kernels, per_device(): pl.pallas_call(functools.partial(cut_body, near, far), out_shape=[pltpu.V...  1.6 us
  transfers between devices with their start and end apart: 15, of which 8 were waited for; matrix products, arithmetic and copies ran while one was open for 0% of the time, Pallas kernels for 12%

profile of v1, /device:TPU:4, one launch (start us, length us, event | category | flops | bytes accessed | tf_op | source)
XLA Modules:
  0.0 70.0 jit_solution(2641457487543593745)
XLA Ops:
  0.7 1.6 %shard_map.111.msg_ref.yes_ref = bf16[1088,128]{1,0:T(8,128)(2,1)S(1)} custom-call(s32[2,16]{1,0:T(2,128)} %picked_hbm.1, bf16[512,128]{1,0:T(8,128)(2,1)} %bitcast.20, bf16[512,128]{1,0:T(8,128)(2,1)} %bitcast.21, bf16[512,128]{1,0:T(8,128)(2,1)} %bitcast.22, f32[2,256]{1,0:T(2,128)} %bitcast.23), custom_call_target="tpu_custom_call" | custom-call | tf_op jit(solution)/shard_map/pallas_call | solution.py:311
  2.3 3.7 %collective-permute-start = (bf16[1088,128]{1,0:T(8,128)(2,1)S(1)}, bf16[1088,128]{1,0:T(8,128)(2,1)S(1)}, u32[]{:S(2)}, u32[]{:S(2)}) collective-permute-start(bf16[1088,128]{1,0:T(8,128)(2,1)S(1)} %shard_map.111.msg_ref.yes_ref), channel_id=1, source_target_pairs={{0,24},{2,26},{4,28},{6,30},{8,0},{10,2},{12,4},{14,6},{16,8},{18,... | collective-permute-start | bytes 835592 | tf_op jit(solution)/shard_map/ppermute | solution.py:22
  5.9 5.9 %collective-permute-done.no_ref.refs_0_ = bf16[1088,128]{1,0:T(8,128)(2,1)S(1)} collective-permute-done((bf16[1088,128]{1,0:T(8,128)(2,1)S(1)}, bf16[1088,128]{1,0:T(8,128)(2,1)S(1)}, u32[]{:S(2)}, u32[]{:S(2)}) %collective-permute-start) | collective-permute-done | bytes 278560 | tf_op jit(solution)/shard_map/ppermute | solution.py:22
  11.9 0.6 collective-permute-start.1
  12.4 1.6 %shard_map.120 = (bf16[256,1024]{1,0:T(8,128)(2,1)S(1)}, bf16[256,1024]{1,0:T(8,128)(2,1)S(1)}, bf16[128,1024]{1,0:T(8,128)(2,1)S(1)}, bf16[128,1024]{1,0:T(8,128)(2,1)S(1)}) custom-call(bf16[256,4096]{1,0:T(8,128)(2,1)} %x_hbm.1), custom_call_target="tpu_custom_call" | custom-call | flops 1048576 | bytes 1048576 | tf_op jit(solution)/shard_map/pallas_call | solution.py:335
  14.0 1.6 %collective-permute-start.9 = (bf16[128,1024]{1,0:T(8,128)(2,1)S(1)}, bf16[128,1024]{1,0:T(8,128)(2,1)S(1)}, u32[]{:S(2)}, u32[]{:S(2)}) collective-permute-start(bf16[128,1024]{1,0:T(8,128)(2,1)S(1)} %get-tuple-element.43), channel_id=1, source_target_pairs={{0,4},{2,6},{4,0},{6,2},{8,12},{10,14},{12,8},{14,10},{16,20},{18,... | collective-permute-start | bytes 786440 | tf_op jit(solution)/shard_map/ppermute | solution.py:27
  15.6 4.3 %collective-permute-start.3 = (bf16[1088,128]{1,0:T(8,128)(2,1)S(1)}, bf16[1088,128]{1,0:T(8,128)(2,1)S(1)}, u32[]{:S(2)}, u32[]{:S(2)}) collective-permute-start(bf16[1088,128]{1,0:T(8,128)(2,1)S(1)} %collective-permute-done.no_ref.refs_0_), channel_id=1, source_target_pairs={{0,24},{2,26},{4,28},{6,30},{8,0},{10,2},{12,4},{14,6},{16,8},{18,... | collective-permute-start | bytes 835592 | tf_op jit(solution)/shard_map/ppermute | solution.py:22
  19.9 0.3 collective-permute-start.8
  20.2 1.2 %collective-permute-done.1.no_ref.refs_0_ = bf16[1088,128]{1,0:T(8,128)(2,1)S(1)} collective-permute-done((bf16[1088,128]{1,0:T(8,128)(2,1)S(1)}, bf16[1088,128]{1,0:T(8,128)(2,1)S(1)}, u32[]{:S(2)}, u32[]{:S(2)}) %collective-permute-start.1) | collective-permute-done | bytes 278560 | tf_op jit(solution)/shard_map/ppermute | solution.py:27
  21.5 0.1 collective-permute-start.2
  21.6 1.0 %shard_map.112 = (f32[512,128]{1,0:T(8,128)S(1)}, f32[512,128]{1,0:T(8,128)S(1)}, f32[512,128]{1,0:T(8,128)S(1)}) custom-call(bf16[1088,128]{1,0:T(8,128)(2,1)S(1)} %shard_map.111.msg_ref.yes_ref, bf16[512,128]{1,0:T(8,128)(2,1)S(1)} %bitcast.9, bf16[512,128]{1,0:T(8,128)(2,1)S(1)} %bitcast.14), custom_call_target="tpu_custom_call" | custom-call | flops 335544320 | bytes 2097152 | tf_op jit(solution)/shard_map/pallas_call | solution.py:351
  22.5 4.5 %collective-permute-done.9.refs_2_ = bf16[128,1024]{1,0:T(8,128)(2,1)S(1)} collective-permute-done((bf16[128,1024]{1,0:T(8,128)(2,1)S(1)}, bf16[128,1024]{1,0:T(8,128)(2,1)S(1)}, u32[]{:S(2)}, u32[]{:S(2)}) %collective-permute-start.9) | collective-permute-done | bytes 262176 | tf_op jit(solution)/shard_map/ppermute | solution.py:27
  27.1 1.5 %collective-permute-start.10 = (bf16[128,1024]{1,0:T(8,128)(2,1)S(1)}, bf16[128,1024]{1,0:T(8,128)(2,1)S(1)}, u32[]{:S(2)}, u32[]{:S(2)}) collective-permute-start(bf16[128,1024]{1,0:T(8,128)(2,1)S(1)} %collective-permute-done.9.refs_2_), channel_id=1, source_target_pairs={{1,0},{0,1},{3,2},{2,3},{5,4},{4,5},{7,6},{6,7},{9,8},{8,9},{11,10... | collective-permute-start | bytes 786440 | tf_op jit(solution)/shard_map/ppermute | solution.py:350
  28.6 0.2 collective-permute-done.11.refs_4_
  28.7 1.5 %collective-permute-start.12 = (bf16[128,1024]{1,0:T(8,128)(2,1)S(1)}, bf16[128,1024]{1,0:T(8,128)(2,1)S(1)}, u32[]{:S(2)}, u32[]{:S(2)}) collective-permute-start(bf16[128,1024]{1,0:T(8,128)(2,1)S(1)} %collective-permute-done.11.refs_4_), channel_id=1, source_target_pairs={{1,0},{0,1},{3,2},{2,3},{5,4},{4,5},{7,6},{6,7},{9,8},{8,9},{11,10... | collective-permute-start | bytes 786440 | tf_op jit(solution)/shard_map/ppermute | solution.py:350
  30.2 0.9 %shard_map.115 = (bf16[512,128]{1,0:T(8,128)(2,1)S(1)}, f32[512,128]{1,0:T(8,128)S(1)}, f32[512,128]{1,0:T(8,128)S(1)}) custom-call(bf16[1088,128]{1,0:T(8,128)(2,1)S(1)} %collective-permute-done.no_ref.refs_0_, bf16[512,128]{1,0:T(8,128)(2,1)S(1)} %bitcast.10, bf16[512,128]{1,0:T(8,128)(2,1)S(1)} %bitcast.15, f32[512,128]{1,0:T(8,128)S(1)} %get-tuple-element.27.refs_3_, ...), custom_call_target="tpu_custom_call" | custom-call | flops 335544320 | bytes 524288 | tf_op jit(solution)/shard_map/pallas_call | solution.py:362
  31.1 0.9 %shard_map.116 = (bf16[512,128]{1,0:T(8,128)(2,1)S(1)}, f32[512,128]{1,0:T(8,128)S(1)}, f32[512,128]{1,0:T(8,128)S(1)}) custom-call(bf16[1088,128]{1,0:T(8,128)(2,1)S(1)} %collective-permute-done.1.no_ref.refs_0_, bf16[512,128]{1,0:T(8,128)(2,1)S(1)} %bitcast.11, bf16[512,128]{1,0:T(8,128)(2,1)S(1)} %bitcast.16, f32[512,128]{1,0:T(8,128)S(1)} %get-tuple-element.29.refs_3_, ...), custom_call_target="tpu_custom_call" | custom-call | flops 335544320 | bytes 524288 | tf_op jit(solution)/shard_map/pallas_call | solution.py:362
  32.0 0.9 %shard_map.117 = (bf16[512,128]{1,0:T(8,128)(2,1)S(1)}, f32[512,128]{1,0:T(8,128)S(1)}, f32[512,128]{1,0:T(8,128)S(1)}) custom-call(bf16[1088,128]{1,0:T(8,128)(2,1)S(1)} %collective-permute-done.3.refs_0_, bf16[512,128]{1,0:T(8,128)(2,1)S(1)} %bitcast.12, bf16[512,128]{1,0:T(8,128)(2,1)S(1)} %bitcast.17, f32[512,128]{1,0:T(8,128)S(1)} %get-tuple-element.31.refs_3_, ...), custom_call_target="tpu_custom_call" | custom-call | flops 335544320 | bytes 524288 | tf_op jit(solution)/shard_map/pallas_call | solution.py:362
  32.8 1.6 %shard_map.118 = (bf16[512,128]{1,0:T(8,128)(2,1)S(1)}, f32[512,128]{1,0:T(8,128)}, f32[512,128]{1,0:T(8,128)}, bf16[256,256]{1,0:T(8,128)(2,1)S(1)}) custom-call(bf16[1088,128]{1,0:T(8,128)(2,1)S(1)} %collective-permute-done.2.refs_0_, bf16[512,128]{1,0:T(8,128)(2,1)S(1)} %bitcast.13, bf16[512,128]{1,0:T(8,128)(2,1)S(1)} %bitcast.18, ...), custom_call_target="tpu_custom_call" | custom-call | flops 335544320 | bytes 524288 | tf_op jit(solution)/shard_map/pallas_call | solution.py:362
  34.5 7.8 %all_gather.3.refs_6_ = bf16[1024,256]{1,0:T(8,128)(2,1)S(1)} all-gather(bf16[256,256]{1,0:T(8,128)(2,1)S(1)} %get-tuple-element.45), channel_id=1, replica_groups={{0,2,4,6},{8,10,12,14},{16,18,20,22},{24,26,28,30},{1,3,5,7},{9,11,13,1..., dimensions={0}, use_global_device_ids=true | all-gather | bytes 655360 | tf_op jit(solution)/shard_map/all_gather | solution.py:384
  42.3 0.5 shard_map.122
  42.8 0.5 collective-permute-start.13
  43.4 1.6 %collective-permute-start.6 = (bf16[512,128]{1,0:T(8,128)(2,1)S(1)}, bf16[512,128]{1,0:T(8,128)(2,1)S(1)}, u32[]{:S(2)}, u32[]{:S(2)}) collective-permute-start(bf16[512,128]{1,0:T(8,128)(2,1)S(1)} %get-tuple-element.37), channel_id=1, source_target_pairs={{0,8},{2,10},{4,12},{6,14},{8,16},{10,18},{12,20},{14,22},{16,24},... | collective-permute-start | bytes 393224 | tf_op jit(solution)/shard_map/ppermute | solution.py:22
  44.9 2.9 %collective-permute-start.7 = (bf16[512,128]{1,0:T(8,128)(2,1)S(1)}, bf16[512,128]{1,0:T(8,128)(2,1)S(1)}, u32[]{:S(2)}, u32[]{:S(2)}) collective-permute-start(bf16[512,128]{1,0:T(8,128)(2,1)S(1)} %get-tuple-element.38), channel_id=1, source_target_pairs={{0,16},{2,18},{4,20},{6,22},{8,24},{10,26},{12,28},{14,30},{16,0},... | collective-permute-start | bytes 393224 | tf_op jit(solution)/shard_map/ppermute | solution.py:22
  47.8 1.3 %collective-permute-start.5 = (bf16[512,128]{1,0:T(8,128)(2,1)S(1)}, bf16[512,128]{1,0:T(8,128)(2,1)S(1)}, u32[]{:S(2)}, u32[]{:S(2)}) collective-permute-start(bf16[512,128]{1,0:T(8,128)(2,1)S(1)} %get-tuple-element.36), channel_id=1, source_target_pairs={{0,4},{2,6},{4,8},{6,10},{8,12},{10,14},{12,16},{14,18},{16,20},{1... | collective-permute-start | bytes 393224 | tf_op jit(solution)/shard_map/ppermute | solution.py:22
  49.2 0.5 shard_map.121.keep_ref
  49.7 6.9 %collective-permute-done.13.came_ref = bf16[512,256]{1,0:T(8,128)(2,1)S(1)} collective-permute-done((bf16[512,256]{1,0:T(8,128)(2,1)S(1)}, bf16[512,256]{1,0:T(8,128)(2,1)S(1)}, u32[]{:S(2)}, u32[]{:S(2)}) %collective-permute-start.13) | collective-permute-done | bytes 262176 | tf_op jit(solution)/shard_map/ppermute | solution.py:27
  56.7 0.5 collective-permute-done.6.refs_2_
  57.2 1.3 %collective-permute-done.5.refs_1_ = bf16[512,128]{1,0:T(8,128)(2,1)S(1)} collective-permute-done((bf16[512,128]{1,0:T(8,128)(2,1)S(1)}, bf16[512,128]{1,0:T(8,128)(2,1)S(1)}, u32[]{:S(2)}, u32[]{:S(2)}) %collective-permute-start.5) | collective-permute-done | bytes 131104 | tf_op jit(solution)/shard_map/ppermute | solution.py:22
  58.5 0.8 %shard_map.119 = f32[512,128]{1,0:T(8,128)} custom-call(f32[512,128]{1,0:T(8,128)S(1)} %get-tuple-element.26.dq_ref, bf16[512,128]{1,0:T(8,128)(2,1)S(1)} %collective-permute-done.4.refs_0_, bf16[512,128]{1,0:T(8,128)(2,1)S(1)} %collective-permute-done.5.refs_1_, bf16[512,128]{1,0:T(8,128)(2,1)S(1)} %collective-permute-done.6.refs_2_, ...), custom_call_target="tpu_custom_call" | custom-call | flops 1048576 | bytes 1048576 | tf_op jit(solution)/shard_map/pallas_call | solution.py:416
  59.3 10.0 %collective-permute-done.14.came_ref = bf16[256,256]{1,0:T(8,128)(2,1)S(1)} collective-permute-done((bf16[256,256]{1,0:T(8,128)(2,1)S(1)}, bf16[256,256]{1,0:T(8,128)(2,1)S(1)}, u32[]{:S(2)}, u32[]{:S(2)}) %collective-permute-start.14) | collective-permute-done | bytes 131104 | tf_op jit(solution)/shard_map/ppermute | solution.py:27
  69.3 0.7 %shard_map.124 = f32[256,256]{1,0:T(8,128)} custom-call(f32[256,256]{1,0:T(8,128)S(1)} %get-tuple-element.46.keep_ref, bf16[256,256]{1,0:T(8,128)(2,1)S(1)} %collective-permute-done.14.came_ref), custom_call_target="tpu_custom_call" | custom-call | flops 262144 | bytes 655360 | tf_op jit(solution)/shard_map/pallas_call | solution.py:410
  (17 shorter events, 0.2 us)
Async XLA Ops:
  0.6 20.9 %copy-start = (bf16[256,2,128]{2,1,0:T(2,128)(2,1)S(1)}, bf16[256,2,128]{2,1,0:T(2,128)(2,1)}, u32[]{:S(2)}) copy-start(bf16[256,2,128]{2,1,0:T(2,128)(2,1)} %param.9) | copy-start | bytes 393220
  0.6 20.9 %copy-start.1 = (bf16[256,2,128]{2,1,0:T(2,128)(2,1)S(1)}, bf16[256,2,128]{2,1,0:T(2,128)(2,1)}, u32[]{:S(2)}) copy-start(bf16[256,2,128]{2,1,0:T(2,128)(2,1)} %param.10) | copy-start | bytes 393220
  2.3 9.6 %collective-permute-start = (bf16[1088,128]{1,0:T(8,128)(2,1)S(1)}, bf16[1088,128]{1,0:T(8,128)(2,1)S(1)}, u32[]{:S(2)}, u32[]{:S(2)}) collective-permute-start(bf16[1088,128]{1,0:T(8,128)(2,1)S(1)} %shard_map.111.msg_ref.yes_ref), channel_id=1, source_target_pairs={{0,24},{2,26},{4,28},{6,30},{8,0},{10,2},{12,4},{14,6},{16,8},{18,... | collective-permute-start | bytes 835592 | tf_op jit(solution)/shard_map/ppermute | solution.py:22
  11.9 9.6 %collective-permute-start.1 = (bf16[1088,128]{1,0:T(8,128)(2,1)S(1)}, bf16[1088,128]{1,0:T(8,128)(2,1)S(1)}, u32[]{:S(2)}, u32[]{:S(2)}) collective-permute-start(bf16[1088,128]{1,0:T(8,128)(2,1)S(1)} %shard_map.113), channel_id=1, source_target_pairs={{0,4},{2,6},{4,0},{6,2},{8,12},{10,14},{12,8},{14,10},{16,20},{18,... | collective-permute-start | bytes 835592 | tf_op jit(solution)/shard_map/ppermute | solution.py:27
  14.0 13.0 %collective-permute-start.9 = (bf16[128,1024]{1,0:T(8,128)(2,1)S(1)}, bf16[128,1024]{1,0:T(8,128)(2,1)S(1)}, u32[]{:S(2)}, u32[]{:S(2)}) collective-permute-start(bf16[128,1024]{1,0:T(8,128)(2,1)S(1)} %get-tuple-element.43), channel_id=1, source_target_pairs={{0,4},{2,6},{4,0},{6,2},{8,12},{10,14},{12,8},{14,10},{16,20},{18,... | collective-permute-start | bytes 786440 | tf_op jit(solution)/shard_map/ppermute | solution.py:27
  15.6 13.1 %collective-permute-start.11 = (bf16[128,1024]{1,0:T(8,128)(2,1)S(1)}, bf16[128,1024]{1,0:T(8,128)(2,1)S(1)}, u32[]{:S(2)}, u32[]{:S(2)}) collective-permute-start(bf16[128,1024]{1,0:T(8,128)(2,1)S(1)} %get-tuple-element.44), channel_id=1, source_target_pairs={{0,6},{2,4},{4,2},{6,0},{8,14},{10,12},{12,10},{14,8},{16,22},{18,... | collective-permute-start | bytes 786440 | tf_op jit(solution)/shard_map/ppermute | solution.py:27
  15.6 16.3 %collective-permute-start.3 = (bf16[1088,128]{1,0:T(8,128)(2,1)S(1)}, bf16[1088,128]{1,0:T(8,128)(2,1)S(1)}, u32[]{:S(2)}, u32[]{:S(2)}) collective-permute-start(bf16[1088,128]{1,0:T(8,128)(2,1)S(1)} %collective-permute-done.no_ref.refs_0_), channel_id=1, source_target_pairs={{0,24},{2,26},{4,28},{6,30},{8,0},{10,2},{12,4},{14,6},{16,8},{18,... | collective-permute-start | bytes 835592 | tf_op jit(solution)/shard_map/ppermute | solution.py:22
  19.9 22.4 %collective-permute-start.8 = (bf16[256,1024]{1,0:T(8,128)(2,1)S(1)}, bf16[256,1024]{1,0:T(8,128)(2,1)S(1)}, u32[]{:S(2)}, u32[]{:S(2)}) collective-permute-start(bf16[256,1024]{1,0:T(8,128)(2,1)S(1)} %get-tuple-element.42), channel_id=1, source_target_pairs={{0,2},{2,0},{4,6},{6,4},{8,10},{10,8},{12,14},{14,12},{16,18},{18,... | collective-permute-start | bytes 1572872 | tf_op jit(solution)/shard_map/ppermute | solution.py:27
  21.5 11.4 %collective-permute-start.2 = (bf16[1088,128]{1,0:T(8,128)(2,1)S(1)}, bf16[1088,128]{1,0:T(8,128)(2,1)S(1)}, u32[]{:S(2)}, u32[]{:S(2)}) collective-permute-start(bf16[1088,128]{1,0:T(8,128)(2,1)S(1)} %shard_map.114), channel_id=1, source_target_pairs={{0,2},{2,0},{4,6},{6,4},{8,10},{10,8},{12,14},{14,12},{16,18},{18,... | collective-permute-start | bytes 835592 | tf_op jit(solution)/shard_map/ppermute | solution.py:27
  27.1 15.2 %collective-permute-start.10 = (bf16[128,1024]{1,0:T(8,128)(2,1)S(1)}, bf16[128,1024]{1,0:T(8,128)(2,1)S(1)}, u32[]{:S(2)}, u32[]{:S(2)}) collective-permute-start(bf16[128,1024]{1,0:T(8,128)(2,1)S(1)} %collective-permute-done.9.refs_2_), channel_id=1, source_target_pairs={{1,0},{0,1},{3,2},{2,3},{5,4},{4,5},{7,6},{6,7},{9,8},{8,9},{11,10... | collective-permute-start | bytes 786440 | tf_op jit(solution)/shard_map/ppermute | solution.py:350
  28.7 13.6 %collective-permute-start.12 = (bf16[128,1024]{1,0:T(8,128)(2,1)S(1)}, bf16[128,1024]{1,0:T(8,128)(2,1)S(1)}, u32[]{:S(2)}, u32[]{:S(2)}) collective-permute-start(bf16[128,1024]{1,0:T(8,128)(2,1)S(1)} %collective-permute-done.11.refs_4_), channel_id=1, source_target_pairs={{1,0},{0,1},{3,2},{2,3},{5,4},{4,5},{7,6},{6,7},{9,8},{8,9},{11,10... | collective-permute-start | bytes 786440 | tf_op jit(solution)/shard_map/ppermute | solution.py:350
  42.8 13.8 %collective-permute-start.13 = (bf16[512,256]{1,0:T(8,128)(2,1)S(1)}, bf16[512,256]{1,0:T(8,128)(2,1)S(1)}, u32[]{:S(2)}, u32[]{:S(2)}) collective-permute-start(bf16[512,256]{1,0:T(8,128)(2,1)S(1)} %shard_map.122), channel_id=1, source_target_pairs={{0,8},{2,10},{4,12},{6,14},{8,0},{10,2},{12,4},{14,6},{16,24},{18,... | collective-permute-start | bytes 786440 | tf_op jit(solution)/shard_map/ppermute | solution.py:27
  43.4 13.9 %collective-permute-start.6 = (bf16[512,128]{1,0:T(8,128)(2,1)S(1)}, bf16[512,128]{1,0:T(8,128)(2,1)S(1)}, u32[]{:S(2)}, u32[]{:S(2)}) collective-permute-start(bf16[512,128]{1,0:T(8,128)(2,1)S(1)} %get-tuple-element.37), channel_id=1, source_target_pairs={{0,8},{2,10},{4,12},{6,14},{8,16},{10,18},{12,20},{14,22},{16,24},... | collective-permute-start | bytes 393224 | tf_op jit(solution)/shard_map/ppermute | solution.py:22
  44.9 12.3 %collective-permute-start.7 = (bf16[512,128]{1,0:T(8,128)(2,1)S(1)}, bf16[512,128]{1,0:T(8,128)(2,1)S(1)}, u32[]{:S(2)}, u32[]{:S(2)}) collective-permute-start(bf16[512,128]{1,0:T(8,128)(2,1)S(1)} %get-tuple-element.38), channel_id=1, source_target_pairs={{0,16},{2,18},{4,20},{6,22},{8,24},{10,26},{12,28},{14,30},{16,0},... | collective-permute-start | bytes 393224 | tf_op jit(solution)/shard_map/ppermute | solution.py:22
  47.8 10.7 %collective-permute-start.5 = (bf16[512,128]{1,0:T(8,128)(2,1)S(1)}, bf16[512,128]{1,0:T(8,128)(2,1)S(1)}, u32[]{:S(2)}, u32[]{:S(2)}) collective-permute-start(bf16[512,128]{1,0:T(8,128)(2,1)S(1)} %get-tuple-element.36), channel_id=1, source_target_pairs={{0,4},{2,6},{4,8},{6,10},{8,12},{10,14},{12,16},{14,18},{16,20},{1... | collective-permute-start | bytes 393224 | tf_op jit(solution)/shard_map/ppermute | solution.py:22
  49.2 9.4 %collective-permute-start.4 = (bf16[512,128]{1,0:T(8,128)(2,1)S(1)}, bf16[512,128]{1,0:T(8,128)(2,1)S(1)}, u32[]{:S(2)}, u32[]{:S(2)}) collective-permute-start(bf16[512,128]{1,0:T(8,128)(2,1)S(1)} %get-tuple-element.35), channel_id=1, source_target_pairs={{0,2},{2,4},{4,6},{6,8},{8,10},{10,12},{12,14},{14,16},{16,18},{18... | collective-permute-start | bytes 393224 | tf_op jit(solution)/shard_map/ppermute | solution.py:22
  56.6 12.7 %collective-permute-start.14 = (bf16[256,256]{1,0:T(8,128)(2,1)S(1)}, bf16[256,256]{1,0:T(8,128)(2,1)S(1)}, u32[]{:S(2)}, u32[]{:S(2)}) collective-permute-start(bf16[256,256]{1,0:T(8,128)(2,1)S(1)} %get-tuple-element.47), channel_id=1, source_target_pairs={{0,16},{2,18},{4,20},{6,22},{8,24},{10,26},{12,28},{14,30},{16,0},... | collective-permute-start | bytes 393224 | tf_op jit(solution)/shard_map/ppermute | solution.py:27

commit v2 on v1

--- a/solution.py
+++ b/solution.py
@@ -82,7 +82,8 @@
     return high, middle, (rest - middle.astype(F32)).astype(BF16)
 
 
-def pack_body(levels, heads, picked_hbm, q_hbm, g_hbm, a_hbm, lse_hbm, msg_ref, picked_ref, a_ref, lse_ref, sem):
+def pack_body(levels, heads, near, far, wanted, picked_hbm, q_hbm, g_hbm, a_hbm, lse_hbm, x_hbm, msg_ref, *refs):
+    picked_ref, a_ref, lse_ref, sem, cut_sem = refs[-5:]
     rows = q_hbm.shape[0]
     tok = rows // heads
     sel = picked_ref.shape[1]
@@ -96,7 +97,8 @@
         pltpu.make_async_copy(a_hbm, a_ref, sem.at[3]),
         pltpu.make_async_copy(q_hbm, msg_ref.at[0:rows, :], sem.at[4]),
     ]
-    for copy in copies:
+    pieces = cuts(near, far, wanted, x_hbm, refs[:-5], cut_sem)
+    for copy in copies + pieces:
         copy.start()
     me = lax.axis_index("kv")
     copies[0].wait()
@@ -133,6 +135,8 @@
     for c in range(rows // 128):
         msg_ref[stats + c * PER : stats + (c + 1) * PER, :] = table[:, c * 128 : (c + 1) * 128]
     copies[4].wait()
+    for copy in pieces:
+        copy.wait()
 
 
 def unsplit(rows):
@@ -230,13 +234,12 @@
     return tok // tp if m > 1 and tok % (16 * tp) == 0 else tok
 
 
-def cut_body(near, far, x_hbm, *refs):
-    out_refs, sem = refs[:-1], refs[-1]
+def cuts(near, far, wanted, x_hbm, out_refs, sem):
     rank = lax.rem(lax.axis_index("kv"), near)
     width = x_hbm.shape[1] // (near * far)
     copies = []
-    for m in [*range(1, near), 0]:
-        share = out_refs[m].shape[0]
+    for index, (m, ref) in enumerate(zip(wanted, out_refs)):
+        share = ref.shape[0]
         rows = slice(None)
         if share < x_hbm.shape[0]:
             rows = pl.ds(pl.multiple_of(lax.axis_index("tp") * share, share), share)
@@ -245,10 +248,15 @@
             copies.append(
                 pltpu.make_async_copy(
                     x_hbm.at[rows, pl.ds(at, width)],
-                    out_refs[m].at[:, z * width : (z + 1) * width],
-                    sem.at[m * far + z],
+                    ref.at[:, z * width : (z + 1) * width],
+                    sem.at[index * far + z],
                 )
             )
+    return copies
+
+
+def cut_body(near, far, wanted, x_hbm, *refs):
+    copies = cuts(near, far, wanted, x_hbm, refs[:-1], refs[-1])
     for copy in copies:
         copy.start()
     for copy in copies:
@@ -257,18 +265,18 @@
 
 def weight_body(near, far, parity, counts, *refs):
     pieces = refs[: sum(counts)]
-    rounds_ref, out_ref = refs[sum(counts) :]
+    rounds_refs, out_ref = refs[sum(counts) : -1], refs[-1]
     me = lax.axis_index("kv")
-    rank, depth = lax.rem(me, near), lax.div(me, near)
-    tok = rounds_ref.shape[0] // near
+    depth = lax.div(me, near)
+    tok = rounds_refs[0].shape[0]
     width = pieces[0].shape[1] // far
     step = 2 if parity is not None else 1
     rights = []
     for m in range(near):
         for s in range(counts[m]):
             share = tok // counts[m]
-            at = (rank ^ m) * tok + lax.rem(lax.axis_index("tp") + s, counts[m]) * share
-            rights.append(rounds_ref[pl.ds(pl.multiple_of(at, share), share), :])
+            at = lax.rem(lax.axis_index("tp") + s, counts[m]) * share if counts[m] > 1 else 0
+            rights.append(rounds_refs[m][pl.ds(pl.multiple_of(at, share), share), :] if counts[m] > 1 else rounds_refs[m][...])
     right = jnp.concatenate(rights, axis=0)
     for index, rel in enumerate(range(parity or 0, far, step)):
         at = pl.multiple_of((depth ^ rel) * width, width)
@@ -308,19 +316,25 @@
         return jax.ShapeDtypeStruct(dims, kind)
 
     pairs = rows * rows * dim * 10
-    msg = pl.pallas_call(
-        functools.partial(pack_body, levels, heads),
-        out_shape=pltpu.VMEM((msg_rows, dim), BF16),
-        in_specs=[HBM] * 5,
-        out_specs=VMEM,
+    width = layer_input.shape[1] // count
+    blocked = width % 128 == 0 and far > 1
+    shares = [share_of(tok, m, tp) for m in range(near)]
+    early = list(range(2, near)) if blocked else []
+    msg, *first = pl.pallas_call(
+        functools.partial(pack_body, levels, heads, near, far, early),
+        out_shape=[pltpu.VMEM((msg_rows, dim), BF16)]
+        + [pltpu.VMEM((shares[m], far * width), BF16) for m in early],
+        in_specs=[HBM] * 6,
+        out_specs=[VMEM] * (1 + len(early)),
         scratch_shapes=[
             pltpu.SMEM(picked.shape, jnp.int32),
             pltpu.VMEM((rows, dim), BF16),
             pltpu.VMEM((heads, tok), F32),
             pltpu.SemaphoreType.DMA((5,)),
+            pltpu.SemaphoreType.DMA((max(1, len(early)) * far,)),
         ],
         compiler_params=pltpu.CompilerParams(vmem_limit_bytes=62000000),
-    )(picked, flat(queries), flat(out_grad), flat(attended), log_sum.T)
+    )(picked, flat(queries), flat(out_grad), flat(attended), log_sum.T, layer_input)
 
     def mix(bit, yes, no):
         return call(
@@ -328,22 +342,21 @@
         )(yes, no)
 
     got = forward(msg, levels, mix)
-    width = layer_input.shape[1] // count
-    blocked = width % 128 == 0 and far > 1
     if blocked:
-        shares = [share_of(tok, m, tp) for m in range(near)]
-        cuts = pl.pallas_call(
-            functools.partial(cut_body, near, far),
-            out_shape=[pltpu.VMEM((share, far * width), BF16) for share in shares],
+        wanted = [m for m in (1, 0) if m < near]
+        later = pl.pallas_call(
+            functools.partial(cut_body, near, far, wanted),
+            out_shape=[pltpu.VMEM((tok, far * width), BF16) for _ in wanted],
             in_specs=[HBM],
-            out_specs=[VMEM] * near,
-            scratch_shapes=[pltpu.SemaphoreType.DMA((near * far,))],
+            out_specs=[VMEM] * len(wanted),
+            scratch_shapes=[pltpu.SemaphoreType.DMA((len(wanted) * far,))],
             cost_estimate=pl.CostEstimate(flops=1 << 20, bytes_accessed=layer_input.size, transcendentals=0),
             compiler_params=pltpu.CompilerParams(vmem_limit_bytes=56 << 20),
         )(layer_input)
-        pieces, counts = [cuts[0]], [1]
+        cut = dict(zip(early + wanted, first + list(later)))
+        pieces, counts = [cut[0]], [1]
         for m in range(1, near):
-            pieces.append(swap(cuts[m], m))
+            pieces.append(swap(cut[m], m))
             counts.append(tok // shares[m])
             first = pieces[-1]
             for s in range(1, counts[m]):
@@ -363,7 +376,7 @@
             functools.partial(far_body, sel, heads, groups, last),
             kinds,
             [VMEM] * (len(groups) + 4),
-            pairs * len(groups), 8 * rows * dim, not last,
+            pairs * len(groups), 8 * rows * dim,
         )(*[got[group - 1] for group in groups], key, value, dk, dv)
 
     back, dk, dv = {}, dk_own, dv_own
@@ -380,9 +393,12 @@
         dk, dv = outs[:2]
     key_grad, value_grad, rounded = outs
     if blocked:
-        bunches = [[g * near + r for r in range(near)] for g in range(far)]
-        rounds = lax.all_gather(rounded, "kv", axis_index_groups=bunches, tiled=True)
-
+        rounds = {0: rounded}
+        bit = near // 2
+        while bit:
+            for m in list(rounds):
+                rounds[m ^ bit] = swap(rounds[m], bit)
+            bit //= 2
         columns = heads * dim
 
         def weight(parity, kind):
@@ -390,9 +406,9 @@
             return call(
                 functools.partial(weight_body, near, far, parity, counts),
                 shape((blocks * width, columns), kind),
-                [VMEM] * (len(pieces) + 1),
+                [VMEM] * (len(pieces) + near),
                 2 * near * tok * blocks * width * columns, near * tok * far * width * 2,
-            )(*pieces, rounds)
+            )(*pieces, *[rounds[m] for m in range(near)])
 
         send = weight(1, BF16)
         total = weight(0, F32)

time: 70.4 us -> 69.3 us (0.984)
  blocking collectives: 7.82 us -> 0 us
  starting transfers between devices: 19.9 us -> 23.3 us
  waiting for transfers between devices: 30.5 us -> 33.4 us
  local copies, waits for them, and re-layouts: 0.01 us -> 1.42 us
  Pallas kernels: 11 us -> 10.1 us
    all_gather x1 -> x0, blocking collectives: 7.82 us -> none  [per_device(): lax.all_gather(rounded, 'kv', axis_index_groups=bunches, tiled=True)]
    ppermute x7 -> x10, waiting for transfers between devices: 22.8 us -> 27.4 us  [swap(): return lax.ppermute(value, 'kv', [(i, i ^ bit) for i in range(count)])]
    ppermute x7 -> x10, starting transfers between devices: 3.15 us -> 6.08 us  [swap(): return lax.ppermute(value, 'kv', [(i, i ^ bit) for i in range(count)])]
    ppermute x6, waiting for transfers between devices: 7.72 us -> 5.93 us  [ring(): lax.ppermute(value, 'kv', [(i, (i + by) % count) for i in range(count)])]
    unnamed x4 -> x6, local copies, waits for them, and re-layouts: 0.01 us -> 1.42 us
  transfers between devices with their start and end apart: 15 -> 18, of which waited for: 8 -> 8; matrix products, arithmetic and copies ran while one was open for 0% -> 2% of each run, Pallas kernels for 12% -> 10%
where the time goes in v2:
time: 69.3 us; the launch traced here: 68.9 us
  waiting for transfers between devices  33.4 us (48%)
  starting transfers between devices  23.3 us (34%)
  Pallas kernels  10.1 us (15%)
  local copies, waits for them, and re-layouts  1.42 us (2%)
  between operations  0.79 us (1%)
    ppermute x10, waiting for transfers between devices, swap(): return lax.ppermute(value, 'kv', [(i, i ^ bit) for i in range(count)])  27.4 us
    ppermute x6, starting transfers between devices, ring(): lax.ppermute(value, 'kv', [(i, (i + by) % count) for i in range(count)])  14.2 us
    ppermute x10, starting transfers between devices, swap(): return lax.ppermute(value, 'kv', [(i, i ^ bit) for i in range(count)])  6.08 us
    ppermute x6, waiting for transfers between devices, ring(): lax.ppermute(value, 'kv', [(i, (i + by) % count) for i in range(count)])  5.93 us
    pallas_call x4, Pallas kernels, far_call(): call(functools.partial(far_body, sel, heads, groups, last), kinds, [VMEM]...  3.52 us
    ppermute x2, starting transfers between devices, per_device(): lax.ppermute(first, 'tp', [((i + s) % tp, i) for i in range(tp)])  2.98 us
    pallas_call x1, Pallas kernels, per_device(): pl.pallas_call(functools.partial(pack_body, levels, heads, near, far, ear...  1.6 us
    unnamed x6, local copies, waits for them, and re-layouts  1.42 us
  transfers between devices with their start and end apart: 18, of which 8 were waited for; matrix products, arithmetic and copies ran while one was open for 2% of the time, Pallas kernels for 10%

profile of v2, /device:TPU:4, one launch (start us, length us, event | category | flops | bytes accessed | tf_op | source)
XLA Modules:
  0.0 68.9 jit_solution(14292420995800027598)
XLA Ops:
  0.6 1.6 %shard_map.111 = (bf16[1088,128]{1,0:T(8,128)(2,1)S(1)}, bf16[128,1024]{1,0:T(8,128)(2,1)S(1)}, bf16[128,1024]{1,0:T(8,128)(2,1)S(1)}) custom-call(s32[2,16]{1,0:T(2,128)} %picked_hbm.1, bf16[512,128]{1,0:T(8,128)(2,1)} %bitcast.22, bf16[512,128]{1,0:T(8,128)(2,1)} %bitcast.23, bf16[512,128]{1,0:T(8,128)(2,1)} %bitcast.24, f32[2,256]{1,0:T(2,128)} %bitcast.25, ...), custom_call_target="tpu_custom_call" | custom-call | tf_op jit(solution)/shard_map/pallas_call | solution.py:323
  2.3 3.7 %collective-permute-start = (bf16[1088,128]{1,0:T(8,128)(2,1)S(1)}, bf16[1088,128]{1,0:T(8,128)(2,1)S(1)}, u32[]{:S(2)}, u32[]{:S(2)}) collective-permute-start(bf16[1088,128]{1,0:T(8,128)(2,1)S(1)} %get-tuple-element.27.msg_ref.yes_ref), channel_id=1, source_target_pairs={{0,24},{2,26},{4,28},{6,30},{8,0},{10,2},{12,4},{14,6},{16,8},{18,... | collective-permute-start | bytes 835592 | tf_op jit(solution)/shard_map/ppermute | solution.py:22
  5.9 5.9 %collective-permute-done.no_ref.refs_0_ = bf16[1088,128]{1,0:T(8,128)(2,1)S(1)} collective-permute-done((bf16[1088,128]{1,0:T(8,128)(2,1)S(1)}, bf16[1088,128]{1,0:T(8,128)(2,1)S(1)}, u32[]{:S(2)}, u32[]{:S(2)}) %collective-permute-start) | collective-permute-done | bytes 278560 | tf_op jit(solution)/shard_map/ppermute | solution.py:22
  11.9 0.6 collective-permute-start.1
  12.4 1.5 %collective-permute-start.9 = (bf16[128,1024]{1,0:T(8,128)(2,1)S(1)}, bf16[128,1024]{1,0:T(8,128)(2,1)S(1)}, u32[]{:S(2)}, u32[]{:S(2)}) collective-permute-start(bf16[128,1024]{1,0:T(8,128)(2,1)S(1)} %get-tuple-element.45), channel_id=1, source_target_pairs={{0,4},{2,6},{4,0},{6,2},{8,12},{10,14},{12,8},{14,10},{16,20},{18,... | collective-permute-start | bytes 786440 | tf_op jit(solution)/shard_map/ppermute | solution.py:27
  14.0 4.3 %collective-permute-start.3 = (bf16[1088,128]{1,0:T(8,128)(2,1)S(1)}, bf16[1088,128]{1,0:T(8,128)(2,1)S(1)}, u32[]{:S(2)}, u32[]{:S(2)}) collective-permute-start(bf16[1088,128]{1,0:T(8,128)(2,1)S(1)} %collective-permute-done.no_ref.refs_0_), channel_id=1, source_target_pairs={{0,24},{2,26},{4,28},{6,30},{8,0},{10,2},{12,4},{14,6},{16,8},{18,... | collective-permute-start | bytes 835592 | tf_op jit(solution)/shard_map/ppermute | solution.py:22
  18.2 3.2 %collective-permute-done.1.no_ref.refs_0_ = bf16[1088,128]{1,0:T(8,128)(2,1)S(1)} collective-permute-done((bf16[1088,128]{1,0:T(8,128)(2,1)S(1)}, bf16[1088,128]{1,0:T(8,128)(2,1)S(1)}, u32[]{:S(2)}, u32[]{:S(2)}) %collective-permute-start.1) | collective-permute-done | bytes 278560 | tf_op jit(solution)/shard_map/ppermute | solution.py:27
  21.6 1.4 %shard_map.120 = (bf16[256,1024]{1,0:T(8,128)(2,1)S(1)}, bf16[256,1024]{1,0:T(8,128)(2,1)S(1)}) custom-call(bf16[256,4096]{1,0:T(8,128)(2,1)} %x_hbm.3), custom_call_target="tpu_custom_call" | custom-call | flops 1048576 | bytes 1048576 | tf_op jit(solution)/shard_map/pallas_call | solution.py:347
  22.9 0.5 collective-permute-start.8
  23.5 1.0 %shard_map.112 = (f32[512,128]{1,0:T(8,128)S(1)}, f32[512,128]{1,0:T(8,128)S(1)}, f32[512,128]{1,0:T(8,128)S(1)}) custom-call(bf16[1088,128]{1,0:T(8,128)(2,1)S(1)} %get-tuple-element.27.msg_ref.yes_ref, bf16[512,128]{1,0:T(8,128)(2,1)S(1)} %bitcast.11, bf16[512,128]{1,0:T(8,128)(2,1)S(1)} %bitcast.16), custom_call_target="tpu_custom_call" | custom-call | flops 335544320 | bytes 2097152 | tf_op jit(solution)/shard_map/pallas_call | solution.py:364
  24.5 2.6 %collective-permute-done.9.refs_2_ = bf16[128,1024]{1,0:T(8,128)(2,1)S(1)} collective-permute-done((bf16[128,1024]{1,0:T(8,128)(2,1)S(1)}, bf16[128,1024]{1,0:T(8,128)(2,1)S(1)}, u32[]{:S(2)}, u32[]{:S(2)}) %collective-permute-start.9) | collective-permute-done | bytes 262176 | tf_op jit(solution)/shard_map/ppermute | solution.py:27
  27.1 1.5 %collective-permute-start.10 = (bf16[128,1024]{1,0:T(8,128)(2,1)S(1)}, bf16[128,1024]{1,0:T(8,128)(2,1)S(1)}, u32[]{:S(2)}, u32[]{:S(2)}) collective-permute-start(bf16[128,1024]{1,0:T(8,128)(2,1)S(1)} %collective-permute-done.9.refs_2_), channel_id=1, source_target_pairs={{1,0},{0,1},{3,2},{2,3},{5,4},{4,5},{7,6},{6,7},{9,8},{8,9},{11,10... | collective-permute-start | bytes 786440 | tf_op jit(solution)/shard_map/ppermute | solution.py:363
  28.7 1.5 %collective-permute-start.12 = (bf16[128,1024]{1,0:T(8,128)(2,1)S(1)}, bf16[128,1024]{1,0:T(8,128)(2,1)S(1)}, u32[]{:S(2)}, u32[]{:S(2)}) collective-permute-start(bf16[128,1024]{1,0:T(8,128)(2,1)S(1)} %collective-permute-done.11.refs_4_), channel_id=1, source_target_pairs={{1,0},{0,1},{3,2},{2,3},{5,4},{4,5},{7,6},{6,7},{9,8},{8,9},{11,10... | collective-permute-start | bytes 786440 | tf_op jit(solution)/shard_map/ppermute | solution.py:363
  30.2 0.9 %shard_map.115 = (bf16[512,128]{1,0:T(8,128)(2,1)S(1)}, f32[512,128]{1,0:T(8,128)S(1)}, f32[512,128]{1,0:T(8,128)S(1)}) custom-call(bf16[1088,128]{1,0:T(8,128)(2,1)S(1)} %collective-permute-done.no_ref.refs_0_, bf16[512,128]{1,0:T(8,128)(2,1)S(1)} %bitcast.12, bf16[512,128]{1,0:T(8,128)(2,1)S(1)} %bitcast.17, f32[512,128]{1,0:T(8,128)S(1)} %get-tuple-element.29.refs_3_, ...), custom_call_target="tpu_custom_call" | custom-call | flops 335544320 | bytes 524288 | tf_op jit(solution)/shard_map/pallas_call | solution.py:375
  31.1 0.9 %shard_map.116 = (bf16[512,128]{1,0:T(8,128)(2,1)S(1)}, f32[512,128]{1,0:T(8,128)S(1)}, f32[512,128]{1,0:T(8,128)S(1)}) custom-call(bf16[1088,128]{1,0:T(8,128)(2,1)S(1)} %collective-permute-done.1.no_ref.refs_0_, bf16[512,128]{1,0:T(8,128)(2,1)S(1)} %bitcast.13, bf16[512,128]{1,0:T(8,128)(2,1)S(1)} %bitcast.18, f32[512,128]{1,0:T(8,128)S(1)} %get-tuple-element.31.refs_3_, ...), custom_call_target="tpu_custom_call" | custom-call | flops 335544320 | bytes 524288 | tf_op jit(solution)/shard_map/pallas_call | solution.py:375
  32.0 0.9 %shard_map.117 = (bf16[512,128]{1,0:T(8,128)(2,1)S(1)}, f32[512,128]{1,0:T(8,128)S(1)}, f32[512,128]{1,0:T(8,128)S(1)}) custom-call(bf16[1088,128]{1,0:T(8,128)(2,1)S(1)} %collective-permute-done.3.refs_0_, bf16[512,128]{1,0:T(8,128)(2,1)S(1)} %bitcast.14, bf16[512,128]{1,0:T(8,128)(2,1)S(1)} %bitcast.19, f32[512,128]{1,0:T(8,128)S(1)} %get-tuple-element.33.refs_3_, ...), custom_call_target="tpu_custom_call" | custom-call | flops 335544320 | bytes 524288 | tf_op jit(solution)/shard_map/pallas_call | solution.py:375
  32.8 0.9 %shard_map.118 = (bf16[512,128]{1,0:T(8,128)(2,1)S(1)}, f32[512,128]{1,0:T(8,128)S(1)}, f32[512,128]{1,0:T(8,128)S(1)}, bf16[256,256]{1,0:T(8,128)(2,1)S(1)}) custom-call(bf16[1088,128]{1,0:T(8,128)(2,1)S(1)} %collective-permute-done.2.refs_0_, bf16[512,128]{1,0:T(8,128)(2,1)S(1)} %bitcast.15, bf16[512,128]{1,0:T(8,128)(2,1)S(1)} %bitcast.20, ...), custom_call_target="tpu_custom_call" | custom-call | flops 335544320 | bytes 524288 | tf_op jit(solution)/shard_map/pallas_call | solution.py:375
  33.8 1.6 %collective-permute-start.14 = (bf16[256,256]{1,0:T(8,128)(2,1)S(1)}, bf16[256,256]{1,0:T(8,128)(2,1)S(1)}, u32[]{:S(2)}, u32[]{:S(2)}) collective-permute-start(bf16[256,256]{1,0:T(8,128)(2,1)S(1)} %get-tuple-element.47.refs_6_), channel_id=1, source_target_pairs={{0,4},{2,6},{4,0},{6,2},{8,12},{10,14},{12,8},{14,10},{16,20},{18,... | collective-permute-start | bytes 393224 | tf_op jit(solution)/shard_map/ppermute | solution.py:27
  35.9 3.5 %collective-permute-done.14.refs_8_ = bf16[256,256]{1,0:T(8,128)(2,1)S(1)} collective-permute-done((bf16[256,256]{1,0:T(8,128)(2,1)S(1)}, bf16[256,256]{1,0:T(8,128)(2,1)S(1)}, u32[]{:S(2)}, u32[]{:S(2)}) %collective-permute-start.14) | collective-permute-done | bytes 131104 | tf_op jit(solution)/shard_map/ppermute | solution.py:27
  39.4 0.7 collective-permute-start.15
  40.1 1.0 %collective-permute-done.15.refs_9_ = bf16[256,256]{1,0:T(8,128)(2,1)S(1)} collective-permute-done((bf16[256,256]{1,0:T(8,128)(2,1)S(1)}, bf16[256,256]{1,0:T(8,128)(2,1)S(1)}, u32[]{:S(2)}, u32[]{:S(2)}) %collective-permute-start.15) | collective-permute-done | bytes 131104 | tf_op jit(solution)/shard_map/ppermute | solution.py:27
  41.0 0.5 shard_map.122
  41.5 0.5 collective-permute-start.16
  42.1 1.6 %collective-permute-start.6 = (bf16[512,128]{1,0:T(8,128)(2,1)S(1)}, bf16[512,128]{1,0:T(8,128)(2,1)S(1)}, u32[]{:S(2)}, u32[]{:S(2)}) collective-permute-start(bf16[512,128]{1,0:T(8,128)(2,1)S(1)} %get-tuple-element.39), channel_id=1, source_target_pairs={{0,8},{2,10},{4,12},{6,14},{8,16},{10,18},{12,20},{14,22},{16,24},... | collective-permute-start | bytes 393224 | tf_op jit(solution)/shard_map/ppermute | solution.py:22
  43.6 2.9 %collective-permute-start.7 = (bf16[512,128]{1,0:T(8,128)(2,1)S(1)}, bf16[512,128]{1,0:T(8,128)(2,1)S(1)}, u32[]{:S(2)}, u32[]{:S(2)}) collective-permute-start(bf16[512,128]{1,0:T(8,128)(2,1)S(1)} %get-tuple-element.40), channel_id=1, source_target_pairs={{0,16},{2,18},{4,20},{6,22},{8,24},{10,26},{12,28},{14,30},{16,0},... | collective-permute-start | bytes 393224 | tf_op jit(solution)/shard_map/ppermute | solution.py:22
  46.5 1.8 %collective-permute-start.5 = (bf16[512,128]{1,0:T(8,128)(2,1)S(1)}, bf16[512,128]{1,0:T(8,128)(2,1)S(1)}, u32[]{:S(2)}, u32[]{:S(2)}) collective-permute-start(bf16[512,128]{1,0:T(8,128)(2,1)S(1)} %get-tuple-element.38), channel_id=1, source_target_pairs={{0,4},{2,6},{4,8},{6,10},{8,12},{10,14},{12,16},{14,18},{16,20},{1... | collective-permute-start | bytes 393224 | tf_op jit(solution)/shard_map/ppermute | solution.py:22
  48.9 6.8 %collective-permute-done.16.came_ref = bf16[512,256]{1,0:T(8,128)(2,1)S(1)} collective-permute-done((bf16[512,256]{1,0:T(8,128)(2,1)S(1)}, bf16[512,256]{1,0:T(8,128)(2,1)S(1)}, u32[]{:S(2)}, u32[]{:S(2)}) %collective-permute-start.16) | collective-permute-done | bytes 262176 | tf_op jit(solution)/shard_map/ppermute | solution.py:27
  55.8 0.7 %copy.12 = f32[256,2,128]{2,1,0:T(2,128)} copy(f32[256,2,128]{2,1,0:T(2,128)S(1)} %bitcast.10) | data formatting | bytes 524288
  56.5 0.7 %copy.13 = f32[256,2,128]{2,1,0:T(2,128)} copy(f32[256,2,128]{2,1,0:T(2,128)S(1)} %bitcast.9) | data formatting | bytes 524288
  57.2 0.8 %shard_map.119 = f32[512,128]{1,0:T(8,128)} custom-call(f32[512,128]{1,0:T(8,128)S(1)} %get-tuple-element.28.dq_ref, bf16[512,128]{1,0:T(8,128)(2,1)S(1)} %collective-permute-done.4.refs_0_, bf16[512,128]{1,0:T(8,128)(2,1)S(1)} %collective-permute-done.5.refs_1_, bf16[512,128]{1,0:T(8,128)(2,1)S(1)} %collective-permute-done.6.refs_2_, ...), custom_call_target="tpu_custom_call" | custom-call | flops 1048576 | bytes 1048576 | tf_op jit(solution)/shard_map/pallas_call | solution.py:432
  58.0 10.2 %collective-permute-done.17.came_ref = bf16[256,256]{1,0:T(8,128)(2,1)S(1)} collective-permute-done((bf16[256,256]{1,0:T(8,128)(2,1)S(1)}, bf16[256,256]{1,0:T(8,128)(2,1)S(1)}, u32[]{:S(2)}, u32[]{:S(2)}) %collective-permute-start.17) | collective-permute-done | bytes 131104 | tf_op jit(solution)/shard_map/ppermute | solution.py:27
  68.2 0.7 %shard_map.124 = f32[256,256]{1,0:T(8,128)} custom-call(f32[256,256]{1,0:T(8,128)S(1)} %get-tuple-element.48.keep_ref, bf16[256,256]{1,0:T(8,128)(2,1)S(1)} %collective-permute-done.17.came_ref), custom_call_target="tpu_custom_call" | custom-call | flops 262144 | bytes 655360 | tf_op jit(solution)/shard_map/pallas_call | solution.py:426
  (24 shorter events, 1.5 us)
Async XLA Ops:
  2.2 21.3 %copy-start = (bf16[256,2,128]{2,1,0:T(2,128)(2,1)S(1)}, bf16[256,2,128]{2,1,0:T(2,128)(2,1)}, u32[]{:S(2)}) copy-start(bf16[256,2,128]{2,1,0:T(2,128)(2,1)} %param.9) | copy-start | bytes 393220
  2.3 21.2 %copy-start.1 = (bf16[256,2,128]{2,1,0:T(2,128)(2,1)S(1)}, bf16[256,2,128]{2,1,0:T(2,128)(2,1)}, u32[]{:S(2)}) copy-start(bf16[256,2,128]{2,1,0:T(2,128)(2,1)} %param.10) | copy-start | bytes 393220
  2.3 9.6 %collective-permute-start = (bf16[1088,128]{1,0:T(8,128)(2,1)S(1)}, bf16[1088,128]{1,0:T(8,128)(2,1)S(1)}, u32[]{:S(2)}, u32[]{:S(2)}) collective-permute-start(bf16[1088,128]{1,0:T(8,128)(2,1)S(1)} %get-tuple-element.27.msg_ref.yes_ref), channel_id=1, source_target_pairs={{0,24},{2,26},{4,28},{6,30},{8,0},{10,2},{12,4},{14,6},{16,8},{18,... | collective-permute-start | bytes 835592 | tf_op jit(solution)/shard_map/ppermute | solution.py:22
  11.9 9.6 %collective-permute-start.1 = (bf16[1088,128]{1,0:T(8,128)(2,1)S(1)}, bf16[1088,128]{1,0:T(8,128)(2,1)S(1)}, u32[]{:S(2)}, u32[]{:S(2)}) collective-permute-start(bf16[1088,128]{1,0:T(8,128)(2,1)S(1)} %shard_map.113), channel_id=1, source_target_pairs={{0,4},{2,6},{4,0},{6,2},{8,12},{10,14},{12,8},{14,10},{16,20},{18,... | collective-permute-start | bytes 835592 | tf_op jit(solution)/shard_map/ppermute | solution.py:27
  12.4 14.6 %collective-permute-start.9 = (bf16[128,1024]{1,0:T(8,128)(2,1)S(1)}, bf16[128,1024]{1,0:T(8,128)(2,1)S(1)}, u32[]{:S(2)}, u32[]{:S(2)}) collective-permute-start(bf16[128,1024]{1,0:T(8,128)(2,1)S(1)} %get-tuple-element.45), channel_id=1, source_target_pairs={{0,4},{2,6},{4,0},{6,2},{8,12},{10,14},{12,8},{14,10},{16,20},{18,... | collective-permute-start | bytes 786440 | tf_op jit(solution)/shard_map/ppermute | solution.py:27
  14.0 14.8 %collective-permute-start.11 = (bf16[128,1024]{1,0:T(8,128)(2,1)S(1)}, bf16[128,1024]{1,0:T(8,128)(2,1)S(1)}, u32[]{:S(2)}, u32[]{:S(2)}) collective-permute-start(bf16[128,1024]{1,0:T(8,128)(2,1)S(1)} %get-tuple-element.46), channel_id=1, source_target_pairs={{0,6},{2,4},{4,2},{6,0},{8,14},{10,12},{12,10},{14,8},{16,22},{18,... | collective-permute-start | bytes 786440 | tf_op jit(solution)/shard_map/ppermute | solution.py:27
  14.0 18.0 %collective-permute-start.3 = (bf16[1088,128]{1,0:T(8,128)(2,1)S(1)}, bf16[1088,128]{1,0:T(8,128)(2,1)S(1)}, u32[]{:S(2)}, u32[]{:S(2)}) collective-permute-start(bf16[1088,128]{1,0:T(8,128)(2,1)S(1)} %collective-permute-done.no_ref.refs_0_), channel_id=1, source_target_pairs={{0,24},{2,26},{4,28},{6,30},{8,0},{10,2},{12,4},{14,6},{16,8},{18,... | collective-permute-start | bytes 835592 | tf_op jit(solution)/shard_map/ppermute | solution.py:22
  21.5 11.4 %collective-permute-start.2 = (bf16[1088,128]{1,0:T(8,128)(2,1)S(1)}, bf16[1088,128]{1,0:T(8,128)(2,1)S(1)}, u32[]{:S(2)}, u32[]{:S(2)}) collective-permute-start(bf16[1088,128]{1,0:T(8,128)(2,1)S(1)} %shard_map.114), channel_id=1, source_target_pairs={{0,2},{2,0},{4,6},{6,4},{8,10},{10,8},{12,14},{14,12},{16,18},{18,... | collective-permute-start | bytes 835592 | tf_op jit(solution)/shard_map/ppermute | solution.py:27
  22.9 17.1 %collective-permute-start.8 = (bf16[256,1024]{1,0:T(8,128)(2,1)S(1)}, bf16[256,1024]{1,0:T(8,128)(2,1)S(1)}, u32[]{:S(2)}, u32[]{:S(2)}) collective-permute-start(bf16[256,1024]{1,0:T(8,128)(2,1)S(1)} %get-tuple-element.44), channel_id=1, source_target_pairs={{0,2},{2,0},{4,6},{6,4},{8,10},{10,8},{12,14},{14,12},{16,18},{18,... | collective-permute-start | bytes 1572872 | tf_op jit(solution)/shard_map/ppermute | solution.py:27
  27.1 13.0 %collective-permute-start.10 = (bf16[128,1024]{1,0:T(8,128)(2,1)S(1)}, bf16[128,1024]{1,0:T(8,128)(2,1)S(1)}, u32[]{:S(2)}, u32[]{:S(2)}) collective-permute-start(bf16[128,1024]{1,0:T(8,128)(2,1)S(1)} %collective-permute-done.9.refs_2_), channel_id=1, source_target_pairs={{1,0},{0,1},{3,2},{2,3},{5,4},{4,5},{7,6},{6,7},{9,8},{8,9},{11,10... | collective-permute-start | bytes 786440 | tf_op jit(solution)/shard_map/ppermute | solution.py:363
  28.7 11.3 %collective-permute-start.12 = (bf16[128,1024]{1,0:T(8,128)(2,1)S(1)}, bf16[128,1024]{1,0:T(8,128)(2,1)S(1)}, u32[]{:S(2)}, u32[]{:S(2)}) collective-permute-start(bf16[128,1024]{1,0:T(8,128)(2,1)S(1)} %collective-permute-done.11.refs_4_), channel_id=1, source_target_pairs={{1,0},{0,1},{3,2},{2,3},{5,4},{4,5},{7,6},{6,7},{9,8},{8,9},{11,10... | collective-permute-start | bytes 786440 | tf_op jit(solution)/shard_map/ppermute | solution.py:363
  33.8 5.6 %collective-permute-start.14 = (bf16[256,256]{1,0:T(8,128)(2,1)S(1)}, bf16[256,256]{1,0:T(8,128)(2,1)S(1)}, u32[]{:S(2)}, u32[]{:S(2)}) collective-permute-start(bf16[256,256]{1,0:T(8,128)(2,1)S(1)} %get-tuple-element.47.refs_6_), channel_id=1, source_target_pairs={{0,4},{2,6},{4,0},{6,2},{8,12},{10,14},{12,8},{14,10},{16,20},{18,... | collective-permute-start | bytes 393224 | tf_op jit(solution)/shard_map/ppermute | solution.py:27
  35.4 4.7 %collective-permute-start.13 = (bf16[256,256]{1,0:T(8,128)(2,1)S(1)}, bf16[256,256]{1,0:T(8,128)(2,1)S(1)}, u32[]{:S(2)}, u32[]{:S(2)}) collective-permute-start(bf16[256,256]{1,0:T(8,128)(2,1)S(1)} %get-tuple-element.47.refs_6_), channel_id=1, source_target_pairs={{0,2},{2,0},{4,6},{6,4},{8,10},{10,8},{12,14},{14,12},{16,18},{18,... | collective-permute-start | bytes 393224 | tf_op jit(solution)/shard_map/ppermute | solution.py:27
  39.4 1.7 %collective-permute-start.15 = (bf16[256,256]{1,0:T(8,128)(2,1)S(1)}, bf16[256,256]{1,0:T(8,128)(2,1)S(1)}, u32[]{:S(2)}, u32[]{:S(2)}) collective-permute-start(bf16[256,256]{1,0:T(8,128)(2,1)S(1)} %collective-permute-done.14.refs_8_), channel_id=1, source_target_pairs={{0,2},{2,0},{4,6},{6,4},{8,10},{10,8},{12,14},{14,12},{16,18},{18,... | collective-permute-start | bytes 393224 | tf_op jit(solution)/shard_map/ppermute | solution.py:27
  41.5 14.1 %collective-permute-start.16 = (bf16[512,256]{1,0:T(8,128)(2,1)S(1)}, bf16[512,256]{1,0:T(8,128)(2,1)S(1)}, u32[]{:S(2)}, u32[]{:S(2)}) collective-permute-start(bf16[512,256]{1,0:T(8,128)(2,1)S(1)} %shard_map.122), channel_id=1, source_target_pairs={{0,8},{2,10},{4,12},{6,14},{8,0},{10,2},{12,4},{14,6},{16,24},{18,... | collective-permute-start | bytes 786440 | tf_op jit(solution)/shard_map/ppermute | solution.py:27
  42.1 15.2 %collective-permute-start.6 = (bf16[512,128]{1,0:T(8,128)(2,1)S(1)}, bf16[512,128]{1,0:T(8,128)(2,1)S(1)}, u32[]{:S(2)}, u32[]{:S(2)}) collective-permute-start(bf16[512,128]{1,0:T(8,128)(2,1)S(1)} %get-tuple-element.39), channel_id=1, source_target_pairs={{0,8},{2,10},{4,12},{6,14},{8,16},{10,18},{12,20},{14,22},{16,24},... | collective-permute-start | bytes 393224 | tf_op jit(solution)/shard_map/ppermute | solution.py:22
  43.6 13.6 %collective-permute-start.7 = (bf16[512,128]{1,0:T(8,128)(2,1)S(1)}, bf16[512,128]{1,0:T(8,128)(2,1)S(1)}, u32[]{:S(2)}, u32[]{:S(2)}) collective-permute-start(bf16[512,128]{1,0:T(8,128)(2,1)S(1)} %get-tuple-element.40), channel_id=1, source_target_pairs={{0,16},{2,18},{4,20},{6,22},{8,24},{10,26},{12,28},{14,30},{16,0},... | collective-permute-start | bytes 393224 | tf_op jit(solution)/shard_map/ppermute | solution.py:22
  46.5 10.7 %collective-permute-start.5 = (bf16[512,128]{1,0:T(8,128)(2,1)S(1)}, bf16[512,128]{1,0:T(8,128)(2,1)S(1)}, u32[]{:S(2)}, u32[]{:S(2)}) collective-permute-start(bf16[512,128]{1,0:T(8,128)(2,1)S(1)} %get-tuple-element.38), channel_id=1, source_target_pairs={{0,4},{2,6},{4,8},{6,10},{8,12},{10,14},{12,16},{14,18},{16,20},{1... | collective-permute-start | bytes 393224 | tf_op jit(solution)/shard_map/ppermute | solution.py:22
  48.3 8.9 %collective-permute-start.4 = (bf16[512,128]{1,0:T(8,128)(2,1)S(1)}, bf16[512,128]{1,0:T(8,128)(2,1)S(1)}, u32[]{:S(2)}, u32[]{:S(2)}) collective-permute-start(bf16[512,128]{1,0:T(8,128)(2,1)S(1)} %get-tuple-element.37), channel_id=1, source_target_pairs={{0,2},{2,4},{4,6},{6,8},{8,10},{10,12},{12,14},{14,16},{16,18},{18... | collective-permute-start | bytes 393224 | tf_op jit(solution)/shard_map/ppermute | solution.py:22
  55.7 12.5 %collective-permute-start.17 = (bf16[256,256]{1,0:T(8,128)(2,1)S(1)}, bf16[256,256]{1,0:T(8,128)(2,1)S(1)}, u32[]{:S(2)}, u32[]{:S(2)}) collective-permute-start(bf16[256,256]{1,0:T(8,128)(2,1)S(1)} %get-tuple-element.49), channel_id=1, source_target_pairs={{0,16},{2,18},{4,20},{6,22},{8,24},{10,26},{12,28},{14,30},{16,0},... | collective-permute-start | bytes 393224 | tf_op jit(solution)/shard_map/ppermute | solution.py:27

commit v3 on v2

--- a/solution.py
+++ b/solution.py
@@ -22,6 +22,11 @@
     return lax.ppermute(value, "kv", [(i, (i + by) % count) for i in range(count)])
 
 
+def line(value, by):
+    count = lax.axis_size("kv")
+    return lax.ppermute(value, "kv", [(i, i + by) for i in range(count) if 0 <= i + by < count])
+
+
 def swap(value, bit):
     count = lax.axis_size("kv")
     return lax.ppermute(value, "kv", [(i, i ^ bit) for i in range(count)])
@@ -30,7 +35,7 @@
 def forward(msg, levels, mix):
     if levels < 4:
         return [ring(msg, -(1 << level)) for level in range(levels)]
-    four = ring(msg, -4)
+    four = line(msg, -4)
     eight = ring(four, -4)
     payload = mix(2, msg, four)
     two = swap(payload, 2)
@@ -82,7 +87,7 @@
     return high, middle, (rest - middle.astype(F32)).astype(BF16)
 
 
-def pack_body(levels, heads, near, far, wanted, picked_hbm, q_hbm, g_hbm, a_hbm, lse_hbm, x_hbm, msg_ref, *refs):
+def pack_body(levels, heads, near, far, wanted, picked_hbm, q_hbm, g_hbm, a_hbm, lse_hbm, x_hbm, k_hbm, v_hbm, msg_ref, *refs):
     picked_ref, a_ref, lse_ref, sem, cut_sem = refs[-5:]
     rows = q_hbm.shape[0]
     tok = rows // heads
@@ -97,7 +102,12 @@
         pltpu.make_async_copy(a_hbm, a_ref, sem.at[3]),
         pltpu.make_async_copy(q_hbm, msg_ref.at[0:rows, :], sem.at[4]),
     ]
-    pieces = cuts(near, far, wanted, x_hbm, refs[:-5], cut_sem)
+    kv_ref = refs[0]
+    pieces = cuts(near, far, wanted, x_hbm, refs[1:-5], cut_sem)
+    pieces += [
+        pltpu.make_async_copy(k_hbm, kv_ref.at[0:rows, :], sem.at[5]),
+        pltpu.make_async_copy(v_hbm, kv_ref.at[rows : 2 * rows, :], sem.at[6]),
+    ]
     for copy in copies + pieces:
         copy.start()
     me = lax.axis_index("kv")
@@ -143,7 +153,7 @@
     return (rows[0:1] + rows[1:2]) + rows[2:3]
 
 
-def group_terms(msg_ref, key, value, group, heads, sel, causal):
+def group_terms(msg_ref, key, value, group, heads, sel, causal, grads=True, side=True):
     rows, dim = key.shape
     tok = rows // heads
     _, codes, stats, _ = layout(tok, heads, sel)
@@ -179,26 +189,38 @@
     score_grad = weights * (nt(value, grad) - dots)
     weight_pairs = weights.astype(BF16)
     grad_pairs = score_grad.astype(BF16)
-    return nn(grad_pairs, query), nn(weight_pairs, grad), tn(grad_pairs, key)
+    query_term = tn(grad_pairs, key) if side else None
+    if not grads:
+        return query_term
+    return nn(grad_pairs, query), nn(weight_pairs, grad), query_term
+
+
+def near_body(sel, heads, group, msg_ref, kv_ref, dq_in, dq_out):
+    rows = kv_ref.shape[0] // 2
+    term = group_terms(msg_ref, kv_ref[0:rows, :], kv_ref[rows : 2 * rows, :], group, heads, sel, False, False)
+    dq_out[...] = dq_in[...] + term
 
 
 def own_body(sel, heads, msg_ref, k_ref, v_ref, dk_ref, dv_ref, dq_ref):
     dk_ref[...], dv_ref[...], dq_ref[...] = group_terms(msg_ref, k_ref[...], v_ref[...], 0, heads, sel, True)
 
 
-def far_body(sel, heads, groups, last, *refs):
+def far_body(sel, heads, groups, last, sides, *refs):
     count = len(groups)
     msgs = refs[:count]
     k_ref, v_ref, dk_in, dv_in = refs[count : count + 4]
-    dqs = refs[count + 4 : 2 * count + 4]
-    dk_out, dv_out = refs[2 * count + 4 : 2 * count + 6]
+    dqs = refs[count + 4 : count + 4 + len(sides)]
+    dk_out, dv_out = refs[count + 4 + len(sides) : count + 6 + len(sides)]
     rows, dim = k_ref.shape
     scale = dim ** (-0.5)
     dk, dv = dk_in[...], dv_in[...]
     for index, group in enumerate(groups):
-        dk_term, dv_term, dq = group_terms(msgs[index], k_ref[...], v_ref[...], group, heads, sel, False)
+        dk_term, dv_term, dq = group_terms(
+            msgs[index], k_ref[...], v_ref[...], group, heads, sel, False, True, group in sides
+        )
         dk, dv = dk + dk_term, dv + dv_term
-        dqs[index][...] = dq.astype(BF16)
+        if group in sides:
+            dqs[sides.index(group)][...] = dq.astype(BF16)
     dv_out[...] = dv
     if not last:
         dk_out[...] = dk
@@ -230,19 +252,24 @@
         out_ref[...] = no_ref[...]
 
 
-def share_of(tok, m, tp):
-    return tok // tp if m > 1 and tok % (16 * tp) == 0 else tok
+def shares_of(tok, m, near, tp):
+    share = tok // tp
+    if m < 2 or share % 32:
+        return [(0, tok)]
+    if m < near - 1:
+        return [(0, share)]
+    return [(0, share // 2), (share // 2, share // 2)]
 
 
 def cuts(near, far, wanted, x_hbm, out_refs, sem):
     rank = lax.rem(lax.axis_index("kv"), near)
     width = x_hbm.shape[1] // (near * far)
     copies = []
-    for index, (m, ref) in enumerate(zip(wanted, out_refs)):
-        share = ref.shape[0]
+    for index, ((m, first, share), ref) in enumerate(zip(wanted, out_refs)):
         rows = slice(None)
         if share < x_hbm.shape[0]:
-            rows = pl.ds(pl.multiple_of(lax.axis_index("tp") * share, share), share)
+            of_plane = x_hbm.shape[0] // lax.axis_size("tp")
+            rows = pl.ds(pl.multiple_of(lax.axis_index("tp") * of_plane + first, share), share)
         for z in range(far):
             at = pl.multiple_of((z * near + (rank ^ m)) * width, width)
             copies.append(
@@ -263,22 +290,22 @@
         copy.wait()
 
 
-def weight_body(near, far, parity, counts, *refs):
-    pieces = refs[: sum(counts)]
-    rounds_refs, out_ref = refs[sum(counts) : -1], refs[-1]
-    me = lax.axis_index("kv")
-    depth = lax.div(me, near)
+def weight_body(near, far, parity, plan, *refs):
+    pieces = refs[: len(plan)]
+    rounds_refs, out_ref = refs[len(plan) : -1], refs[-1]
+    depth = lax.div(lax.axis_index("kv"), near)
     tok = rounds_refs[0].shape[0]
     width = pieces[0].shape[1] // far
-    step = 2 if parity is not None else 1
     rights = []
-    for m in range(near):
-        for s in range(counts[m]):
-            share = tok // counts[m]
-            at = lax.rem(lax.axis_index("tp") + s, counts[m]) * share if counts[m] > 1 else 0
-            rights.append(rounds_refs[m][pl.ds(pl.multiple_of(at, share), share), :] if counts[m] > 1 else rounds_refs[m][...])
+    for m, first, share, turn in plan:
+        if share == tok:
+            rights.append(rounds_refs[m][...])
+            continue
+        planes = lax.axis_size("tp")
+        at = lax.rem(lax.axis_index("tp") + turn, planes) * (tok // planes) + first
+        rights.append(rounds_refs[m][pl.ds(pl.multiple_of(at, share), share), :])
     right = jnp.concatenate(rights, axis=0)
-    for index, rel in enumerate(range(parity or 0, far, step)):
+    for index, rel in enumerate(range(parity, far, 2)):
         at = pl.multiple_of((depth ^ rel) * width, width)
         left = jnp.concatenate([piece[:, pl.ds(at, width)] for piece in pieces], axis=0)
         out_ref[index * width : (index + 1) * width, :] = tn(left, right).astype(out_ref.dtype)
@@ -318,23 +345,25 @@
     pairs = rows * rows * dim * 10
     width = layer_input.shape[1] // count
     blocked = width % 128 == 0 and far > 1
-    shares = [share_of(tok, m, tp) for m in range(near)]
-    early = list(range(2, near)) if blocked else []
-    msg, *first = pl.pallas_call(
+    early = []
+    if blocked:
+        early = [(m, *part) for m in range(2, near) for part in shares_of(tok, m, near, tp)]
+    msg, kv, *first = pl.pallas_call(
         functools.partial(pack_body, levels, heads, near, far, early),
-        out_shape=[pltpu.VMEM((msg_rows, dim), BF16)]
-        + [pltpu.VMEM((shares[m], far * width), BF16) for m in early],
-        in_specs=[HBM] * 6,
-        out_specs=[VMEM] * (1 + len(early)),
+        out_shape=[pltpu.VMEM((msg_rows, dim), BF16), pltpu.VMEM((2 * rows, dim), BF16)]
+        + [pltpu.VMEM((part[2], far * width), BF16) for part in early],
+        in_specs=[HBM] * 8,
+        out_specs=[VMEM] * (2 + len(early)),
         scratch_shapes=[
             pltpu.SMEM(picked.shape, jnp.int32),
             pltpu.VMEM((rows, dim), BF16),
             pltpu.VMEM((heads, tok), F32),
-            pltpu.SemaphoreType.DMA((5,)),
+            pltpu.SemaphoreType.DMA((7,)),
             pltpu.SemaphoreType.DMA((max(1, len(early)) * far,)),
         ],
         compiler_params=pltpu.CompilerParams(vmem_limit_bytes=62000000),
-    )(picked, flat(queries), flat(out_grad), flat(attended), log_sum.T, layer_input)
+    )(picked, flat(queries), flat(out_grad), flat(attended), log_sum.T, layer_input, key, value)
+    far_kv = line(kv, 1 << (levels - 1))
 
     def mix(bit, yes, no):
         return call(
@@ -343,7 +372,7 @@
 
     got = forward(msg, levels, mix)
     if blocked:
-        wanted = [m for m in (1, 0) if m < near]
+        wanted = [(m, 0, tok) for m in (1, 0) if m < near]
         later = pl.pallas_call(
             functools.partial(cut_body, near, far, wanted),
             out_shape=[pltpu.VMEM((tok, far * width), BF16) for _ in wanted],
@@ -354,13 +383,17 @@
             compiler_params=pltpu.CompilerParams(vmem_limit_bytes=56 << 20),
         )(layer_input)
         cut = dict(zip(early + wanted, first + list(later)))
-        pieces, counts = [cut[0]], [1]
-        for m in range(1, near):
-            pieces.append(swap(cut[m], m))
-            counts.append(tok // shares[m])
-            first = pieces[-1]
-            for s in range(1, counts[m]):
-                pieces.append(lax.ppermute(first, "tp", [((i + s) % tp, i) for i in range(tp)]))
+        pieces, plan = [], []
+        for (m, start, share), piece in cut.items():
+            if m:
+                piece = swap(piece, m)
+            pieces.append(piece)
+            plan.append((m, start, share, 0))
+            if share == tok:
+                continue
+            for s in range(1, tp):
+                pieces.append(lax.ppermute(piece, "tp", [((i + s) % tp, i) for i in range(tp)]))
+                plan.append((m, start, share, s))
     dk_own, dv_own, dq_own = call(
         functools.partial(own_body, sel, heads),
         [shape((rows, dim), F32)] * 3,
@@ -368,12 +401,18 @@
         pairs, 8 * rows * dim * 4,
     )(msg, key, value)
 
+    dq_near = call(
+        functools.partial(near_body, sel, heads, levels),
+        shape((rows, dim), F32), [VMEM] * 3, pairs * 3 // 5, 8 * rows * dim,
+    )(msg, far_kv, dq_own)
+
     def far_call(groups, dk, dv, last):
-        kinds = [shape((rows, dim), BF16)] * len(groups) + [shape((rows, dim), F32)] * 2
+        sides = [group for group in groups if group != levels]
+        kinds = [shape((rows, dim), BF16)] * len(sides) + [shape((rows, dim), F32)] * 2
         if last:
             kinds.append(shape((tok, heads * dim), BF16))
         return call(
-            functools.partial(far_body, sel, heads, groups, last),
+            functools.partial(far_body, sel, heads, groups, last, sides),
             kinds,
             [VMEM] * (len(groups) + 4),
             pairs * len(groups), 8 * rows * dim,
@@ -387,9 +426,10 @@
         stages = [(level,) for level in range(1, levels + 1)]
     for stage in stages:
         outs = far_call(stage, dk, dv, stage == stages[-1])
-        for group, side in zip(stage, outs):
+        sides = [group for group in stage if group != levels]
+        for group, side in zip(sides, outs):
             back[group] = ring(side, 1 << (group - 1))
-        outs = outs[len(stage) :]
+        outs = outs[len(sides) :]
         dk, dv = outs[:2]
     key_grad, value_grad, rounded = outs
     if blocked:
@@ -404,7 +444,7 @@
         def weight(parity, kind):
             blocks = far // 2
             return call(
-                functools.partial(weight_body, near, far, parity, counts),
+                functools.partial(weight_body, near, far, parity, plan),
                 shape((blocks * width, columns), kind),
                 [VMEM] * (len(pieces) + near),
                 2 * near * tok * blocks * width * columns, near * tok * far * width * 2,
@@ -430,8 +470,8 @@
         )
         total = lax.psum_scatter(terms, "kv", scatter_dimension=0, tiled=True)
     query_grad = call(
-        query_body, shape((rows, dim), F32), [VMEM] * (levels + 1), 1 << 20, rows * dim * 16, False
-    )(dq_own, *[back[group] for group in range(1, levels + 1)])
+        query_body, shape((rows, dim), F32), [VMEM] * levels, 1 << 20, rows * dim * 16, False
+    )(dq_near, *[back[group] for group in range(1, levels)])
     grads = [x.reshape(tok, heads, dim) for x in (query_grad, key_grad, value_grad)]
     return (*grads, total)
 

time: 69.3 us -> 75.2 us (1.085)
  the two profiles are of different devices: /device:TPU:4 before, /device:TPU:31 now
where the time goes in v3:
time: 75.2 us; the launch traced here: 74.9 us
  waiting for transfers between devices  33.5 us (45%)
  starting transfers between devices  28.1 us (37%)
  Pallas kernels  11.2 us (15%)
  local copies, waits for them, and re-layouts  1.42 us (2%)
  between operations  0.8 us (1%)
    ppermute x11, waiting for transfers between devices, swap(): return lax.ppermute(value, 'kv', [(i, i ^ bit) for i in range(count)])  17.9 us
    ppermute x11, starting transfers between devices, swap(): return lax.ppermute(value, 'kv', [(i, i ^ bit) for i in range(count)])  13.3 us
    ppermute x2, waiting for transfers between devices, line(): lax.ppermute(value, 'kv', [(i, i + by) for i in range(count) if 0 <= i +...  11.4 us
    ppermute x4, starting transfers between devices, ring(): lax.ppermute(value, 'kv', [(i, (i + by) % count) for i in range(count)])  9.58 us
    ppermute x3, waiting for transfers between devices, per_device(): lax.ppermute(piece, 'tp', [((i + s) % tp, i) for i in range(tp)])  4.18 us
    pallas_call x4, Pallas kernels, far_call(): call(functools.partial(far_body, sel, heads, groups, last, sides), kinds,...  3.61 us
    ppermute x2, starting transfers between devices, line(): lax.ppermute(value, 'kv', [(i, i + by) for i in range(count) if 0 <= i +...  3.5 us
    ppermute x3, starting transfers between devices, per_device(): lax.ppermute(piece, 'tp', [((i + s) % tp, i) for i in range(tp)])  1.72 us
  transfers between devices with their start and end apart: 20, of which 8 were waited for; matrix products, arithmetic and copies ran while one was open for 2% of the time, Pallas kernels for 11%

profile of v3, /device:TPU:31, one launch (start us, length us, event | category | flops | bytes accessed | tf_op | source)
XLA Modules:
  0.0 74.9 jit_solution(1500827383442810270)
XLA Ops:
  0.6 1.7 %shard_map.111 = (bf16[1088,128]{1,0:T(8,128)(2,1)S(1)}, bf16[1024,128]{1,0:T(8,128)(2,1)S(1)}, bf16[128,1024]{1,0:T(8,128)(2,1)S(1)}, bf16[64,1024]{1,0:T(8,128)(2,1)S(1)}, bf16[64,1024]{1,0:T(8,128)(2,1)S(1)}) custom-call(s32[2,16]{1,0:T(2,128)} %picked_hbm.1, bf16[512,128]{1,0:T(8,128)(2,1)} %bitcast.24, bf16[512,128]{1,0:T(8,128)(2,1)} %bitcast.25, ...), custom_call_target="tpu_custom_call" | custom-call | tf_op jit(solution)/shard_map/pallas_call | solution.py:351
  2.3 2.2 %collective-permute-start.1 = (bf16[1088,128]{1,0:T(8,128)(2,1)S(1)}, bf16[1088,128]{1,0:T(8,128)(2,1)S(1)}, u32[]{:S(2)}, u32[]{:S(2)}) collective-permute-start(bf16[1088,128]{1,0:T(8,128)(2,1)S(1)} %get-tuple-element.28.msg_ref.yes_ref), channel_id=1, source_target_pairs={{8,0},{10,2},{12,4},{14,6},{16,8},{18,10},{20,12},{22,14},{24,16},... | collective-permute-start | bytes 835592 | tf_op jit(solution)/shard_map/ppermute | solution.py:27
  4.6 5.3 %collective-permute-done.1.no_ref.refs_0_ = bf16[1088,128]{1,0:T(8,128)(2,1)S(1)} collective-permute-done((bf16[1088,128]{1,0:T(8,128)(2,1)S(1)}, bf16[1088,128]{1,0:T(8,128)(2,1)S(1)}, u32[]{:S(2)}, u32[]{:S(2)}) %collective-permute-start.1) | collective-permute-done | bytes 278560 | tf_op jit(solution)/shard_map/ppermute | solution.py:27
  10.2 2.2 %collective-permute-start.4 = (bf16[1088,128]{1,0:T(8,128)(2,1)S(1)}, bf16[1088,128]{1,0:T(8,128)(2,1)S(1)}, u32[]{:S(2)}, u32[]{:S(2)}) collective-permute-start(bf16[1088,128]{1,0:T(8,128)(2,1)S(1)} %collective-permute-done.1.no_ref.refs_0_), channel_id=1, source_target_pairs={{0,24},{2,26},{4,28},{6,30},{8,0},{10,2},{12,4},{14,6},{16,8},{18,... | collective-permute-start | bytes 835592 | tf_op jit(solution)/shard_map/ppermute | solution.py:22
  12.4 1.2 %collective-permute-start.8 = (bf16[128,1024]{1,0:T(8,128)(2,1)S(1)}, bf16[128,1024]{1,0:T(8,128)(2,1)S(1)}, u32[]{:S(2)}, u32[]{:S(2)}) collective-permute-start(bf16[128,1024]{1,0:T(8,128)(2,1)S(1)} %get-tuple-element.44), channel_id=1, source_target_pairs={{0,4},{2,6},{4,0},{6,2},{8,12},{10,14},{12,8},{14,10},{16,20},{18,... | collective-permute-start | bytes 786440 | tf_op jit(solution)/shard_map/ppermute | solution.py:32
  13.6 3.0 %collective-permute-done.2.no_ref.refs_0_ = bf16[1088,128]{1,0:T(8,128)(2,1)S(1)} collective-permute-done((bf16[1088,128]{1,0:T(8,128)(2,1)S(1)}, bf16[1088,128]{1,0:T(8,128)(2,1)S(1)}, u32[]{:S(2)}, u32[]{:S(2)}) %collective-permute-start.2) | collective-permute-done | bytes 278560 | tf_op jit(solution)/shard_map/ppermute | solution.py:32
  16.7 4.4 %collective-permute-start.3 = (bf16[1088,128]{1,0:T(8,128)(2,1)S(1)}, bf16[1088,128]{1,0:T(8,128)(2,1)S(1)}, u32[]{:S(2)}, u32[]{:S(2)}) collective-permute-start(bf16[1088,128]{1,0:T(8,128)(2,1)S(1)} %shard_map.115), channel_id=1, source_target_pairs={{0,2},{2,0},{4,6},{6,4},{8,10},{10,8},{12,14},{14,12},{16,18},{18,... | collective-permute-start | bytes 835592 | tf_op jit(solution)/shard_map/ppermute | solution.py:32
  21.1 1.4 %shard_map.121 = (bf16[256,1024]{1,0:T(8,128)(2,1)S(1)}, bf16[256,1024]{1,0:T(8,128)(2,1)S(1)}) custom-call(bf16[256,4096]{1,0:T(8,128)(2,1)} %x_hbm.3), custom_call_target="tpu_custom_call" | custom-call | flops 1048576 | bytes 1048576 | tf_op jit(solution)/shard_map/pallas_call | solution.py:376
  23.2 1.1 %shard_map.112 = (f32[512,128]{1,0:T(8,128)S(1)}, f32[512,128]{1,0:T(8,128)S(1)}, f32[512,128]{1,0:T(8,128)S(1)}) custom-call(bf16[1088,128]{1,0:T(8,128)(2,1)S(1)} %get-tuple-element.28.msg_ref.yes_ref, bf16[512,128]{1,0:T(8,128)(2,1)S(1)} %bitcast.12, bf16[512,128]{1,0:T(8,128)(2,1)S(1)} %bitcast.18), custom_call_target="tpu_custom_call" | custom-call | flops 335544320 | bytes 2097152 | tf_op jit(solution)/shard_map/pallas_call | solution.py:397
  24.3 0.9 %shard_map.116 = (bf16[512,128]{1,0:T(8,128)(2,1)S(1)}, f32[512,128]{1,0:T(8,128)S(1)}, f32[512,128]{1,0:T(8,128)S(1)}) custom-call(bf16[1088,128]{1,0:T(8,128)(2,1)S(1)} %collective-permute-done.1.no_ref.refs_0_, bf16[512,128]{1,0:T(8,128)(2,1)S(1)} %bitcast.13, bf16[512,128]{1,0:T(8,128)(2,1)S(1)} %bitcast.19, f32[512,128]{1,0:T(8,128)S(1)} %get-tuple-element.31.refs_3_, ...), custom_call_target="tpu_custom_call" | custom-call | flops 335544320 | bytes 524288 | tf_op jit(solution)/shard_map/pallas_call | solution.py:414
  25.3 0.9 %shard_map.117 = (bf16[512,128]{1,0:T(8,128)(2,1)S(1)}, f32[512,128]{1,0:T(8,128)S(1)}, f32[512,128]{1,0:T(8,128)S(1)}) custom-call(bf16[1088,128]{1,0:T(8,128)(2,1)S(1)} %collective-permute-done.2.no_ref.refs_0_, bf16[512,128]{1,0:T(8,128)(2,1)S(1)} %bitcast.14, bf16[512,128]{1,0:T(8,128)(2,1)S(1)} %bitcast.20, f32[512,128]{1,0:T(8,128)S(1)} %get-tuple-element.33.refs_3_, ...), custom_call_target="tpu_custom_call" | custom-call | flops 335544320 | bytes 524288 | tf_op jit(solution)/shard_map/pallas_call | solution.py:414
  26.2 2.0 %collective-permute-done.10.refs_2_ = bf16[64,1024]{1,0:T(8,128)(2,1)S(1)} collective-permute-done((bf16[64,1024]{1,0:T(8,128)(2,1)S(1)}, bf16[64,1024]{1,0:T(8,128)(2,1)S(1)}, u32[]{:S(2)}, u32[]{:S(2)}) %collective-permute-start.10) | collective-permute-done | bytes 131104 | tf_op jit(solution)/shard_map/ppermute | solution.py:32
  29.0 1.2 %collective-permute-start.9 = (bf16[128,1024]{1,0:T(8,128)(2,1)S(1)}, bf16[128,1024]{1,0:T(8,128)(2,1)S(1)}, u32[]{:S(2)}, u32[]{:S(2)}) collective-permute-start(bf16[128,1024]{1,0:T(8,128)(2,1)S(1)} %collective-permute-done.8.refs_0_), channel_id=1, source_target_pairs={{1,0},{0,1},{3,2},{2,3},{5,4},{4,5},{7,6},{6,7},{9,8},{8,9},{11,10... | collective-permute-start | bytes 786440 | tf_op jit(solution)/shard_map/ppermute | solution.py:395
  30.2 0.7 shard_map.118
  30.9 1.0 %shard_map.119 = (bf16[512,128]{1,0:T(8,128)(2,1)S(1)}, f32[512,128]{1,0:T(8,128)S(1)}, f32[512,128]{1,0:T(8,128)S(1)}, bf16[256,256]{1,0:T(8,128)(2,1)S(1)}) custom-call(bf16[1088,128]{1,0:T(8,128)(2,1)S(1)} %collective-permute-done.3.refs_0_, bf16[512,128]{1,0:T(8,128)(2,1)S(1)} %bitcast.16, bf16[512,128]{1,0:T(8,128)(2,1)S(1)} %bitcast.22, ...), custom_call_target="tpu_custom_call" | custom-call | flops 335544320 | bytes 524288 | tf_op jit(solution)/shard_map/pallas_call | solution.py:414
  31.9 1.3 %collective-permute-start.16 = (bf16[256,256]{1,0:T(8,128)(2,1)S(1)}, bf16[256,256]{1,0:T(8,128)(2,1)S(1)}, u32[]{:S(2)}, u32[]{:S(2)}) collective-permute-start(bf16[256,256]{1,0:T(8,128)(2,1)S(1)} %get-tuple-element.49.refs_8_), channel_id=1, source_target_pairs={{0,4},{2,6},{4,0},{6,2},{8,12},{10,14},{12,8},{14,10},{16,20},{18,... | collective-permute-start | bytes 393224 | tf_op jit(solution)/shard_map/ppermute | solution.py:32
  33.2 0.8 %collective-permute-done.12.refs_4_ = bf16[64,1024]{1,0:T(8,128)(2,1)S(1)} collective-permute-done((bf16[64,1024]{1,0:T(8,128)(2,1)S(1)}, bf16[64,1024]{1,0:T(8,128)(2,1)S(1)}, u32[]{:S(2)}, u32[]{:S(2)}) %collective-permute-start.12) | collective-permute-done | bytes 131104 | tf_op jit(solution)/shard_map/ppermute | solution.py:32
  34.3 0.9 %collective-permute-start.15 = (bf16[256,256]{1,0:T(8,128)(2,1)S(1)}, bf16[256,256]{1,0:T(8,128)(2,1)S(1)}, u32[]{:S(2)}, u32[]{:S(2)}) collective-permute-start(bf16[256,256]{1,0:T(8,128)(2,1)S(1)} %get-tuple-element.49.refs_8_), channel_id=1, source_target_pairs={{0,2},{2,0},{4,6},{6,4},{8,10},{10,8},{12,14},{14,12},{16,18},{18,... | collective-permute-start | bytes 393224 | tf_op jit(solution)/shard_map/ppermute | solution.py:32
  35.2 1.2 %collective-permute-done.16.refs_10_ = bf16[256,256]{1,0:T(8,128)(2,1)S(1)} collective-permute-done((bf16[256,256]{1,0:T(8,128)(2,1)S(1)}, bf16[256,256]{1,0:T(8,128)(2,1)S(1)}, u32[]{:S(2)}, u32[]{:S(2)}) %collective-permute-start.16) | collective-permute-done | bytes 131104 | tf_op jit(solution)/shard_map/ppermute | solution.py:32
  36.4 1.5 %collective-permute-start.17 = (bf16[256,256]{1,0:T(8,128)(2,1)S(1)}, bf16[256,256]{1,0:T(8,128)(2,1)S(1)}, u32[]{:S(2)}, u32[]{:S(2)}) collective-permute-start(bf16[256,256]{1,0:T(8,128)(2,1)S(1)} %collective-permute-done.16.refs_10_), channel_id=1, source_target_pairs={{0,2},{2,0},{4,6},{6,4},{8,10},{10,8},{12,14},{14,12},{16,18},{18,... | collective-permute-start | bytes 393224 | tf_op jit(solution)/shard_map/ppermute | solution.py:32
  37.9 4.2 %collective-permute-done.13.refs_5_ = bf16[64,1024]{1,0:T(8,128)(2,1)S(1)} collective-permute-done((bf16[64,1024]{1,0:T(8,128)(2,1)S(1)}, bf16[64,1024]{1,0:T(8,128)(2,1)S(1)}, u32[]{:S(2)}, u32[]{:S(2)}) %collective-permute-start.13) | collective-permute-done | bytes 131104 | tf_op jit(solution)/shard_map/ppermute | solution.py:395
  42.6 2.3 %collective-permute-start.18 = (bf16[512,256]{1,0:T(8,128)(2,1)S(1)}, bf16[512,256]{1,0:T(8,128)(2,1)S(1)}, u32[]{:S(2)}, u32[]{:S(2)}) collective-permute-start(bf16[512,256]{1,0:T(8,128)(2,1)S(1)} %shard_map.123), channel_id=1, source_target_pairs={{0,8},{2,10},{4,12},{6,14},{8,0},{10,2},{12,4},{14,6},{16,24},{18,... | collective-permute-start | bytes 786440 | tf_op jit(solution)/shard_map/ppermute | solution.py:32
  44.9 1.3 %collective-permute-start = (bf16[1024,128]{1,0:T(8,128)(2,1)S(1)}, bf16[1024,128]{1,0:T(8,128)(2,1)S(1)}, u32[]{:S(2)}, u32[]{:S(2)}) collective-permute-start(bf16[1024,128]{1,0:T(8,128)(2,1)S(1)} %get-tuple-element.29), channel_id=1, source_target_pairs={{0,16},{2,18},{4,20},{6,22},{8,24},{10,26},{12,28},{14,30},{1,17},... | collective-permute-start | bytes 786440 | tf_op jit(solution)/shard_map/ppermute | solution.py:27
  46.2 2.8 %collective-permute-start.7 = (bf16[512,128]{1,0:T(8,128)(2,1)S(1)}, bf16[512,128]{1,0:T(8,128)(2,1)S(1)}, u32[]{:S(2)}, u32[]{:S(2)}) collective-permute-start(bf16[512,128]{1,0:T(8,128)(2,1)S(1)} %get-tuple-element.41), channel_id=1, source_target_pairs={{0,8},{2,10},{4,12},{6,14},{8,16},{10,18},{12,20},{14,22},{16,24},... | collective-permute-start | bytes 393224 | tf_op jit(solution)/shard_map/ppermute | solution.py:22
  49.0 2.4 %collective-permute-start.6 = (bf16[512,128]{1,0:T(8,128)(2,1)S(1)}, bf16[512,128]{1,0:T(8,128)(2,1)S(1)}, u32[]{:S(2)}, u32[]{:S(2)}) collective-permute-start(bf16[512,128]{1,0:T(8,128)(2,1)S(1)} %get-tuple-element.40), channel_id=1, source_target_pairs={{0,4},{2,6},{4,8},{6,10},{8,12},{10,14},{12,16},{14,18},{16,20},{1... | collective-permute-start | bytes 393224 | tf_op jit(solution)/shard_map/ppermute | solution.py:22
  51.4 2.2 %collective-permute-start.5 = (bf16[512,128]{1,0:T(8,128)(2,1)S(1)}, bf16[512,128]{1,0:T(8,128)(2,1)S(1)}, u32[]{:S(2)}, u32[]{:S(2)}) collective-permute-start(bf16[512,128]{1,0:T(8,128)(2,1)S(1)} %get-tuple-element.39), channel_id=1, source_target_pairs={{0,2},{2,4},{4,6},{6,8},{8,10},{10,12},{12,14},{14,16},{16,18},{18... | collective-permute-start | bytes 393224 | tf_op jit(solution)/shard_map/ppermute | solution.py:22
  54.3 6.1 %collective-permute-done.kv_ref = bf16[1024,128]{1,0:T(8,128)(2,1)S(1)} collective-permute-done((bf16[1024,128]{1,0:T(8,128)(2,1)S(1)}, bf16[1024,128]{1,0:T(8,128)(2,1)S(1)}, u32[]{:S(2)}, u32[]{:S(2)}) %collective-permute-start) | collective-permute-done | bytes 262176 | tf_op jit(solution)/shard_map/ppermute | solution.py:27
  60.4 0.7 shard_map.113.dq_ref
  61.1 0.7 copy.12
  62.5 0.8 %shard_map.120 = f32[512,128]{1,0:T(8,128)} custom-call(f32[512,128]{1,0:T(8,128)S(1)} %shard_map.113.dq_ref, bf16[512,128]{1,0:T(8,128)(2,1)S(1)} %collective-permute-done.5.refs_0_, bf16[512,128]{1,0:T(8,128)(2,1)S(1)} %collective-permute-done.6.refs_1_, bf16[512,128]{1,0:T(8,128)(2,1)S(1)} %collective-permute-done.7.refs_2_), custom_call_target="tpu_custom_call" | custom-call | flops 1048576 | bytes 1048576 | tf_op jit(solution)/shard_map/pallas_call | solution.py:472
  63.3 10.9 %collective-permute-done.19.came_ref = bf16[256,256]{1,0:T(8,128)(2,1)S(1)} collective-permute-done((bf16[256,256]{1,0:T(8,128)(2,1)S(1)}, bf16[256,256]{1,0:T(8,128)(2,1)S(1)}, u32[]{:S(2)}, u32[]{:S(2)}) %collective-permute-start.19) | collective-permute-done | bytes 131104 | tf_op jit(solution)/shard_map/ppermute | solution.py:32
  74.2 0.7 shard_map.125
  (29 shorter events, 3.9 us)
Async XLA Ops:
  2.3 20.9 %copy-start = (bf16[256,2,128]{2,1,0:T(2,128)(2,1)S(1)}, bf16[256,2,128]{2,1,0:T(2,128)(2,1)}, u32[]{:S(2)}) copy-start(bf16[256,2,128]{2,1,0:T(2,128)(2,1)} %param.9) | copy-start | bytes 393220
  2.3 20.8 %copy-start.1 = (bf16[256,2,128]{2,1,0:T(2,128)(2,1)S(1)}, bf16[256,2,128]{2,1,0:T(2,128)(2,1)}, u32[]{:S(2)}) copy-start(bf16[256,2,128]{2,1,0:T(2,128)(2,1)} %param.10) | copy-start | bytes 393220
  2.3 7.5 %collective-permute-start.1 = (bf16[1088,128]{1,0:T(8,128)(2,1)S(1)}, bf16[1088,128]{1,0:T(8,128)(2,1)S(1)}, u32[]{:S(2)}, u32[]{:S(2)}) collective-permute-start(bf16[1088,128]{1,0:T(8,128)(2,1)S(1)} %get-tuple-element.28.msg_ref.yes_ref), channel_id=1, source_target_pairs={{8,0},{10,2},{12,4},{14,6},{16,8},{18,10},{20,12},{22,14},{24,16},... | collective-permute-start | bytes 835592 | tf_op jit(solution)/shard_map/ppermute | solution.py:27
  9.9 6.8 %collective-permute-start.2 = (bf16[1088,128]{1,0:T(8,128)(2,1)S(1)}, bf16[1088,128]{1,0:T(8,128)(2,1)S(1)}, u32[]{:S(2)}, u32[]{:S(2)}) collective-permute-start(bf16[1088,128]{1,0:T(8,128)(2,1)S(1)} %shard_map.114), channel_id=1, source_target_pairs={{0,4},{2,6},{4,0},{6,2},{8,12},{10,14},{12,8},{14,10},{16,20},{18,... | collective-permute-start | bytes 835592 | tf_op jit(solution)/shard_map/ppermute | solution.py:32
  10.2 18.8 %collective-permute-start.4 = (bf16[1088,128]{1,0:T(8,128)(2,1)S(1)}, bf16[1088,128]{1,0:T(8,128)(2,1)S(1)}, u32[]{:S(2)}, u32[]{:S(2)}) collective-permute-start(bf16[1088,128]{1,0:T(8,128)(2,1)S(1)} %collective-permute-done.1.no_ref.refs_0_), channel_id=1, source_target_pairs={{0,24},{2,26},{4,28},{6,30},{8,0},{10,2},{12,4},{14,6},{16,8},{18,... | collective-permute-start | bytes 835592 | tf_op jit(solution)/shard_map/ppermute | solution.py:22
  12.4 16.3 %collective-permute-start.8 = (bf16[128,1024]{1,0:T(8,128)(2,1)S(1)}, bf16[128,1024]{1,0:T(8,128)(2,1)S(1)}, u32[]{:S(2)}, u32[]{:S(2)}) collective-permute-start(bf16[128,1024]{1,0:T(8,128)(2,1)S(1)} %get-tuple-element.44), channel_id=1, source_target_pairs={{0,4},{2,6},{4,0},{6,2},{8,12},{10,14},{12,8},{14,10},{16,20},{18,... | collective-permute-start | bytes 786440 | tf_op jit(solution)/shard_map/ppermute | solution.py:32
  16.7 14.2 %collective-permute-start.3 = (bf16[1088,128]{1,0:T(8,128)(2,1)S(1)}, bf16[1088,128]{1,0:T(8,128)(2,1)S(1)}, u32[]{:S(2)}, u32[]{:S(2)}) collective-permute-start(bf16[1088,128]{1,0:T(8,128)(2,1)S(1)} %shard_map.115), channel_id=1, source_target_pairs={{0,2},{2,0},{4,6},{6,4},{8,10},{10,8},{12,14},{14,12},{16,18},{18,... | collective-permute-start | bytes 835592 | tf_op jit(solution)/shard_map/ppermute | solution.py:32
  22.5 19.6 %collective-permute-start.14 = (bf16[256,1024]{1,0:T(8,128)(2,1)S(1)}, bf16[256,1024]{1,0:T(8,128)(2,1)S(1)}, u32[]{:S(2)}, u32[]{:S(2)}) collective-permute-start(bf16[256,1024]{1,0:T(8,128)(2,1)S(1)} %get-tuple-element.47), channel_id=1, source_target_pairs={{0,2},{2,0},{4,6},{6,4},{8,10},{10,8},{12,14},{14,12},{16,18},{18,... | collective-permute-start | bytes 1572872 | tf_op jit(solution)/shard_map/ppermute | solution.py:32
  22.6 5.6 %collective-permute-start.10 = (bf16[64,1024]{1,0:T(8,128)(2,1)S(1)}, bf16[64,1024]{1,0:T(8,128)(2,1)S(1)}, u32[]{:S(2)}, u32[]{:S(2)}) collective-permute-start(bf16[64,1024]{1,0:T(8,128)(2,1)S(1)} %get-tuple-element.45), channel_id=1, source_target_pairs={{0,6},{2,4},{4,2},{6,0},{8,14},{10,12},{12,10},{14,8},{16,22},{18,... | collective-permute-start | bytes 393224 | tf_op jit(solution)/shard_map/ppermute | solution.py:32
  28.2 5.8 %collective-permute-start.12 = (bf16[64,1024]{1,0:T(8,128)(2,1)S(1)}, bf16[64,1024]{1,0:T(8,128)(2,1)S(1)}, u32[]{:S(2)}, u32[]{:S(2)}) collective-permute-start(bf16[64,1024]{1,0:T(8,128)(2,1)S(1)} %get-tuple-element.46), channel_id=1, source_target_pairs={{0,6},{2,4},{4,2},{6,0},{8,14},{10,12},{12,10},{14,8},{16,22},{18,... | collective-permute-start | bytes 393224 | tf_op jit(solution)/shard_map/ppermute | solution.py:32
  28.7 5.6 %collective-permute-start.11 = (bf16[64,1024]{1,0:T(8,128)(2,1)S(1)}, bf16[64,1024]{1,0:T(8,128)(2,1)S(1)}, u32[]{:S(2)}, u32[]{:S(2)}) collective-permute-start(bf16[64,1024]{1,0:T(8,128)(2,1)S(1)} %collective-permute-done.10.refs_2_), channel_id=1, source_target_pairs={{1,0},{0,1},{3,2},{2,3},{5,4},{4,5},{7,6},{6,7},{9,8},{8,9},{11,10... | collective-permute-start | bytes 393224 | tf_op jit(solution)/shard_map/ppermute | solution.py:395
  29.0 13.1 %collective-permute-start.9 = (bf16[128,1024]{1,0:T(8,128)(2,1)S(1)}, bf16[128,1024]{1,0:T(8,128)(2,1)S(1)}, u32[]{:S(2)}, u32[]{:S(2)}) collective-permute-start(bf16[128,1024]{1,0:T(8,128)(2,1)S(1)} %collective-permute-done.8.refs_0_), channel_id=1, source_target_pairs={{1,0},{0,1},{3,2},{2,3},{5,4},{4,5},{7,6},{6,7},{9,8},{8,9},{11,10... | collective-permute-start | bytes 786440 | tf_op jit(solution)/shard_map/ppermute | solution.py:395
  31.9 4.4 %collective-permute-start.16 = (bf16[256,256]{1,0:T(8,128)(2,1)S(1)}, bf16[256,256]{1,0:T(8,128)(2,1)S(1)}, u32[]{:S(2)}, u32[]{:S(2)}) collective-permute-start(bf16[256,256]{1,0:T(8,128)(2,1)S(1)} %get-tuple-element.49.refs_8_), channel_id=1, source_target_pairs={{0,4},{2,6},{4,0},{6,2},{8,12},{10,14},{12,8},{14,10},{16,20},{18,... | collective-permute-start | bytes 393224 | tf_op jit(solution)/shard_map/ppermute | solution.py:32
  34.0 8.1 %collective-permute-start.13 = (bf16[64,1024]{1,0:T(8,128)(2,1)S(1)}, bf16[64,1024]{1,0:T(8,128)(2,1)S(1)}, u32[]{:S(2)}, u32[]{:S(2)}) collective-permute-start(bf16[64,1024]{1,0:T(8,128)(2,1)S(1)} %collective-permute-done.12.refs_4_), channel_id=1, source_target_pairs={{1,0},{0,1},{3,2},{2,3},{5,4},{4,5},{7,6},{6,7},{9,8},{8,9},{11,10... | collective-permute-start | bytes 393224 | tf_op jit(solution)/shard_map/ppermute | solution.py:395
  34.3 7.8 %collective-permute-start.15 = (bf16[256,256]{1,0:T(8,128)(2,1)S(1)}, bf16[256,256]{1,0:T(8,128)(2,1)S(1)}, u32[]{:S(2)}, u32[]{:S(2)}) collective-permute-start(bf16[256,256]{1,0:T(8,128)(2,1)S(1)} %get-tuple-element.49.refs_8_), channel_id=1, source_target_pairs={{0,2},{2,0},{4,6},{6,4},{8,10},{10,8},{12,14},{14,12},{16,18},{18,... | collective-permute-start | bytes 393224 | tf_op jit(solution)/shard_map/ppermute | solution.py:32
  36.4 5.7 %collective-permute-start.17 = (bf16[256,256]{1,0:T(8,128)(2,1)S(1)}, bf16[256,256]{1,0:T(8,128)(2,1)S(1)}, u32[]{:S(2)}, u32[]{:S(2)}) collective-permute-start(bf16[256,256]{1,0:T(8,128)(2,1)S(1)} %collective-permute-done.16.refs_10_), channel_id=1, source_target_pairs={{0,2},{2,0},{4,6},{6,4},{8,10},{10,8},{12,14},{14,12},{16,18},{18,... | collective-permute-start | bytes 393224 | tf_op jit(solution)/shard_map/ppermute | solution.py:32
  42.6 11.5 %collective-permute-start.18 = (bf16[512,256]{1,0:T(8,128)(2,1)S(1)}, bf16[512,256]{1,0:T(8,128)(2,1)S(1)}, u32[]{:S(2)}, u32[]{:S(2)}) collective-permute-start(bf16[512,256]{1,0:T(8,128)(2,1)S(1)} %shard_map.123), channel_id=1, source_target_pairs={{0,8},{2,10},{4,12},{6,14},{8,0},{10,2},{12,4},{14,6},{16,24},{18,... | collective-permute-start | bytes 786440 | tf_op jit(solution)/shard_map/ppermute | solution.py:32
  44.9 15.4 %collective-permute-start = (bf16[1024,128]{1,0:T(8,128)(2,1)S(1)}, bf16[1024,128]{1,0:T(8,128)(2,1)S(1)}, u32[]{:S(2)}, u32[]{:S(2)}) collective-permute-start(bf16[1024,128]{1,0:T(8,128)(2,1)S(1)} %get-tuple-element.29), channel_id=1, source_target_pairs={{0,16},{2,18},{4,20},{6,22},{8,24},{10,26},{12,28},{14,30},{1,17},... | collective-permute-start | bytes 786440 | tf_op jit(solution)/shard_map/ppermute | solution.py:27
  46.2 16.3 %collective-permute-start.7 = (bf16[512,128]{1,0:T(8,128)(2,1)S(1)}, bf16[512,128]{1,0:T(8,128)(2,1)S(1)}, u32[]{:S(2)}, u32[]{:S(2)}) collective-permute-start(bf16[512,128]{1,0:T(8,128)(2,1)S(1)} %get-tuple-element.41), channel_id=1, source_target_pairs={{0,8},{2,10},{4,12},{6,14},{8,16},{10,18},{12,20},{14,22},{16,24},... | collective-permute-start | bytes 393224 | tf_op jit(solution)/shard_map/ppermute | solution.py:22
  49.0 13.5 %collective-permute-start.6 = (bf16[512,128]{1,0:T(8,128)(2,1)S(1)}, bf16[512,128]{1,0:T(8,128)(2,1)S(1)}, u32[]{:S(2)}, u32[]{:S(2)}) collective-permute-start(bf16[512,128]{1,0:T(8,128)(2,1)S(1)} %get-tuple-element.40), channel_id=1, source_target_pairs={{0,4},{2,6},{4,8},{6,10},{8,12},{10,14},{12,16},{14,18},{16,20},{1... | collective-permute-start | bytes 393224 | tf_op jit(solution)/shard_map/ppermute | solution.py:22
  51.4 11.1 %collective-permute-start.5 = (bf16[512,128]{1,0:T(8,128)(2,1)S(1)}, bf16[512,128]{1,0:T(8,128)(2,1)S(1)}, u32[]{:S(2)}, u32[]{:S(2)}) collective-permute-start(bf16[512,128]{1,0:T(8,128)(2,1)S(1)} %get-tuple-element.39), channel_id=1, source_target_pairs={{0,2},{2,4},{4,6},{6,8},{8,10},{10,12},{12,14},{14,16},{16,18},{18... | collective-permute-start | bytes 393224 | tf_op jit(solution)/shard_map/ppermute | solution.py:22
  54.2 20.0 %collective-permute-start.19 = (bf16[256,256]{1,0:T(8,128)(2,1)S(1)}, bf16[256,256]{1,0:T(8,128)(2,1)S(1)}, u32[]{:S(2)}, u32[]{:S(2)}) collective-permute-start(bf16[256,256]{1,0:T(8,128)(2,1)S(1)} %get-tuple-element.51), channel_id=1, source_target_pairs={{0,16},{2,18},{4,20},{6,22},{8,24},{10,26},{12,28},{14,30},{16,0},... | collective-permute-start | bytes 393224 | tf_op jit(solution)/shard_map/ppermute | solution.py:32

commit v4 on v3

--- a/solution.py
+++ b/solution.py
@@ -201,17 +201,21 @@
     dq_out[...] = dq_in[...] + term
 
 
-def own_body(sel, heads, msg_ref, k_ref, v_ref, dk_ref, dv_ref, dq_ref):
+def own_body(sel, heads, msg_ref, kv_ref, dk_ref, dv_ref, dq_ref):
+    rows = kv_ref.shape[0] // 2
+    k_ref, v_ref = kv_ref.at[0:rows, :], kv_ref.at[rows : 2 * rows, :]
     dk_ref[...], dv_ref[...], dq_ref[...] = group_terms(msg_ref, k_ref[...], v_ref[...], 0, heads, sel, True)
 
 
 def far_body(sel, heads, groups, last, sides, *refs):
     count = len(groups)
     msgs = refs[:count]
-    k_ref, v_ref, dk_in, dv_in = refs[count : count + 4]
-    dqs = refs[count + 4 : count + 4 + len(sides)]
-    dk_out, dv_out = refs[count + 4 + len(sides) : count + 6 + len(sides)]
-    rows, dim = k_ref.shape
+    kv_ref, dk_in, dv_in = refs[count : count + 3]
+    rows = kv_ref.shape[0] // 2
+    k_ref, v_ref = kv_ref.at[0:rows, :], kv_ref.at[rows : 2 * rows, :]
+    dqs = refs[count + 3 : count + 3 + len(sides)]
+    dk_out, dv_out = refs[count + 3 + len(sides) : count + 5 + len(sides)]
+    dim = kv_ref.shape[1]
     scale = dim ** (-0.5)
     dk, dv = dk_in[...], dv_in[...]
     for index, group in enumerate(groups):
@@ -397,9 +401,9 @@
     dk_own, dv_own, dq_own = call(
         functools.partial(own_body, sel, heads),
         [shape((rows, dim), F32)] * 3,
-        [VMEM] * 3,
+        [VMEM] * 2,
         pairs, 8 * rows * dim * 4,
-    )(msg, key, value)
+    )(msg, kv)
 
     dq_near = call(
         functools.partial(near_body, sel, heads, levels),
@@ -414,9 +418,9 @@
         return call(
             functools.partial(far_body, sel, heads, groups, last, sides),
             kinds,
-            [VMEM] * (len(groups) + 4),
+            [VMEM] * (len(groups) + 3),
             pairs * len(groups), 8 * rows * dim,
-        )(*[got[group - 1] for group in groups], key, value, dk, dv)
+        )(*[got[group - 1] for group in groups], kv, dk, dv)
 
     back, dk, dv = {}, dk_own, dv_own
     stages = [(3,), (2,), (4,), (1,)] + [(level,) for level in range(5, levels + 1)]

time: 75.2 us -> 75 us (level)
  no operation moved by 1% of the time
where the time goes in v4:
time: 75 us; the launch traced here: 74.8 us
  waiting for transfers between devices  33.5 us (45%)
  starting transfers between devices  27.9 us (37%)
  Pallas kernels  11.2 us (15%)
  local copies, waits for them, and re-layouts  1.41 us (2%)
  between operations  0.79 us (1%)
    ppermute x11, waiting for transfers between devices, swap(): return lax.ppermute(value, 'kv', [(i, i ^ bit) for i in range(count)])  17.9 us
    ppermute x11, starting transfers between devices, swap(): return lax.ppermute(value, 'kv', [(i, i ^ bit) for i in range(count)])  13.3 us
    ppermute x2, waiting for transfers between devices, line(): lax.ppermute(value, 'kv', [(i, i + by) for i in range(count) if 0 <= i +...  11.4 us
    ppermute x4, starting transfers between devices, ring(): lax.ppermute(value, 'kv', [(i, (i + by) % count) for i in range(count)])  9.59 us
    ppermute x3, waiting for transfers between devices, per_device(): lax.ppermute(piece, 'tp', [((i + s) % tp, i) for i in range(tp)])  4.19 us
    pallas_call x4, Pallas kernels, far_call(): call(functools.partial(far_body, sel, heads, groups, last, sides), kinds,...  3.62 us
    ppermute x2, starting transfers between devices, line(): lax.ppermute(value, 'kv', [(i, i + by) for i in range(count) if 0 <= i +...  3.37 us
    ppermute x3, starting transfers between devices, per_device(): lax.ppermute(piece, 'tp', [((i + s) % tp, i) for i in range(tp)])  1.72 us
  transfers between devices with their start and end apart: 20, of which 8 were waited for; matrix products, arithmetic and copies ran while one was open for 2% of the time, Pallas kernels for 11%

profile of v4, /device:TPU:31, one launch (start us, length us, event | category | flops | bytes accessed | tf_op | source)
XLA Modules:
  0.0 74.8 jit_solution(3401579230591506088)
XLA Ops:
  0.6 1.7 %shard_map.111 = (bf16[1088,128]{1,0:T(8,128)(2,1)S(1)}, bf16[1024,128]{1,0:T(8,128)(2,1)S(1)}, bf16[128,1024]{1,0:T(8,128)(2,1)S(1)}, bf16[64,1024]{1,0:T(8,128)(2,1)S(1)}, bf16[64,1024]{1,0:T(8,128)(2,1)S(1)}) custom-call(s32[2,16]{1,0:T(2,128)} %picked_hbm.1, bf16[512,128]{1,0:T(8,128)(2,1)} %bitcast.12, bf16[512,128]{1,0:T(8,128)(2,1)} %bitcast.13, ...), custom_call_target="tpu_custom_call" | custom-call | tf_op jit(solution)/shard_map/pallas_call | solution.py:355
  2.3 2.1 %collective-permute-start.1 = (bf16[1088,128]{1,0:T(8,128)(2,1)S(1)}, bf16[1088,128]{1,0:T(8,128)(2,1)S(1)}, u32[]{:S(2)}, u32[]{:S(2)}) collective-permute-start(bf16[1088,128]{1,0:T(8,128)(2,1)S(1)} %get-tuple-element.28.msg_ref.yes_ref), channel_id=1, source_target_pairs={{8,0},{10,2},{12,4},{14,6},{16,8},{18,10},{20,12},{22,14},{24,16},... | collective-permute-start | bytes 835592 | tf_op jit(solution)/shard_map/ppermute | solution.py:27
  4.4 5.3 %collective-permute-done.1.no_ref.refs_0_ = bf16[1088,128]{1,0:T(8,128)(2,1)S(1)} collective-permute-done((bf16[1088,128]{1,0:T(8,128)(2,1)S(1)}, bf16[1088,128]{1,0:T(8,128)(2,1)S(1)}, u32[]{:S(2)}, u32[]{:S(2)}) %collective-permute-start.1) | collective-permute-done | bytes 278560 | tf_op jit(solution)/shard_map/ppermute | solution.py:27
  10.0 2.2 %collective-permute-start.4 = (bf16[1088,128]{1,0:T(8,128)(2,1)S(1)}, bf16[1088,128]{1,0:T(8,128)(2,1)S(1)}, u32[]{:S(2)}, u32[]{:S(2)}) collective-permute-start(bf16[1088,128]{1,0:T(8,128)(2,1)S(1)} %collective-permute-done.1.no_ref.refs_0_), channel_id=1, source_target_pairs={{0,24},{2,26},{4,28},{6,30},{8,0},{10,2},{12,4},{14,6},{16,8},{18,... | collective-permute-start | bytes 835592 | tf_op jit(solution)/shard_map/ppermute | solution.py:22
  12.2 1.2 %collective-permute-start.8 = (bf16[128,1024]{1,0:T(8,128)(2,1)S(1)}, bf16[128,1024]{1,0:T(8,128)(2,1)S(1)}, u32[]{:S(2)}, u32[]{:S(2)}) collective-permute-start(bf16[128,1024]{1,0:T(8,128)(2,1)S(1)} %get-tuple-element.44), channel_id=1, source_target_pairs={{0,4},{2,6},{4,0},{6,2},{8,12},{10,14},{12,8},{14,10},{16,20},{18,... | collective-permute-start | bytes 786440 | tf_op jit(solution)/shard_map/ppermute | solution.py:32
  13.5 3.0 %collective-permute-done.2.no_ref.refs_0_ = bf16[1088,128]{1,0:T(8,128)(2,1)S(1)} collective-permute-done((bf16[1088,128]{1,0:T(8,128)(2,1)S(1)}, bf16[1088,128]{1,0:T(8,128)(2,1)S(1)}, u32[]{:S(2)}, u32[]{:S(2)}) %collective-permute-start.2) | collective-permute-done | bytes 278560 | tf_op jit(solution)/shard_map/ppermute | solution.py:32
  16.5 4.4 %collective-permute-start.3 = (bf16[1088,128]{1,0:T(8,128)(2,1)S(1)}, bf16[1088,128]{1,0:T(8,128)(2,1)S(1)}, u32[]{:S(2)}, u32[]{:S(2)}) collective-permute-start(bf16[1088,128]{1,0:T(8,128)(2,1)S(1)} %shard_map.115), channel_id=1, source_target_pairs={{0,2},{2,0},{4,6},{6,4},{8,10},{10,8},{12,14},{14,12},{16,18},{18,... | collective-permute-start | bytes 835592 | tf_op jit(solution)/shard_map/ppermute | solution.py:32
  21.0 1.4 %shard_map.121 = (bf16[256,1024]{1,0:T(8,128)(2,1)S(1)}, bf16[256,1024]{1,0:T(8,128)(2,1)S(1)}) custom-call(bf16[256,4096]{1,0:T(8,128)(2,1)} %x_hbm.3), custom_call_target="tpu_custom_call" | custom-call | flops 1048576 | bytes 1048576 | tf_op jit(solution)/shard_map/pallas_call | solution.py:380
  23.0 1.1 %shard_map.112 = (f32[512,128]{1,0:T(8,128)S(1)}, f32[512,128]{1,0:T(8,128)S(1)}, f32[512,128]{1,0:T(8,128)S(1)}) custom-call(bf16[1088,128]{1,0:T(8,128)(2,1)S(1)} %get-tuple-element.28.msg_ref.yes_ref, bf16[1024,128]{1,0:T(8,128)(2,1)S(1)} %get-tuple-element.29.kv_ref.refs_1_), custom_call_target="tpu_custom_call" | custom-call | flops 335544320 | bytes 2097152 | tf_op jit(solution)/shard_map/pallas_call | solution.py:401
  24.1 0.9 %shard_map.116 = (bf16[512,128]{1,0:T(8,128)(2,1)S(1)}, f32[512,128]{1,0:T(8,128)S(1)}, f32[512,128]{1,0:T(8,128)S(1)}) custom-call(bf16[1088,128]{1,0:T(8,128)(2,1)S(1)} %collective-permute-done.1.no_ref.refs_0_, bf16[1024,128]{1,0:T(8,128)(2,1)S(1)} %get-tuple-element.29.kv_ref.refs_1_, f32[512,128]{1,0:T(8,128)S(1)} %get-tuple-element.31.refs_2_, ...), custom_call_target="tpu_custom_call" | custom-call | flops 335544320 | bytes 524288 | tf_op jit(solution)/shard_map/pallas_call | solution.py:418
  25.1 0.9 %shard_map.117 = (bf16[512,128]{1,0:T(8,128)(2,1)S(1)}, f32[512,128]{1,0:T(8,128)S(1)}, f32[512,128]{1,0:T(8,128)S(1)}) custom-call(bf16[1088,128]{1,0:T(8,128)(2,1)S(1)} %collective-permute-done.2.no_ref.refs_0_, bf16[1024,128]{1,0:T(8,128)(2,1)S(1)} %get-tuple-element.29.kv_ref.refs_1_, f32[512,128]{1,0:T(8,128)S(1)} %get-tuple-element.33.refs_2_, ...), custom_call_target="tpu_custom_call" | custom-call | flops 335544320 | bytes 524288 | tf_op jit(solution)/shard_map/pallas_call | solution.py:418
  26.0 2.0 %collective-permute-done.10.refs_2_ = bf16[64,1024]{1,0:T(8,128)(2,1)S(1)} collective-permute-done((bf16[64,1024]{1,0:T(8,128)(2,1)S(1)}, bf16[64,1024]{1,0:T(8,128)(2,1)S(1)}, u32[]{:S(2)}, u32[]{:S(2)}) %collective-permute-start.10) | collective-permute-done | bytes 131104 | tf_op jit(solution)/shard_map/ppermute | solution.py:32
  28.8 1.2 %collective-permute-start.9 = (bf16[128,1024]{1,0:T(8,128)(2,1)S(1)}, bf16[128,1024]{1,0:T(8,128)(2,1)S(1)}, u32[]{:S(2)}, u32[]{:S(2)}) collective-permute-start(bf16[128,1024]{1,0:T(8,128)(2,1)S(1)} %collective-permute-done.8.refs_0_), channel_id=1, source_target_pairs={{1,0},{0,1},{3,2},{2,3},{5,4},{4,5},{7,6},{6,7},{9,8},{8,9},{11,10... | collective-permute-start | bytes 786440 | tf_op jit(solution)/shard_map/ppermute | solution.py:399
  30.0 0.7 shard_map.118
  30.8 1.0 %shard_map.119 = (bf16[512,128]{1,0:T(8,128)(2,1)S(1)}, f32[512,128]{1,0:T(8,128)S(1)}, f32[512,128]{1,0:T(8,128)S(1)}, bf16[256,256]{1,0:T(8,128)(2,1)S(1)}) custom-call(bf16[1088,128]{1,0:T(8,128)(2,1)S(1)} %collective-permute-done.3.refs_0_, bf16[1024,128]{1,0:T(8,128)(2,1)S(1)} %get-tuple-element.29.kv_ref.refs_1_, ...), custom_call_target="tpu_custom_call" | custom-call | flops 335544320 | bytes 524288 | tf_op jit(solution)/shard_map/pallas_call | solution.py:418
  31.8 1.3 %collective-permute-start.16 = (bf16[256,256]{1,0:T(8,128)(2,1)S(1)}, bf16[256,256]{1,0:T(8,128)(2,1)S(1)}, u32[]{:S(2)}, u32[]{:S(2)}) collective-permute-start(bf16[256,256]{1,0:T(8,128)(2,1)S(1)} %get-tuple-element.49.refs_8_), channel_id=1, source_target_pairs={{0,4},{2,6},{4,0},{6,2},{8,12},{10,14},{12,8},{14,10},{16,20},{18,... | collective-permute-start | bytes 393224 | tf_op jit(solution)/shard_map/ppermute | solution.py:32
  33.1 0.8 %collective-permute-done.12.refs_4_ = bf16[64,1024]{1,0:T(8,128)(2,1)S(1)} collective-permute-done((bf16[64,1024]{1,0:T(8,128)(2,1)S(1)}, bf16[64,1024]{1,0:T(8,128)(2,1)S(1)}, u32[]{:S(2)}, u32[]{:S(2)}) %collective-permute-start.12) | collective-permute-done | bytes 131104 | tf_op jit(solution)/shard_map/ppermute | solution.py:32
  34.1 0.9 %collective-permute-start.15 = (bf16[256,256]{1,0:T(8,128)(2,1)S(1)}, bf16[256,256]{1,0:T(8,128)(2,1)S(1)}, u32[]{:S(2)}, u32[]{:S(2)}) collective-permute-start(bf16[256,256]{1,0:T(8,128)(2,1)S(1)} %get-tuple-element.49.refs_8_), channel_id=1, source_target_pairs={{0,2},{2,0},{4,6},{6,4},{8,10},{10,8},{12,14},{14,12},{16,18},{18,... | collective-permute-start | bytes 393224 | tf_op jit(solution)/shard_map/ppermute | solution.py:32
  35.0 1.2 %collective-permute-done.16.refs_10_ = bf16[256,256]{1,0:T(8,128)(2,1)S(1)} collective-permute-done((bf16[256,256]{1,0:T(8,128)(2,1)S(1)}, bf16[256,256]{1,0:T(8,128)(2,1)S(1)}, u32[]{:S(2)}, u32[]{:S(2)}) %collective-permute-start.16) | collective-permute-done | bytes 131104 | tf_op jit(solution)/shard_map/ppermute | solution.py:32
  36.2 1.5 %collective-permute-start.17 = (bf16[256,256]{1,0:T(8,128)(2,1)S(1)}, bf16[256,256]{1,0:T(8,128)(2,1)S(1)}, u32[]{:S(2)}, u32[]{:S(2)}) collective-permute-start(bf16[256,256]{1,0:T(8,128)(2,1)S(1)} %collective-permute-done.16.refs_10_), channel_id=1, source_target_pairs={{0,2},{2,0},{4,6},{6,4},{8,10},{10,8},{12,14},{14,12},{16,18},{18,... | collective-permute-start | bytes 393224 | tf_op jit(solution)/shard_map/ppermute | solution.py:32
  37.7 4.2 %collective-permute-done.13.refs_5_ = bf16[64,1024]{1,0:T(8,128)(2,1)S(1)} collective-permute-done((bf16[64,1024]{1,0:T(8,128)(2,1)S(1)}, bf16[64,1024]{1,0:T(8,128)(2,1)S(1)}, u32[]{:S(2)}, u32[]{:S(2)}) %collective-permute-start.13) | collective-permute-done | bytes 131104 | tf_op jit(solution)/shard_map/ppermute | solution.py:399
  42.5 2.3 %collective-permute-start.18 = (bf16[512,256]{1,0:T(8,128)(2,1)S(1)}, bf16[512,256]{1,0:T(8,128)(2,1)S(1)}, u32[]{:S(2)}, u32[]{:S(2)}) collective-permute-start(bf16[512,256]{1,0:T(8,128)(2,1)S(1)} %shard_map.123), channel_id=1, source_target_pairs={{0,8},{2,10},{4,12},{6,14},{8,0},{10,2},{12,4},{14,6},{16,24},{18,... | collective-permute-start | bytes 786440 | tf_op jit(solution)/shard_map/ppermute | solution.py:32
  44.8 1.3 %collective-permute-start = (bf16[1024,128]{1,0:T(8,128)(2,1)S(1)}, bf16[1024,128]{1,0:T(8,128)(2,1)S(1)}, u32[]{:S(2)}, u32[]{:S(2)}) collective-permute-start(bf16[1024,128]{1,0:T(8,128)(2,1)S(1)} %get-tuple-element.29.kv_ref.refs_1_), channel_id=1, source_target_pairs={{0,16},{2,18},{4,20},{6,22},{8,24},{10,26},{12,28},{14,30},{1,17},... | collective-permute-start | bytes 786440 | tf_op jit(solution)/shard_map/ppermute | solution.py:27
  46.0 2.8 %collective-permute-start.7 = (bf16[512,128]{1,0:T(8,128)(2,1)S(1)}, bf16[512,128]{1,0:T(8,128)(2,1)S(1)}, u32[]{:S(2)}, u32[]{:S(2)}) collective-permute-start(bf16[512,128]{1,0:T(8,128)(2,1)S(1)} %get-tuple-element.41), channel_id=1, source_target_pairs={{0,8},{2,10},{4,12},{6,14},{8,16},{10,18},{12,20},{14,22},{16,24},... | collective-permute-start | bytes 393224 | tf_op jit(solution)/shard_map/ppermute | solution.py:22
  48.8 2.4 %collective-permute-start.6 = (bf16[512,128]{1,0:T(8,128)(2,1)S(1)}, bf16[512,128]{1,0:T(8,128)(2,1)S(1)}, u32[]{:S(2)}, u32[]{:S(2)}) collective-permute-start(bf16[512,128]{1,0:T(8,128)(2,1)S(1)} %get-tuple-element.40), channel_id=1, source_target_pairs={{0,4},{2,6},{4,8},{6,10},{8,12},{10,14},{12,16},{14,18},{16,20},{1... | collective-permute-start | bytes 393224 | tf_op jit(solution)/shard_map/ppermute | solution.py:22
  51.2 2.2 %collective-permute-start.5 = (bf16[512,128]{1,0:T(8,128)(2,1)S(1)}, bf16[512,128]{1,0:T(8,128)(2,1)S(1)}, u32[]{:S(2)}, u32[]{:S(2)}) collective-permute-start(bf16[512,128]{1,0:T(8,128)(2,1)S(1)} %get-tuple-element.39), channel_id=1, source_target_pairs={{0,2},{2,4},{4,6},{6,8},{8,10},{10,12},{12,14},{14,16},{16,18},{18... | collective-permute-start | bytes 393224 | tf_op jit(solution)/shard_map/ppermute | solution.py:22
  54.1 6.1 %collective-permute-done.kv_ref = bf16[1024,128]{1,0:T(8,128)(2,1)S(1)} collective-permute-done((bf16[1024,128]{1,0:T(8,128)(2,1)S(1)}, bf16[1024,128]{1,0:T(8,128)(2,1)S(1)}, u32[]{:S(2)}, u32[]{:S(2)}) %collective-permute-start) | collective-permute-done | bytes 262176 | tf_op jit(solution)/shard_map/ppermute | solution.py:27
  60.2 0.7 shard_map.113.dq_ref
  61.0 0.7 copy.12
  62.4 0.8 %shard_map.120 = f32[512,128]{1,0:T(8,128)} custom-call(f32[512,128]{1,0:T(8,128)S(1)} %shard_map.113.dq_ref, bf16[512,128]{1,0:T(8,128)(2,1)S(1)} %collective-permute-done.5.refs_0_, bf16[512,128]{1,0:T(8,128)(2,1)S(1)} %collective-permute-done.6.refs_1_, bf16[512,128]{1,0:T(8,128)(2,1)S(1)} %collective-permute-done.7.refs_2_), custom_call_target="tpu_custom_call" | custom-call | flops 1048576 | bytes 1048576 | tf_op jit(solution)/shard_map/pallas_call | solution.py:476
  63.1 10.9 %collective-permute-done.19.came_ref = bf16[256,256]{1,0:T(8,128)(2,1)S(1)} collective-permute-done((bf16[256,256]{1,0:T(8,128)(2,1)S(1)}, bf16[256,256]{1,0:T(8,128)(2,1)S(1)}, u32[]{:S(2)}, u32[]{:S(2)}) %collective-permute-start.19) | collective-permute-done | bytes 131104 | tf_op jit(solution)/shard_map/ppermute | solution.py:32
  74.1 0.7 shard_map.125
  (25 shorter events, 3.9 us)
Async XLA Ops:
  2.3 7.4 %collective-permute-start.1 = (bf16[1088,128]{1,0:T(8,128)(2,1)S(1)}, bf16[1088,128]{1,0:T(8,128)(2,1)S(1)}, u32[]{:S(2)}, u32[]{:S(2)}) collective-permute-start(bf16[1088,128]{1,0:T(8,128)(2,1)S(1)} %get-tuple-element.28.msg_ref.yes_ref), channel_id=1, source_target_pairs={{8,0},{10,2},{12,4},{14,6},{16,8},{18,10},{20,12},{22,14},{24,16},... | collective-permute-start | bytes 835592 | tf_op jit(solution)/shard_map/ppermute | solution.py:27
  9.7 6.8 %collective-permute-start.2 = (bf16[1088,128]{1,0:T(8,128)(2,1)S(1)}, bf16[1088,128]{1,0:T(8,128)(2,1)S(1)}, u32[]{:S(2)}, u32[]{:S(2)}) collective-permute-start(bf16[1088,128]{1,0:T(8,128)(2,1)S(1)} %shard_map.114), channel_id=1, source_target_pairs={{0,4},{2,6},{4,0},{6,2},{8,12},{10,14},{12,8},{14,10},{16,20},{18,... | collective-permute-start | bytes 835592 | tf_op jit(solution)/shard_map/ppermute | solution.py:32
  10.0 18.8 %collective-permute-start.4 = (bf16[1088,128]{1,0:T(8,128)(2,1)S(1)}, bf16[1088,128]{1,0:T(8,128)(2,1)S(1)}, u32[]{:S(2)}, u32[]{:S(2)}) collective-permute-start(bf16[1088,128]{1,0:T(8,128)(2,1)S(1)} %collective-permute-done.1.no_ref.refs_0_), channel_id=1, source_target_pairs={{0,24},{2,26},{4,28},{6,30},{8,0},{10,2},{12,4},{14,6},{16,8},{18,... | collective-permute-start | bytes 835592 | tf_op jit(solution)/shard_map/ppermute | solution.py:22
  12.2 16.3 %collective-permute-start.8 = (bf16[128,1024]{1,0:T(8,128)(2,1)S(1)}, bf16[128,1024]{1,0:T(8,128)(2,1)S(1)}, u32[]{:S(2)}, u32[]{:S(2)}) collective-permute-start(bf16[128,1024]{1,0:T(8,128)(2,1)S(1)} %get-tuple-element.44), channel_id=1, source_target_pairs={{0,4},{2,6},{4,0},{6,2},{8,12},{10,14},{12,8},{14,10},{16,20},{18,... | collective-permute-start | bytes 786440 | tf_op jit(solution)/shard_map/ppermute | solution.py:32
  16.5 14.2 %collective-permute-start.3 = (bf16[1088,128]{1,0:T(8,128)(2,1)S(1)}, bf16[1088,128]{1,0:T(8,128)(2,1)S(1)}, u32[]{:S(2)}, u32[]{:S(2)}) collective-permute-start(bf16[1088,128]{1,0:T(8,128)(2,1)S(1)} %shard_map.115), channel_id=1, source_target_pairs={{0,2},{2,0},{4,6},{6,4},{8,10},{10,8},{12,14},{14,12},{16,18},{18,... | collective-permute-start | bytes 835592 | tf_op jit(solution)/shard_map/ppermute | solution.py:32
  22.3 19.6 %collective-permute-start.14 = (bf16[256,1024]{1,0:T(8,128)(2,1)S(1)}, bf16[256,1024]{1,0:T(8,128)(2,1)S(1)}, u32[]{:S(2)}, u32[]{:S(2)}) collective-permute-start(bf16[256,1024]{1,0:T(8,128)(2,1)S(1)} %get-tuple-element.47), channel_id=1, source_target_pairs={{0,2},{2,0},{4,6},{6,4},{8,10},{10,8},{12,14},{14,12},{16,18},{18,... | collective-permute-start | bytes 1572872 | tf_op jit(solution)/shard_map/ppermute | solution.py:32
  22.4 5.6 %collective-permute-start.10 = (bf16[64,1024]{1,0:T(8,128)(2,1)S(1)}, bf16[64,1024]{1,0:T(8,128)(2,1)S(1)}, u32[]{:S(2)}, u32[]{:S(2)}) collective-permute-start(bf16[64,1024]{1,0:T(8,128)(2,1)S(1)} %get-tuple-element.45), channel_id=1, source_target_pairs={{0,6},{2,4},{4,2},{6,0},{8,14},{10,12},{12,10},{14,8},{16,22},{18,... | collective-permute-start | bytes 393224 | tf_op jit(solution)/shard_map/ppermute | solution.py:32
  28.0 5.8 %collective-permute-start.12 = (bf16[64,1024]{1,0:T(8,128)(2,1)S(1)}, bf16[64,1024]{1,0:T(8,128)(2,1)S(1)}, u32[]{:S(2)}, u32[]{:S(2)}) collective-permute-start(bf16[64,1024]{1,0:T(8,128)(2,1)S(1)} %get-tuple-element.46), channel_id=1, source_target_pairs={{0,6},{2,4},{4,2},{6,0},{8,14},{10,12},{12,10},{14,8},{16,22},{18,... | collective-permute-start | bytes 393224 | tf_op jit(solution)/shard_map/ppermute | solution.py:32
  28.5 5.6 %collective-permute-start.11 = (bf16[64,1024]{1,0:T(8,128)(2,1)S(1)}, bf16[64,1024]{1,0:T(8,128)(2,1)S(1)}, u32[]{:S(2)}, u32[]{:S(2)}) collective-permute-start(bf16[64,1024]{1,0:T(8,128)(2,1)S(1)} %collective-permute-done.10.refs_2_), channel_id=1, source_target_pairs={{1,0},{0,1},{3,2},{2,3},{5,4},{4,5},{7,6},{6,7},{9,8},{8,9},{11,10... | collective-permute-start | bytes 393224 | tf_op jit(solution)/shard_map/ppermute | solution.py:399
  28.8 13.1 %collective-permute-start.9 = (bf16[128,1024]{1,0:T(8,128)(2,1)S(1)}, bf16[128,1024]{1,0:T(8,128)(2,1)S(1)}, u32[]{:S(2)}, u32[]{:S(2)}) collective-permute-start(bf16[128,1024]{1,0:T(8,128)(2,1)S(1)} %collective-permute-done.8.refs_0_), channel_id=1, source_target_pairs={{1,0},{0,1},{3,2},{2,3},{5,4},{4,5},{7,6},{6,7},{9,8},{8,9},{11,10... | collective-permute-start | bytes 786440 | tf_op jit(solution)/shard_map/ppermute | solution.py:399
  31.8 4.4 %collective-permute-start.16 = (bf16[256,256]{1,0:T(8,128)(2,1)S(1)}, bf16[256,256]{1,0:T(8,128)(2,1)S(1)}, u32[]{:S(2)}, u32[]{:S(2)}) collective-permute-start(bf16[256,256]{1,0:T(8,128)(2,1)S(1)} %get-tuple-element.49.refs_8_), channel_id=1, source_target_pairs={{0,4},{2,6},{4,0},{6,2},{8,12},{10,14},{12,8},{14,10},{16,20},{18,... | collective-permute-start | bytes 393224 | tf_op jit(solution)/shard_map/ppermute | solution.py:32
  33.8 8.1 %collective-permute-start.13 = (bf16[64,1024]{1,0:T(8,128)(2,1)S(1)}, bf16[64,1024]{1,0:T(8,128)(2,1)S(1)}, u32[]{:S(2)}, u32[]{:S(2)}) collective-permute-start(bf16[64,1024]{1,0:T(8,128)(2,1)S(1)} %collective-permute-done.12.refs_4_), channel_id=1, source_target_pairs={{1,0},{0,1},{3,2},{2,3},{5,4},{4,5},{7,6},{6,7},{9,8},{8,9},{11,10... | collective-permute-start | bytes 393224 | tf_op jit(solution)/shard_map/ppermute | solution.py:399
  34.1 7.8 %collective-permute-start.15 = (bf16[256,256]{1,0:T(8,128)(2,1)S(1)}, bf16[256,256]{1,0:T(8,128)(2,1)S(1)}, u32[]{:S(2)}, u32[]{:S(2)}) collective-permute-start(bf16[256,256]{1,0:T(8,128)(2,1)S(1)} %get-tuple-element.49.refs_8_), channel_id=1, source_target_pairs={{0,2},{2,0},{4,6},{6,4},{8,10},{10,8},{12,14},{14,12},{16,18},{18,... | collective-permute-start | bytes 393224 | tf_op jit(solution)/shard_map/ppermute | solution.py:32
  36.2 5.7 %collective-permute-start.17 = (bf16[256,256]{1,0:T(8,128)(2,1)S(1)}, bf16[256,256]{1,0:T(8,128)(2,1)S(1)}, u32[]{:S(2)}, u32[]{:S(2)}) collective-permute-start(bf16[256,256]{1,0:T(8,128)(2,1)S(1)} %collective-permute-done.16.refs_10_), channel_id=1, source_target_pairs={{0,2},{2,0},{4,6},{6,4},{8,10},{10,8},{12,14},{14,12},{16,18},{18,... | collective-permute-start | bytes 393224 | tf_op jit(solution)/shard_map/ppermute | solution.py:32
  42.5 11.5 %collective-permute-start.18 = (bf16[512,256]{1,0:T(8,128)(2,1)S(1)}, bf16[512,256]{1,0:T(8,128)(2,1)S(1)}, u32[]{:S(2)}, u32[]{:S(2)}) collective-permute-start(bf16[512,256]{1,0:T(8,128)(2,1)S(1)} %shard_map.123), channel_id=1, source_target_pairs={{0,8},{2,10},{4,12},{6,14},{8,0},{10,2},{12,4},{14,6},{16,24},{18,... | collective-permute-start | bytes 786440 | tf_op jit(solution)/shard_map/ppermute | solution.py:32
  44.8 15.5 %collective-permute-start = (bf16[1024,128]{1,0:T(8,128)(2,1)S(1)}, bf16[1024,128]{1,0:T(8,128)(2,1)S(1)}, u32[]{:S(2)}, u32[]{:S(2)}) collective-permute-start(bf16[1024,128]{1,0:T(8,128)(2,1)S(1)} %get-tuple-element.29.kv_ref.refs_1_), channel_id=1, source_target_pairs={{0,16},{2,18},{4,20},{6,22},{8,24},{10,26},{12,28},{14,30},{1,17},... | collective-permute-start | bytes 786440 | tf_op jit(solution)/shard_map/ppermute | solution.py:27
  46.0 16.3 %collective-permute-start.7 = (bf16[512,128]{1,0:T(8,128)(2,1)S(1)}, bf16[512,128]{1,0:T(8,128)(2,1)S(1)}, u32[]{:S(2)}, u32[]{:S(2)}) collective-permute-start(bf16[512,128]{1,0:T(8,128)(2,1)S(1)} %get-tuple-element.41), channel_id=1, source_target_pairs={{0,8},{2,10},{4,12},{6,14},{8,16},{10,18},{12,20},{14,22},{16,24},... | collective-permute-start | bytes 393224 | tf_op jit(solution)/shard_map/ppermute | solution.py:22
  48.8 13.5 %collective-permute-start.6 = (bf16[512,128]{1,0:T(8,128)(2,1)S(1)}, bf16[512,128]{1,0:T(8,128)(2,1)S(1)}, u32[]{:S(2)}, u32[]{:S(2)}) collective-permute-start(bf16[512,128]{1,0:T(8,128)(2,1)S(1)} %get-tuple-element.40), channel_id=1, source_target_pairs={{0,4},{2,6},{4,8},{6,10},{8,12},{10,14},{12,16},{14,18},{16,20},{1... | collective-permute-start | bytes 393224 | tf_op jit(solution)/shard_map/ppermute | solution.py:22
  51.2 11.1 %collective-permute-start.5 = (bf16[512,128]{1,0:T(8,128)(2,1)S(1)}, bf16[512,128]{1,0:T(8,128)(2,1)S(1)}, u32[]{:S(2)}, u32[]{:S(2)}) collective-permute-start(bf16[512,128]{1,0:T(8,128)(2,1)S(1)} %get-tuple-element.39), channel_id=1, source_target_pairs={{0,2},{2,4},{4,6},{6,8},{8,10},{10,12},{12,14},{14,16},{16,18},{18... | collective-permute-start | bytes 393224 | tf_op jit(solution)/shard_map/ppermute | solution.py:22
  54.0 20.0 %collective-permute-start.19 = (bf16[256,256]{1,0:T(8,128)(2,1)S(1)}, bf16[256,256]{1,0:T(8,128)(2,1)S(1)}, u32[]{:S(2)}, u32[]{:S(2)}) collective-permute-start(bf16[256,256]{1,0:T(8,128)(2,1)S(1)} %get-tuple-element.51), channel_id=1, source_target_pairs={{0,16},{2,18},{4,20},{6,22},{8,24},{10,26},{12,28},{14,30},{16,0},... | collective-permute-start | bytes 393224 | tf_op jit(solution)/shard_map/ppermute | solution.py:32
